TPU v7x, 128 devices: a whole 4x4x4 slice. The times are simulated.
128 devices in a mesh: sp: 64 (over z, y, x), tp: 2 (over core).
Axes of the slice: x: 4, y: 4, z: 4, core: 2. Of those that a mesh axis runs over, the one named last changes fastest.
Arguments:
- gate_pre: bfloat16 [16384, 2048], P('sp', 'tp'), may hold values from -6 to 6
- conv_in: bfloat16 [16384, 2048], P('sp', 'tp'), may hold values from -6 to 6
- conv_taps: bfloat16 [4, 2048], P(None, 'tp'), may hold values from -3 to 3
- recur_map: bfloat16 [8, 256, 256], P('tp'), may hold values from -0.375 to 0.375
- input_map: bfloat16 [8, 256, 256], P('tp'), may hold values from -0.375 to 0.375
- rate_logit: float32 [2048], P('tp'), may hold values from 4.5 to 15
- decay_shift: float32 [16384, 8], P('sp', 'tp'), may hold values from -1.5 to 0
- out_weight: bfloat16 [2048, 2048], replicated, may hold values from -0.25 to 0.25
- residual: bfloat16 [16384, 2048], P(('sp', 'tp')), may hold values from -6 to 6
- gain_mix: float32 [2048], replicated, may hold values from 0.1 to 1.9
- routes: int32 [16384, 4], P(('sp', 'tp')), may hold values from 0 to 127, all different within a row; in each aligned block of 128 rows (0 to 127, 128 to 255, ...) at most 8 rows name the same one
- route_weight: float32 [16384, 4], P(('sp', 'tp')), may hold values from 0.2 to 1
- shared_gate: bfloat16 [2048, 512], replicated, may hold values from -0.125 to 0.125
- shared_up: bfloat16 [2048, 512], replicated, may hold values from -0.125 to 0.125
- shared_down: bfloat16 [512, 2048], replicated, may hold values from -0.375 to 0.375
- expert_gate: bfloat16 [128, 2048, 512], P(('sp', 'tp')), may hold values from -0.125 to 0.125
- expert_up: bfloat16 [128, 2048, 512], P(('sp', 'tp')), may hold values from -0.125 to 0.125
- expert_down: bfloat16 [128, 512, 2048], P(('sp', 'tp')), may hold values from -0.375 to 0.375
- gain_out: float32 [2048], replicated, may hold values from 0.1 to 1.9
Outputs:
- layer_out: bfloat16 [16384, 2048], P(('sp', 'tp'))
Inputs may be any that keep to these rules, and one draw needn't show every extreme that they name: `routes`: each row names 4 different experts. In the rows of one device (aligned blocks of 128 rows) no expert is named more than 8 times, and in some blocks one expert is named exactly 8 times.
All inputs are finite; a program needn't handle non-finite values.
Results may differ from a plain program's by a relative error of at most 0.014.
Values may be sent and summed in bfloat16 or wider, within the bound.
No kernel may reach another device: no remote copies, remote signals or barrier semaphores. Data moves between devices by JAX's collectives and lax.ppermute only.
A program may use at most 128 MiB of HBM per device.

v0:
```python
import jax
import jax.numpy as jnp
from jax import lax
from jax.sharding import PartitionSpec as P

ALPHA = 8.0**0.25
RATE_C = 8.0
NORM_EPS = 1e-05


def from_behind(block, axis, distance):
    devices = range(lax.axis_size(axis))
    route = [(i - distance, i) for i in devices if i - distance in devices]
    return lax.ppermute(block, axis, route)


def sent_to_all(x, axis):
    count = lax.axis_size(axis)
    return lax.all_to_all(jnp.broadcast_to(x[None], (count, *x.shape)), axis, 0, 0, tiled=True)


def gathered_once(x, axis):
    leaves = jax.tree.leaves(x)
    order = sorted(range(len(leaves)), key=lambda k: -leaves[k].size)
    width = (1, *leaves[order[0]].shape)[-1]
    lines = [
        jnp.pad(leaves[k].reshape(-1), (0, -leaves[k].size % width)).reshape(-1, width)
        for k in order
    ]
    both, at, found = (sent_to_all(jnp.concatenate(lines), axis), 0, {})
    for k, line in zip(order, lines):
        slab = both[:, at : at + len(line)].reshape(len(both), -1)
        found[k] = slab[:, : leaves[k].size].reshape(-1, *leaves[k].shape)
        at += len(line)
    numbers = iter(range(len(leaves)))
    return jax.tree.map(lambda _: found[next(numbers)], x)


def folded_in_pairs(pieces, combine):
    while len(jax.tree.leaves(pieces)[0]) > 1:
        pieces = jax.vmap(combine)(
            *(jax.tree.map(lambda part: part[side::2], pieces) for side in (0, 1))
        )
    return jax.tree.map(lambda part: part[0], pieces)


def entering(x, axis, combine, identity):
    count, here = (lax.axis_size(axis), lax.axis_index(axis))
    passed = jnp.arange(count) < here

    def kept(part, zero, own):
        part = jnp.where(
            passed.reshape(-1, *(1 for _ in own.shape)), part, jnp.asarray(zero, own.dtype)
        )
        return part

    pieces = gathered_once(x, axis)
    return folded_in_pairs(jax.tree.map(kept, pieces, identity, x), combine)


def layer_norm(values, gains):
    center = values - jnp.mean(values, axis=-1, keepdims=True)
    spread = jnp.mean(center * center, axis=-1, keepdims=True)
    return center * lax.rsqrt(spread + NORM_EPS) * gains


def combine(former, latter):
    return (former[0] * latter[0], latter[0] * former[1] + latter[1])


def on_device(
    gate_pre,
    conv_in,
    conv_taps,
    recur_map,
    input_map,
    rate_logit,
    decay_shift,
    out_weight,
    residual,
    gain_mix,
    routes,
    route_weight,
    shared_gate,
    shared_up,
    shared_down,
    expert_gate,
    expert_up,
    expert_down,
    gain_out,
):
    tokens, channels = conv_in.shape
    reach = conv_taps.shape[0] - 1
    head_count, head_width = (recur_map.shape[0], recur_map.shape[1])
    before = from_behind(conv_in[tokens - reach :], "sp", 1)
    extended = jnp.concatenate([before, conv_in], axis=0).astype(jnp.float32)
    filter_tap_weight = conv_taps.astype(jnp.float32)
    summed = jnp.zeros((tokens, channels), jnp.float32)
    for offset in range(reach + 1):
        summed = summed + filter_tap_weight[offset] * extended[offset : offset + tokens]
    conv_out = summed.astype(jnp.bfloat16).reshape(tokens, head_count, head_width)
    recur_gate = jax.nn.sigmoid(
        jnp.einsum("thc,hcd->thd", conv_out, recur_map, preferred_element_type=jnp.float32)
    )
    input_gate = jax.nn.sigmoid(
        jnp.einsum("thc,hcd->thd", conv_out, input_map, preferred_element_type=jnp.float32)
    )
    log_decay = (
        -RATE_C * jax.nn.softplus(-rate_logit).reshape(head_count, head_width) * recur_gate
        + decay_shift[:, :, None]
    )
    update = jnp.sqrt(-jnp.expm1(2.0 * log_decay)) * input_gate * conv_out.astype(jnp.float32)
    running, local_state = lax.associative_scan(combine, (jnp.exp(log_decay), update), axis=0)
    carried = entering(
        (running[-1], local_state[-1]),
        "sp",
        combine,
        (jnp.ones_like(running[-1]), jnp.zeros_like(local_state[-1])),
    )
    states = local_state + running * carried[1][None]
    mixed_rows = (
        states.reshape(tokens, channels)
        * jax.nn.gelu(gate_pre.astype(jnp.float32), approximate=True)
    ).astype(jnp.bfloat16)
    row_count = tokens // lax.axis_size("tp")
    regrouped = lax.all_to_all(mixed_rows, "tp", split_axis=0, concat_axis=1, tiled=True)
    projected = jnp.dot(regrouped, out_weight, preferred_element_type=jnp.float32)
    normed = layer_norm(ALPHA * residual.astype(jnp.float32) + projected, gain_mix).astype(
        jnp.bfloat16
    )
    model_width = normed.shape[1]
    fanout = routes.shape[1]
    sp_count, tp_count = (lax.axis_size("sp"), lax.axis_size("tp"))
    experts = sp_count * tp_count
    capacity = max(2, 2 * row_count * fanout // experts)
    entries = row_count * fanout
    flat_ids = routes.reshape(entries)
    onehot = (flat_ids[:, None] == lax.iota(jnp.int32, experts)[None, :]).astype(jnp.bfloat16)
    before_mask = (
        lax.iota(jnp.int32, entries)[:, None] > lax.iota(jnp.int32, entries)[None, :]
    ).astype(jnp.bfloat16)
    earlier = jnp.dot(before_mask, onehot, preferred_element_type=jnp.float32)
    slot_rank = jnp.sum(earlier * onehot.astype(jnp.float32), axis=1).astype(jnp.int32)
    slot_index = flat_ids * capacity + slot_rank
    source_row = (
        jnp.full((experts * capacity,), row_count, jnp.int32)
        .at[slot_index]
        .set(lax.iota(jnp.int32, entries) // fanout)
    )
    padded_rows = jnp.concatenate([normed, jnp.zeros((1, model_width), jnp.bfloat16)], axis=0)
    outgoing = padded_rows[source_row].reshape(experts, capacity, model_width)
    shared_hidden = (
        jax.nn.silu(jnp.dot(normed, shared_gate, preferred_element_type=jnp.float32))
        * jnp.dot(normed, shared_up, preferred_element_type=jnp.float32)
    ).astype(jnp.bfloat16)
    shared_out = jnp.dot(shared_hidden, shared_down, preferred_element_type=jnp.float32)
    received = lax.all_to_all(outgoing, ("sp", "tp"), split_axis=0, concat_axis=0, tiled=True)
    senders = received.shape[0]
    slot_count = received.shape[1]
    chosen = received.reshape(senders * slot_count, model_width)
    hidden = (
        jax.nn.silu(jnp.dot(chosen, expert_gate[0], preferred_element_type=jnp.float32))
        * jnp.dot(chosen, expert_up[0], preferred_element_type=jnp.float32)
    ).astype(jnp.bfloat16)
    handed_result = lax.all_to_all(
        jnp.dot(hidden, expert_down[0], preferred_element_type=jnp.float32)
        .astype(jnp.bfloat16)
        .reshape(senders, slot_count, model_width),
        ("sp", "tp"),
        split_axis=0,
        concat_axis=0,
        tiled=True,
    )
    gathered = handed_result.reshape(experts * capacity, model_width)[slot_index].reshape(
        row_count, fanout, model_width
    )
    moe_sum = shared_out + jnp.sum(route_weight[:, :, None] * gathered.astype(jnp.float32), axis=1)
    return layer_norm(ALPHA * normed.astype(jnp.float32) + moe_sum, gain_out).astype(jnp.bfloat16)


def solution(mesh):
    return jax.shard_map(
        on_device,
        mesh=mesh,
        in_specs=(
            P("sp", "tp"),
            P("sp", "tp"),
            P(None, "tp"),
            P("tp", None, None),
            P("tp", None, None),
            P("tp"),
            P("sp", "tp"),
            P(),
            P(("sp", "tp"), None),
            P(),
            P(("sp", "tp"), None),
            P(("sp", "tp"), None),
            P(),
            P(),
            P(),
            P(("sp", "tp"), None, None),
            P(("sp", "tp"), None, None),
            P(("sp", "tp"), None, None),
            P(),
        ),
        out_specs=P(("sp", "tp"), None),
        check_vma=False,
    )
```

profile of v0, /device:TPU:1, one launch (start us, length us, event | category | flops | bytes accessed | tf_op | source)
XLA Modules:
  0.0 347.6 jit_solution(3061634568221742398)
XLA Ops:
  1.8 3.9 %collective-permute-start = (bf16[3,1024]{0,1:T(8,128)(2,1)}, bf16[3,1024]{0,1:T(8,128)(2,1)S(1)}, u32[]{:S(2)}, u32[]{:S(2)}) collective-permute-start(bf16[3,1024]{0,1:T(8,128)(2,1)} %copy.22), channel_id=1, source_target_pairs={{0,2},{2,4},{4,6},{6,8},{8,10},{10,12},{12,14},{14,16},{16,18},{18... | collective-permute-start | bytes 18440 | tf_op jit(solution)/shard_map/ppermute | solution.py:14
  13.8 1.5 fusion.38
  17.1 1.9 fusion.74
  19.1 2.0 fusion.17
  21.1 3.3 slice.353
  24.4 3.3 slice.354
  27.7 1.5 slice.352
  29.2 1.5 slice.356
  30.7 1.7 multiply_add_fusion.1
  35.4 2.0 multiply_add_fusion.2
  38.8 1.6 slice.364
  40.4 1.6 slice.368
  42.0 1.8 multiply_add_fusion.3
  45.1 1.5 slice.370
  46.6 1.5 slice.374
  48.2 1.6 multiply_add_fusion.4
  49.8 1.4 slice.377
  51.2 1.4 slice.378
  52.7 1.5 slice.376
  54.1 1.5 slice.380
  55.6 1.4 multiply_add_fusion.5
  58.4 1.4 slice.383
  61.1 1.4 slice.386
  62.5 1.4 multiply_add_fusion.6
  69.1 1.4 fusion.71
  71.3 1.4 slice.398
  75.4 1.5 slice.375
  76.8 1.5 slice.400
  81.0 1.5 slice.369
  91.6 3.3 slice.408
  94.9 3.3 slice.351
  104.8 1.8 fusion.43
  106.8 1.8 pad.128
  109.5 4.3 %pad.130 = f32[256,4,256]{2,0,1:T(8,128)} pad(f32[128,4,256]{2,0,1:T(8,128)} %add.316, f32[]{:T(128)} %constant.23.clone.1), padding=1_0_1x0_0_0x0_0_0 | pad | bytes 1572868 | tf_op jit(solution)/shard_map/pad | solution.py:113
  113.8 1.7 pad_maximum_fusion.2
  115.5 3.9 %pad.111 = f32[128,4,256]{2,0,1:T(8,128)} pad(f32[64,4,256]{2,0,1:T(8,128)} %pad_maximum_fusion.2, f32[]{:T(128)} %constant.23.clone.1), padding=0_1_1x0_0_0x0_0_0 | pad | bytes 786436 | tf_op jit(solution)/shard_map/pad | solution.py:113
  119.3 2.2 pad.112
  121.5 2.1 add.307
  123.6 2.5 fusion.42
  126.9 4.3 %pad.129 = f32[256,4,256]{2,0,1:T(8,128)} pad(f32[128,4,256]{2,0,1:T(8,128)} %pad_maximum_fusion.1, f32[]{:T(128)} %constant.23.clone.1), padding=0_1_1x0_0_0x0_0_0 | pad | bytes 1572868 | tf_op jit(solution)/shard_map/pad | solution.py:113
  132.0 4.3 %pad.114 = f32[256,4,256]{2,0,1:T(8,128)} pad(f32[128,4,256]{2,0,1:T(8,128)} %add.307, f32[]{:T(128)} %constant.23.clone.1), padding=1_0_1x0_0_0x0_0_0 | pad | bytes 1572868 | tf_op jit(solution)/shard_map/pad | solution.py:113
  136.3 1.9 pad_maximum_fusion
  138.2 4.3 %pad.113 = f32[256,4,256]{2,0,1:T(8,128)} pad(f32[128,4,256]{2,0,1:T(8,128)} %pad_maximum_fusion, f32[]{:T(128)} %constant.23.clone.1), padding=0_1_1x0_0_0x0_0_0 | pad | bytes 1572868 | tf_op jit(solution)/shard_map/pad | solution.py:113
  144.1 11.1 %all-to-all-start = ((f32[64,8,256]{2,1,0:T(8,128)}), f32[64,8,256]{2,1,0:T(8,128)}, u32[]{:S(2)}, u32[]{:S(2)}) async-start(f32[64,8,256]{2,1,0:T(8,128)} %broadcast_in_dim.25), calls=%async_computation | async-start | bytes 1048576 | tf_op jit(solution)/shard_map/all_to_all | solution.py:19
  155.2 2.8 scatter_custom_fusion
  158.1 8.9 %all-to-all-done = f32[64,8,256]{2,1,0:T(8,128)} async-done(((f32[64,8,256]{2,1,0:T(8,128)}), f32[64,8,256]{2,1,0:T(8,128)}, u32[]{:S(2)}, u32[]{:S(2)}) %all-to-all-start) | async-done | bytes 524320 | tf_op jit(solution)/shard_map/all_to_all | solution.py:19
  167.0 1.5 slice_select_fusion.1
  168.9 2.6 multiply_add_fusion
  171.5 1.6 copy.28
  173.0 1.5 fusion.36
  174.6 6.2 %all_to_all.34 = bf16[2,128,1024]{1,2,0:T(8,128)(2,1)S(1)} all-to-all(bf16[2,128,1024]{1,2,0:T(8,128)(2,1)S(1)} %copy_bitcast_fusion), channel_id=1, replica_groups=mesh['sp'=64,'tp'=2] {'tp'}, dimensions={0} | all-to-all | bytes 1048576 | tf_op jit(solution)/shard_map/all_to_all | solution.py:126
  180.7 4.8 %fusion.75 = (f32[128]{0:T(128)S(1)}, f32[128,2048]{1,0:T(8,128)S(1)}) fusion(bf16[128,2048]{0,1:T(8,128)(2,1)S(1)} %bitcast.85, bf16[2048,2048]{1,0:T(8,128)(2,1)} %param.26, bf16[128,2048]{1,0:T(8,128)(2,1)S(1)} %copy-done.9), kind=kOutput, calls=%fused_computation.171 | convolution fusion | flops 1074790272 | bytes 10486272 | tf_op jit(solution)/shard_map/dot_general | solution.py:127
  186.1 6.0 %gather_fusion = bf16[1024,2048]{1,0:T(8,128)(2,1)} fusion(bf16[129,2048]{1,0:T(8,128)(2,1)S(1)} %concatenate.67, s32[1024]{0:T(1024)S(1)} %fusion.61), kind=kCustom, calls=%fused_computation | custom fusion | bytes 8392704 | tf_op jit(solution)/shard_map/gather | solution.py:151
  192.1 57.3 %all_to_all.35 = bf16[128,8,2048]{2,1,0:T(8,128)(2,1)S(1)} all-to-all(bf16[128,8,2048]{2,1,0:T(8,128)(2,1)} %bitcast.84), channel_id=1, replica_groups=mesh['sp'=64,'tp'=2] {'sp','tp'}, dimensions={0} | all-to-all | bytes 8388608 | tf_op jit(solution)/shard_map/all_to_all | solution.py:157
  249.4 2.0 copy-done.5
  251.4 3.6 %fusion.2 = f32[1024,512]{1,0:T(8,128)} fusion(bf16[128,8,2048]{2,1,0:T(8,128)(2,1)S(1)} %all_to_all.35, bf16[1,2048,512]{2,1,0:T(8,128)(2,1)S(1)} %copy-done.39), kind=kOutput, calls=%fused_computation.5 | convolution fusion | flops 2147483648 | bytes 8388608 | tf_op jit(solution)/shard_map/dot_general | solution.py:162
  255.0 10.0 %convert_bitcast_fusion = bf16[128,8,2048]{2,1,0:T(8,128)(2,1)} fusion(bf16[1,512,2048]{2,1,0:T(8,128)(2,1)S(1)} %copy-done, f32[1024,512]{1,0:T(8,128)} %fusion.2, bf16[1,2048,512]{2,1,0:T(8,128)(2,1)} %param.35, bf16[128,8,2048]{2,1,0:T(8,128)(2,1)} %copy-done.5), kind=kOutput, calls=%fused_computation.8 | convolution fusion | flops 4300210176 | bytes 14680064 | tf_op jit(solution)/shard_map/dot_general | solution.py:166
  265.1 5.7 %all-to-all-start.3 = ((bf16[128,8,2048]{2,1,0:T(8,128)(2,1)}), bf16[128,8,2048]{2,1,0:T(8,128)(2,1)}, u32[]{:S(2)}, u32[]{:S(2)}) async-start(bf16[128,8,2048]{2,1,0:T(8,128)(2,1)} %convert_bitcast_fusion), calls=%async_computation.3 | async-start | bytes 8388608 | tf_op jit(solution)/shard_map/all_to_all | solution.py:165
  270.9 2.0 fusion.77
  272.9 50.5 %all-to-all-done.3 = bf16[128,8,2048]{2,1,0:T(8,128)(2,1)} async-done(((bf16[128,8,2048]{2,1,0:T(8,128)(2,1)}), bf16[128,8,2048]{2,1,0:T(8,128)(2,1)}, u32[]{:S(2)}, u32[]{:S(2)}) %all-to-all-start.3) | async-done | bytes 4194336 | tf_op jit(solution)/shard_map/all_to_all | solution.py:165
  323.5 7.9 %gather_fusion.1 = bf16[512,2048]{1,0:T(8,128)(2,1)} fusion(bf16[1024,2048]{1,0:T(8,128)(2,1)} %bitcast.20, s32[1024]{0:T(1024)S(1)} %pad_clamp_fusion), kind=kCustom, calls=%fused_computation.1 | custom fusion | bytes 4196352 | tf_op jit(solution)/shard_map/gather | solution.py:174
  331.4 4.7 %reshape.117 = f32[128,4,2048]{2,1,0:T(4,128)} reshape(bf16[512,2048]{1,0:T(8,128)(2,1)} %gather_fusion.1) | data formatting | bytes 6291456 | tf_op jit(solution)/shard_map/convert_element_type | solution.py:177
  336.2 6.3 %multiply_reduce_fusion = f32[128,2048]{1,0:T(8,128)} fusion(f32[128,4,2048]{2,1,0:T(4,128)} %reshape.117, f32[128,4]{1,0:T(8,128)S(1)} %copy.31), kind=kLoop, calls=%fused_computation.7 | loop fusion | flops 1835008 | bytes 5244928 | tf_op jit(solution)/shard_map/reduce_sum | solution.py:177
  342.5 3.8 %fusion.76 = (f32[128]{0:T(128)S(1)}, f32[128,2048]{1,0:T(8,128)S(1)}) fusion(f32[128,2048]{1,0:T(8,128)} %multiply_reduce_fusion, bf16[512,2048]{1,0:T(8,128)(2,1)} %param.33, bf16[128,2048]{1,0:T(8,128)(2,1)} %copy-done.1, bf16[2048,512]{1,0:T(8,128)(2,1)} %param.32, f32[128,512]{1,0:T(8,128)S(1)} %fusion.77), kind=kOutput, calls=%fused_computation.172 | convolution fusion | flops 538574720 | bytes 7078400 | tf_op jit(solution)/shard_map/dot_general | solution.py:156
  (210 shorter events, 53.3 us)
Async XLA Ops:
  0.0 255.0 %copy-start = (bf16[1,512,2048]{2,1,0:T(8,128)(2,1)S(1)}, bf16[1,512,2048]{2,1,0:T(8,128)(2,1)}, u32[]{:S(2)}) copy-start(bf16[1,512,2048]{2,1,0:T(8,128)(2,1)} %param.36) | copy-start | bytes 6291460
  0.0 11.0 %copy-start.10 = (bf16[256,1024]{1,0:T(8,128)(2,1)S(1)}, bf16[256,1024]{1,0:T(8,128)(2,1)}, u32[]{:S(2)}) copy-start(bf16[256,1024]{1,0:T(8,128)(2,1)} %param.19) | copy-start | bytes 1572868
  1.8 11.6 %collective-permute-start = (bf16[3,1024]{0,1:T(8,128)(2,1)}, bf16[3,1024]{0,1:T(8,128)(2,1)S(1)}, u32[]{:S(2)}, u32[]{:S(2)}) collective-permute-start(bf16[3,1024]{0,1:T(8,128)(2,1)} %copy.22), channel_id=1, source_target_pairs={{0,2},{2,4},{4,6},{6,8},{8,10},{10,12},{12,14},{14,16},{16,18},{18... | collective-permute-start | bytes 18440 | tf_op jit(solution)/shard_map/ppermute | solution.py:14
  13.8 3.4 copy-start.41
  15.3 0.8 copy-start.7
  17.1 2.0 copy-start.8
  17.1 2.0 copy-start.11
  17.1 2.0 copy-start.40
  19.1 10.1 %copy-start.6 = (f32[256,4,256]{2,0,1:T(8,128)}, f32[256,4,256]{2,0,1:T(8,128)S(1)}, u32[]{:S(2)}) copy-start(f32[256,4,256]{2,0,1:T(8,128)S(1)} %get-tuple-element.56) | copy-start | bytes 3145732
  88.8 12.1 %copy-start.19 = (f32[2,4,256]{2,0,1:T(2,128)S(1)}, f32[2,4,256]{2,0,1:T(2,128)}, u32[]{:S(2)}) copy-start(f32[2,4,256]{2,0,1:T(2,128)} %get-tuple-element.63) | copy-start | bytes 24580
  88.8 12.2 %copy-start.18 = (f32[2,4,256]{2,0,1:T(2,128)S(1)}, f32[2,4,256]{2,0,1:T(2,128)}, u32[]{:S(2)}) copy-start(f32[2,4,256]{2,0,1:T(2,128)} %get-tuple-element.62) | copy-start | bytes 24580
  88.8 12.2 %copy-start.30 = (f32[1,4,256]{2,0,1:T(1,128)S(1)}, f32[1,4,256]{2,0,1:T(1,128)}, u32[]{:S(2)}) copy-start(f32[1,4,256]{2,0,1:T(1,128)} %get-tuple-element.40) | copy-start | bytes 12292
  88.8 12.2 %copy-start.31 = (f32[1,4,256]{2,0,1:T(1,128)S(1)}, f32[1,4,256]{2,0,1:T(1,128)}, u32[]{:S(2)}) copy-start(f32[1,4,256]{2,0,1:T(1,128)} %get-tuple-element.41) | copy-start | bytes 12292
  88.8 12.2 %copy-start.32 = (f32[1,4,256]{2,0,1:T(1,128)S(1)}, f32[1,4,256]{2,0,1:T(1,128)}, u32[]{:S(2)}) copy-start(f32[1,4,256]{2,0,1:T(1,128)} %get-tuple-element.42) | copy-start | bytes 12292
  88.8 12.2 %copy-start.33 = (f32[1,4,256]{2,0,1:T(1,128)S(1)}, f32[1,4,256]{2,0,1:T(1,128)}, u32[]{:S(2)}) copy-start(f32[1,4,256]{2,0,1:T(1,128)} %get-tuple-element.43) | copy-start | bytes 12292
  88.8 12.7 %copy-start.15 = (f32[7,4,256]{2,0,1:T(8,128)S(1)}, f32[7,4,256]{2,0,1:T(8,128)}, u32[]{:S(2)}) copy-start(f32[7,4,256]{2,0,1:T(8,128)} %slice.375) | copy-start | bytes 86020
  88.8 12.7 %copy-start.16 = (f32[7,4,256]{2,0,1:T(8,128)S(1)}, f32[7,4,256]{2,0,1:T(8,128)}, u32[]{:S(2)}) copy-start(f32[7,4,256]{2,0,1:T(8,128)} %slice.400) | copy-start | bytes 86020
  90.4 12.8 %copy-start.13 = (f32[15,4,256]{2,0,1:T(8,128)S(1)}, f32[15,4,256]{2,0,1:T(8,128)}, u32[]{:S(2)}) copy-start(f32[15,4,256]{2,0,1:T(8,128)} %slice.369) | copy-start | bytes 184324
  90.4 12.8 %copy-start.14 = (f32[15,4,256]{2,0,1:T(8,128)S(1)}, f32[15,4,256]{2,0,1:T(8,128)}, u32[]{:S(2)}) copy-start(f32[15,4,256]{2,0,1:T(8,128)} %slice.402) | copy-start | bytes 184324
  91.0 10.2 %copy-start.17 = (f32[3,4,256]{2,0,1:T(4,128)S(1)}, f32[3,4,256]{2,0,1:T(4,128)}, u32[]{:S(2)}) copy-start(f32[3,4,256]{2,0,1:T(4,128)} %slice.398) | copy-start | bytes 36868
  91.0 10.3 %copy-start.29 = (f32[1,4,256]{2,0,1:T(1,128)S(1)}, f32[1,4,256]{2,0,1:T(1,128)}, u32[]{:S(2)}) copy-start(f32[1,4,256]{2,0,1:T(1,128)} %slice.494) | copy-start | bytes 12292
  91.0 10.4 %copy-start.28 = (f32[1,4,256]{2,0,1:T(1,128)S(1)}, f32[1,4,256]{2,0,1:T(1,128)}, u32[]{:S(2)}) copy-start(f32[1,4,256]{2,0,1:T(1,128)} %slice.468) | copy-start | bytes 12292
  91.6 11.6 %copy-start.27 = (f32[1,4,256]{2,0,1:T(1,128)S(1)}, f32[1,4,256]{2,0,1:T(1,128)}, u32[]{:S(2)}) copy-start(f32[1,4,256]{2,0,1:T(1,128)} %slice.492) | copy-start | bytes 12292
  94.9 8.5 %copy-start.26 = (f32[1,4,256]{2,0,1:T(1,128)S(1)}, f32[1,4,256]{2,0,1:T(1,128)}, u32[]{:S(2)}) copy-start(f32[1,4,256]{2,0,1:T(1,128)} %slice.466) | copy-start | bytes 12292
  101.2 2.3 copy-start.12
  102.3 1.3 copy-start.25
  103.2 0.7 copy-start.24
  103.9 2.7 copy-start.23
  106.8 7.0 %copy-start.22 = (f32[1,4,256]{2,0,1:T(1,128)S(1)}, f32[1,4,256]{2,0,1:T(1,128)}, u32[]{:S(2)}) copy-start(f32[1,4,256]{2,0,1:T(1,128)} %slice.464) | copy-start | bytes 12292
  123.6 2.5 copy-start.21
  126.1 5.1 %copy-start.2 = (f32[256,4,256]{2,0,1:T(8,128)S(1)}, f32[256,4,256]{2,0,1:T(8,128)}, u32[]{:S(2)}) copy-start(f32[256,4,256]{2,0,1:T(8,128)} %pad.130) | copy-start | bytes 3145732
  126.1 10.2 %copy-start.20 = (f32[1,4,256]{2,0,1:T(1,128)S(1)}, f32[1,4,256]{2,0,1:T(1,128)}, u32[]{:S(2)}) copy-start(f32[1,4,256]{2,0,1:T(1,128)} %slice.463) | copy-start | bytes 12292
  136.3 18.9 %copy-start.36 = (s32[512,1]{0,1:T(1,128)S(1)}, s32[512,1]{0,1:T(1,128)}, u32[]{:S(2)}) copy-start(s32[512,1]{0,1:T(1,128)} %mul.400) | copy-start | bytes 6148
  136.3 18.9 %copy-start.37 = (s32[512]{0:T(512)S(1)}, s32[512]{0:T(512)}, u32[]{:S(2)}) copy-start(s32[512]{0:T(512)} %convert_element_type.77) | copy-start | bytes 6148
  144.1 22.9 %all-to-all-start = ((f32[64,8,256]{2,1,0:T(8,128)}), f32[64,8,256]{2,1,0:T(8,128)}, u32[]{:S(2)}, u32[]{:S(2)}) async-start(f32[64,8,256]{2,1,0:T(8,128)} %broadcast_in_dim.25), calls=%async_computation | async-start | bytes 1048576 | tf_op jit(solution)/shard_map/all_to_all | solution.py:19
  167.0 1.7 copy-start.3
  167.0 1.9 copy-start.4
  173.0 7.7 %copy-start.9 = (bf16[128,2048]{1,0:T(8,128)(2,1)S(1)}, bf16[128,2048]{1,0:T(8,128)(2,1)}, u32[]{:S(2)}) copy-start(bf16[128,2048]{1,0:T(8,128)(2,1)} %param.27) | copy-start | bytes 1572868
  180.7 5.0 %copy-start.34 = (f32[2048]{0:T(1024)S(1)}, f32[2048]{0:T(1024)}, u32[]{:S(2)}) copy-start(f32[2048]{0:T(1024)} %param.28) | copy-start | bytes 24580
  186.0 84.9 %copy-start.1 = (bf16[128,2048]{1,0:T(8,128)(2,1)}, bf16[128,2048]{1,0:T(8,128)(2,1)S(1)}, u32[]{:S(2)}) copy-start(bf16[128,2048]{1,0:T(8,128)(2,1)S(1)} %multiply_convert_fusion.2) | copy-start | bytes 1572868
  192.1 59.3 %copy-start.39 = (bf16[1,2048,512]{2,1,0:T(8,128)(2,1)S(1)}, bf16[1,2048,512]{2,1,0:T(8,128)(2,1)}, u32[]{:S(2)}) copy-start(bf16[1,2048,512]{2,1,0:T(8,128)(2,1)} %param.34) | copy-start | bytes 6291460
  249.4 2.0 copy-start.5
  265.1 5.7 %copy-start.38 = (f32[128,4]{0,1:T(4,128)S(1)}, f32[128,4]{0,1:T(4,128)}, u32[]{:S(2)}) copy-start(f32[128,4]{0,1:T(4,128)} %param.30) | copy-start | bytes 6148
  265.1 58.4 %all-to-all-start.3 = ((bf16[128,8,2048]{2,1,0:T(8,128)(2,1)}), bf16[128,8,2048]{2,1,0:T(8,128)(2,1)}, u32[]{:S(2)}, u32[]{:S(2)}) async-start(bf16[128,8,2048]{2,1,0:T(8,128)(2,1)} %convert_bitcast_fusion), calls=%async_computation.3 | async-start | bytes 8388608 | tf_op jit(solution)/shard_map/all_to_all | solution.py:165
  342.5 4.1 %copy-start.35 = (f32[2048]{0:T(1024)S(1)}, f32[2048]{0:T(1024)}, u32[]{:S(2)}) copy-start(f32[2048]{0:T(1024)} %param.37) | copy-start | bytes 24580
where the time goes:
time: 351 us; the launch traced here: 348 us
  local copies, waits for them, and re-layouts  128 us (36%)
  blocking collectives  63.4 us (18%)
  waiting for transfers between devices  59.5 us (17%)
  other arithmetic  46.7 us (13%)
  matrix products  28.5 us (8%)
  starting transfers between devices  20.7 us (6%)
    slice x52, local copies, waits for them, and re-layouts, on_device(): lax.associative_scan(combine, (jnp.exp(log_decay), update), axis=0)  67 us
    all_to_all x1, blocking collectives, on_device(): lax.all_to_all(outgoing, ('sp', 'tp'), split_axis=0, concat_axis=0, tiled...  57.3 us
    all_to_all x1, waiting for transfers between devices, on_device(): lax.all_to_all(jnp.dot(hidden, expert_down[0], preferred_element_type=jnp...  50.5 us
    pad x28, local copies, waits for them, and re-layouts, on_device(): lax.associative_scan(combine, (jnp.exp(log_decay), update), axis=0)  26.1 us
    add x13, other arithmetic, combine(): return (former[0] * latter[0], latter[0] * former[1] + latter[1])  15.1 us
    all_to_all x1, starting transfers between devices, sent_to_all(): lax.all_to_all(jnp.broadcast_to(x[None], (count, *x.shape)), axis, 0, 0,...  11.1 us
    dot_general x1, matrix products, on_device(): jnp.dot(hidden, expert_down[0], preferred_element_type=jnp.float32)  10 us
    all_to_all x1, waiting for transfers between devices, sent_to_all(): lax.all_to_all(jnp.broadcast_to(x[None], (count, *x.shape)), axis, 0, 0,...  8.93 us
  transfers between devices with their start and end apart: 3, of which 2 were waited for; matrix products, arithmetic and copies ran while one was open for 4% of the time, Pallas kernels for 0%

commit v1 on v0

v1 whole, which is shorter than its diff:
```python
import functools

import jax
import jax.numpy as jnp
from jax import lax
from jax.experimental import pallas as pl
from jax.experimental.pallas import tpu as pltpu
from jax.sharding import PartitionSpec as P

ALPHA = 8.0**0.25
RATE_C = 8.0
NORM_EPS = 1e-05
CAP = 8
PARTS = 2
LANES = 8
F32 = jnp.float32
BF16 = jnp.bfloat16
VMEM = pl.BlockSpec(memory_space=pltpu.VMEM)
SMEM = pl.BlockSpec(memory_space=pltpu.SMEM)


def call(kernel, out_shape, in_specs, flops, scratch=(), name=None):
    return pl.pallas_call(
        kernel,
        out_shape=out_shape,
        in_specs=in_specs,
        out_specs=jax.tree.map(lambda _: VMEM, out_shape),
        scratch_shapes=list(scratch),
        compiler_params=pltpu.CompilerParams(vmem_limit_bytes=48 * 2**20),
        cost_estimate=pl.CostEstimate(flops=flops, bytes_accessed=2**20, transcendentals=0),
        name=name,
    )


def shape(dims, dtype):
    return jax.ShapeDtypeStruct(dims, dtype)


def log1p_unit(u):
    s = u / (2.0 + u)
    q = s * s
    total = jnp.full_like(s, 1.0 / 17.0)
    for k in (15, 13, 11, 9, 7, 5, 3, 1):
        total = total * q + 1.0 / k
    return 2.0 * s * total


def minus_expm1(y):
    total = jnp.full_like(y, 1.0 / 362880.0)
    for k in (40320, 5040, 720, 120, 24, 6, 2, 1):
        total = total * y + 1.0 / k
    return jnp.where(y > -0.5, -y * total, 1.0 - jnp.exp(y))


def strided(ref, start, stride):
    parts = [ref[c, pl.ds(start, LANES, stride=stride), :] for c in range(ref.shape[0])]
    return jnp.concatenate(parts, axis=1)


def layer_norm(values, gains):
    center = values - jnp.mean(values, axis=-1, keepdims=True)
    spread = jnp.mean(center * center, axis=-1, keepdims=True)
    return center * lax.rsqrt(spread + NORM_EPS) * gains


def scan_kernel(
    halo_ref, x_ref, taps_ref, rmap_ref, imap_ref, rate_ref, shift_ref,
    h_ref, a_ref, hex_ref, aex_ref, tot_ref, ext, cv, rg, ig, sh,
):
    tokens, channels = x_ref.shape
    steps = tokens // LANES
    heads, width = rmap_ref.shape[:2]
    reach = halo_ref.shape[0]
    pad = 8 - reach
    for c in range(ext.shape[0]):
        cols = slice(c * 128, (c + 1) * 128)
        ext[c, pl.ds(pad, reach), :] = halo_ref[:, cols].astype(F32)
        ext[c, pl.ds(8, tokens), :] = x_ref[:, cols].astype(F32)
    taps = [taps_ref[pl.ds(j, 1), :].astype(F32) for j in range(reach + 1)]
    full = jnp.concatenate([shift_ref[...], jnp.zeros((128 - heads, tokens), F32)], axis=0)
    sh[...] = jnp.transpose(full)

    def conv(t, _):
        total = jnp.zeros((LANES, channels), F32)
        for j in range(reach + 1):
            total = total + taps[j] * strided(ext, t + pad + j, steps)
        cv[pl.ds(pl.multiple_of(t * LANES, LANES), LANES), :] = total.astype(BF16).astype(F32)
        return 0

    lax.fori_loop(0, steps, conv, 0, unroll=4)
    for k in range(heads):
        cols = slice(k * width, (k + 1) * width)
        block = cv[:, cols].astype(BF16)
        rg[:, cols] = jnp.dot(block, rmap_ref[k], preferred_element_type=F32)
        ig[:, cols] = jnp.dot(block, imap_ref[k], preferred_element_type=F32)
    logit = -rate_ref[...]
    slope = -RATE_C * (jnp.maximum(logit, 0.0) + log1p_unit(jnp.exp(-jnp.abs(logit))))

    def step(t, carry):
        rows = pl.ds(pl.multiple_of(t * LANES, LANES), LANES)
        moved = sh[pl.ds(t, LANES, stride=steps), :]
        out = []
        for k in range(heads):
            h, a = carry[k]
            cols = slice(k * width, (k + 1) * width)
            log_decay = slope[:, cols] * jax.nn.sigmoid(rg[rows, cols]) + moved[:, k : k + 1]
            update = (
                jnp.sqrt(minus_expm1(2.0 * log_decay))
                * jax.nn.sigmoid(ig[rows, cols])
                * cv[rows, cols]
            )
            decay = jnp.exp(log_decay)
            h = decay * h + update
            a = decay * a
            h_ref[rows, cols] = h
            a_ref[rows, cols] = a
            out.append((h, a))
        return tuple(out)

    start = tuple(
        (jnp.zeros((LANES, width), F32), jnp.ones((LANES, width), F32)) for _ in range(heads)
    )
    last = lax.fori_loop(0, steps, step, start, unroll=2)
    row = lax.broadcasted_iota(jnp.int32, (LANES, width), 0)
    for k in range(heads):
        cols = slice(k * width, (k + 1) * width)
        h, a = last[k]
        for d in (1, 2, 4):
            hp, ap = pltpu.roll(h, d, 0), pltpu.roll(a, d, 0)
            h = jnp.where(row >= d, a * hp + h, h)
            a = jnp.where(row >= d, a * ap, a)
        hex_ref[:, cols] = jnp.where(row >= 1, pltpu.roll(h, 1, 0), 0.0)
        aex_ref[:, cols] = jnp.where(row >= 1, pltpu.roll(a, 1, 0), 1.0)
        both = jnp.concatenate([a[LANES - 1 :], h[LANES - 1 :]], axis=0)
        tot_ref[:, :, cols] = jnp.broadcast_to(both[None], (tot_ref.shape[0], 2, width))


def mix_kernel(index_ref, seen_ref, h_ref, a_ref, hex_ref, aex_ref, gate_ref, mine_ref, theirs_ref, st):
    tokens, channels = h_ref.shape
    steps = tokens // LANES
    here, side = index_ref[0], index_ref[1]

    def fold(i, c):
        pair = seen_ref[i]
        return pair[0:1] * c + pair[1:2]

    carried = lax.fori_loop(0, here, fold, jnp.zeros((1, channels), F32))
    entry = hex_ref[...] + aex_ref[...] * carried

    def step(t, _):
        rows = pl.ds(pl.multiple_of(t * LANES, LANES), LANES)
        state = h_ref[rows, :] + a_ref[rows, :] * entry
        for c in range(st.shape[0]):
            st[c, pl.ds(t, LANES, stride=steps), :] = state[:, c * 128 : (c + 1) * 128]
        return 0

    lax.fori_loop(0, steps, step, 0, unroll=4)
    half = tokens // 2
    block = 16

    def mixed(rows):
        state = jnp.concatenate([st[c, rows, :] for c in range(st.shape[0])], axis=1)
        return (state * jax.nn.gelu(gate_ref[rows, :].astype(F32), approximate=True)).astype(BF16)

    def put(i, _):
        at = pl.multiple_of(i * block, block)
        rows = pl.ds(at, block)
        theirs_ref[rows, :] = mixed(pl.ds(pl.multiple_of((1 - side) * half + at, block), block))
        mine_ref[rows, :] = mixed(pl.ds(pl.multiple_of(side * half + at, block), block))
        return 0

    lax.fori_loop(0, half // block, put, 0)


def route_kernel(routes_ref, weight_ref, g_ref, c_ref):
    fanout, rows = routes_ref.shape
    experts = g_ref.shape[1] * PARTS // CAP
    per = CAP // PARTS
    slots = experts * per
    expert = lax.broadcasted_iota(jnp.int32, (experts, rows), 0)
    member = jnp.zeros((experts, rows), F32)
    weight = jnp.zeros((experts, rows), F32)
    for k in range(fanout):
        hit = expert == routes_ref[pl.ds(k, 1), :]
        member = member + jnp.where(hit, 1.0, 0.0)
        weight = weight + jnp.where(hit, weight_ref[pl.ds(k, 1), :], 0.0)
    earlier = (
        lax.broadcasted_iota(jnp.int32, (rows, rows), 0)
        < lax.broadcasted_iota(jnp.int32, (rows, rows), 1)
    )
    rank = jnp.dot(
        member.astype(BF16), jnp.where(earlier, 1.0, 0.0).astype(BF16), preferred_element_type=F32
    )
    rank = jnp.where(member > 0.0, rank, -1.0)
    slot = lax.broadcasted_iota(jnp.int32, (slots, experts), 0)
    spread = jnp.where(slot // per == lax.broadcasted_iota(jnp.int32, (slots, experts), 1), 1.0, 0.0)
    spread = spread.astype(BF16)
    high = weight.astype(BF16)
    low = (weight - high.astype(F32)).astype(BF16)

    def to_slots(values):
        return jnp.dot(spread, values, preferred_element_type=F32)

    rank, high, low = to_slots(rank.astype(BF16)), to_slots(high), to_slots(low)
    place = (lax.broadcasted_iota(jnp.int32, (slots, rows), 0) % per).astype(F32)
    for part in range(PARTS):
        chosen = rank == place + float(part * per)
        g_ref[part] = jnp.where(chosen, 1.0, 0.0).astype(BF16)
        c_ref[part, :rows] = jnp.transpose(jnp.where(chosen, high, 0.0)).astype(BF16)
        c_ref[part, rows:] = jnp.transpose(jnp.where(chosen, low, 0.0)).astype(BF16)


def project_kernel(index_ref, mine_ref, w_ref, res_ref, out_ref):
    depth = mine_ref.shape[1]
    rows = pl.ds(pl.multiple_of(index_ref[1] * depth, depth), depth)
    out_ref[...] = ALPHA * res_ref[...].astype(F32) + jnp.dot(
        mine_ref[...], w_ref[rows, :], preferred_element_type=F32
    )


def dispatch_kernel(index_ref, other_ref, w_ref, acc_ref, gain_ref, g_ref, normed_ref, *out_refs):
    depth = other_ref.shape[1]
    rows = pl.ds(pl.multiple_of((1 - index_ref[1]) * depth, depth), depth)
    values = acc_ref[...] + jnp.dot(other_ref[...], w_ref[rows, :], preferred_element_type=F32)
    normed = layer_norm(values, gain_ref[...]).astype(BF16)
    normed_ref[...] = normed
    for part in range(PARTS):
        out_refs[part][...] = jnp.dot(
            g_ref[part], normed, preferred_element_type=F32
        ).astype(BF16)


def hidden_of(x, gate, up):
    return (
        jax.nn.silu(jnp.dot(x, gate, preferred_element_type=F32))
        * jnp.dot(x, up, preferred_element_type=F32)
    ).astype(BF16)


def shared_kernel(x_ref, gate_ref, up_ref, down_ref, out_ref):
    x = x_ref[...]
    hidden = hidden_of(x, gate_ref[...], up_ref[...])
    out_ref[...] = ALPHA * x.astype(F32) + jnp.dot(
        hidden, down_ref[...], preferred_element_type=F32
    )


def expert_kernel(x_ref, gate_ref, up_ref, down_ref, out_ref):
    block = 256

    def step(i, _):
        rows = pl.ds(pl.multiple_of(i * block, block), block)
        hidden = hidden_of(x_ref[rows, :], gate_ref[0], up_ref[0])
        out_ref[rows, :] = jnp.dot(hidden, down_ref[0], preferred_element_type=F32).astype(BF16)
        return 0

    lax.fori_loop(0, x_ref.shape[0] // block, step, 0)


def weighted(c_ref, back_ref, part):
    both = jnp.dot(c_ref[part], back_ref[...], preferred_element_type=F32)
    rows = both.shape[0] // 2
    return both[:rows] + both[rows:]


def gather_kernel(base_ref, c_ref, back_ref, out_ref, *, part):
    out_ref[...] = base_ref[...] + weighted(c_ref, back_ref, part)


def finish_kernel(base_ref, c_ref, back_ref, gain_ref, out_ref, *, part):
    values = base_ref[...] + weighted(c_ref, back_ref, part)
    out_ref[...] = layer_norm(values, gain_ref[...]).astype(BF16)


def on_device(
    gate_pre, conv_in, conv_taps, recur_map, input_map, rate_logit, decay_shift, out_weight,
    residual, gain_mix, routes, route_weight, shared_gate, shared_up, shared_down, expert_gate,
    expert_up, expert_down, gain_out,
):
    tokens, channels = conv_in.shape
    reach = conv_taps.shape[0] - 1
    sp, tp = lax.axis_size("sp"), lax.axis_size("tp")
    experts = sp * tp
    rows = tokens // tp
    model = out_weight.shape[1]
    slots = experts * CAP // PARTS
    index = jnp.stack([lax.axis_index("sp"), lax.axis_index("tp")]).astype(jnp.int32)
    before = lax.ppermute(conv_in[tokens - reach :], "sp", [(i, i + 1) for i in range(sp - 1)])
    grid = shape((tokens, channels), F32)
    edge = shape((LANES, channels), F32)
    big = pltpu.VMEM((tokens, channels), F32)
    h, a, hex_, aex, totals = call(
        scan_kernel,
        (grid, grid, edge, edge, shape((sp, 2, channels), F32)),
        [VMEM] * 7,
        10**9,
        [pltpu.VMEM((channels // 128, tokens + 8, 128), F32), big, big, big, pltpu.VMEM((tokens, 128), F32)],
        name="scan",
    )(before, conv_in, conv_taps, recur_map, input_map, rate_logit[None], decay_shift.T)
    seen = lax.all_to_all(totals, "sp", 0, 0, tiled=True)
    g, c = call(
        route_kernel,
        (shape((PARTS, slots, rows), BF16), shape((PARTS, 2 * rows, slots), BF16)),
        [VMEM] * 2,
        10**8,
        name="route",
    )(routes.T, route_weight.T)
    piece = shape((rows, channels), BF16)
    mine, theirs = call(
        mix_kernel, (piece, piece), [SMEM] + [VMEM] * 6, 10**8, [pltpu.VMEM((channels // 128, tokens, 128), F32)], name="mix"
    )(index, seen, h, a, hex_, aex, gate_pre)
    other = lax.ppermute(theirs, "tp", [(0, 1), (1, 0)])
    wide = shape((rows, model), F32)
    acc = call(project_kernel, wide, [SMEM] + [VMEM] * 3, 10**9, name="project")(
        index, mine, out_weight, residual
    )
    normed, *outgoing = call(
        dispatch_kernel,
        (shape((rows, model), BF16),) + (shape((slots, model), BF16),) * PARTS,
        [SMEM] + [VMEM] * 5,
        2 * 10**9,
        name="dispatch",
    )(index, other, out_weight, acc, gain_mix[None], g)

    def exchanged(x):
        x = x.reshape(experts, CAP // PARTS, model)
        x = lax.all_to_all(x, ("sp", "tp"), split_axis=0, concat_axis=0, tiled=True)
        return x.reshape(slots, model)

    received = [exchanged(x) for x in outgoing]
    base = call(shared_kernel, wide, [VMEM] * 4, 10**9, name="shared")(
        normed, shared_gate, shared_up, shared_down
    )
    results = [
        call(expert_kernel, shape((slots, model), BF16), [VMEM] * 4, 3 * 10**9, name="expert")(
            x, expert_gate, expert_up, expert_down
        )
        for x in received
    ]
    back = [exchanged(x) for x in results]
    for part in range(PARTS - 1):
        base = call(
            functools.partial(gather_kernel, part=part), wide, [VMEM] * 3, 10**9, name="gather"
        )(base, c, back[part])
    return call(
        functools.partial(finish_kernel, part=PARTS - 1),
        shape((rows, model), BF16),
        [VMEM] * 4,
        10**9,
        name="finish",
    )(base, c, back[-1], gain_out[None])


def solution(mesh):
    return jax.shard_map(
        on_device,
        mesh=mesh,
        in_specs=(
            P("sp", "tp"),
            P("sp", "tp"),
            P(None, "tp"),
            P("tp", None, None),
            P("tp", None, None),
            P("tp"),
            P("sp", "tp"),
            P(),
            P(("sp", "tp"), None),
            P(),
            P(("sp", "tp"), None),
            P(("sp", "tp"), None),
            P(),
            P(),
            P(),
            P(("sp", "tp"), None, None),
            P(("sp", "tp"), None, None),
            P(("sp", "tp"), None, None),
            P(),
        ),
        out_specs=P(("sp", "tp"), None),
        check_vma=False,
    )
```

time: 351 us -> 211 us (0.60)
  local copies, waits for them, and re-layouts: 128 us -> 44 us
  blocking collectives: 63.4 us -> 0 us
  other arithmetic: 46.7 us -> 0.08 us
  Pallas kernels: 0 us -> 37.2 us
  waiting for transfers between devices: 59.5 us -> 89 us
  matrix products: 28.5 us -> 0 us
  starting transfers between devices: 20.7 us -> 39 us
    slice x55 -> x1, local copies, waits for them, and re-layouts: 69.7 us -> 0.72 us  [on_device(): conv_in[tokens - reach:]]
    all_to_all x2 -> x0, blocking collectives: 63.4 us -> none  [the longest x1 57.3 us: on_device(): lax.all_to_all(outgoing, ('sp', 'tp'), split_axis=0, concat_axis=0, tiled...]
    pallas_call x0 -> x10, Pallas kernels: none -> 37.2 us  [the longest x2 13.2 us: on_device(): call(expert_kernel, shape((slots, model), BF16), [VMEM] * 4, 3 * 10 ** 9,...]
    all_to_all x2 -> x5, waiting for transfers between devices: 59.5 us -> 88.2 us  [the longest x4 77.1 us: exchanged(): x = lax.all_to_all(x, ('sp', 'tp'), split_axis=0, concat_axis=0, tiled=True)]
    dot_general x8 -> x0, matrix products: 28.5 us -> none  [the longest x1 10 us: on_device(): jnp.dot(hidden, expert_down[0], preferred_element_type=jnp.float32)]
    pad x28 -> x0, local copies, waits for them, and re-layouts: 26.1 us -> none  [on_device(): lax.associative_scan(combine, (jnp.exp(log_decay), update), axis=0)]
    reshape x1 -> x8, local copies, waits for them, and re-layouts: 0.99 us -> 24.8 us  [the longest x4 14.6 us: exchanged(): x = x.reshape(experts, CAP // PARTS, model)]
    add x29 -> x0, other arithmetic: 23.6 us -> none  [the longest x13 15.1 us: combine(): return (former[0] * latter[0], latter[0] * former[1] + latter[1])]
  transfers between devices with their start and end apart: 3 -> 7, of which waited for: 2 -> 6; matrix products, arithmetic and copies ran while one was open for 4% -> 10% of each run, Pallas kernels for 0% -> 10%
where the time goes in v1:
time: 211 us; the launch traced here: 210 us
  waiting for transfers between devices  89 us (42%)
  local copies, waits for them, and re-layouts  44 us (21%)
  starting transfers between devices  39 us (18%)
  Pallas kernels  37.2 us (18%)
    all_to_all x4, waiting for transfers between devices, exchanged(): x = lax.all_to_all(x, ('sp', 'tp'), split_axis=0, concat_axis=0, tiled=True)  77.1 us
    all_to_all x4, starting transfers between devices, exchanged(): x = lax.all_to_all(x, ('sp', 'tp'), split_axis=0, concat_axis=0, tiled=True)  20.2 us
    unnamed x50, local copies, waits for them, and re-layouts  18.5 us
    reshape x4, local copies, waits for them, and re-layouts, exchanged(): x = x.reshape(experts, CAP // PARTS, model)  14.6 us
    pallas_call x2, Pallas kernels, on_device(): call(expert_kernel, shape((slots, model), BF16), [VMEM] * 4, 3 * 10 ** 9,...  13.2 us
    all_to_all x1, starting transfers between devices, on_device(): seen = lax.all_to_all(totals, 'sp', 0, 0, tiled=True)  11.8 us
    all_to_all x1, waiting for transfers between devices, on_device(): seen = lax.all_to_all(totals, 'sp', 0, 0, tiled=True)  11.2 us
    reshape x4, local copies, waits for them, and re-layouts, exchanged(): return x.reshape(slots, model)  10.2 us
  transfers between devices with their start and end apart: 7, of which 6 were waited for; matrix products, arithmetic and copies ran while one was open for 10% of the time, Pallas kernels for 10%

profile of v1, /device:TPU:1, one launch (start us, length us, event | category | flops | bytes accessed | tf_op | source)
XLA Modules:
  0.0 209.6 jit_solution(14268221615356960919)
XLA Ops:
  0.0 0.7 slice.3
  0.7 3.9 %collective-permute-start = (bf16[3,1024]{1,0:T(4,128)(2,1)S(1)}, bf16[3,1024]{1,0:T(4,128)(2,1)S(1)}, u32[]{:S(2)}, u32[]{:S(2)}) collective-permute-start(bf16[3,1024]{1,0:T(4,128)(2,1)S(1)} %slice.3), channel_id=1, source_target_pairs={{0,2},{2,4},{4,6},{6,8},{8,10},{10,12},{12,14},{14,16},{16,18},{18... | collective-permute-start | bytes 18440 | tf_op jit(solution)/shard_map/ppermute | solution.py:288
  4.7 0.8 collective-permute-done.halo_ref
  5.4 1.0 copy-done.16
  6.5 1.0 copy-done.17
  7.5 1.0 copy-done.18
  8.6 0.7 copy-done.19
  9.3 0.7 copy-done.20
  9.9 0.7 copy-done.21
  10.6 4.9 %scan.1 = (f32[256,1024]{1,0:T(8,128)S(1)}, f32[256,1024]{1,0:T(8,128)S(1)}, f32[8,1024]{1,0:T(8,128)S(1)}, f32[8,1024]{1,0:T(8,128)S(1)}, f32[64,2,1024]{2,1,0:T(2,128)S(1)}) custom-call(bf16[3,1024]{1,0:T(4,128)(2,1)S(1)} %collective-permute-done.halo_ref, bf16[256,1024]{1,0:T(8,128)(2,1)S(1)} %copy-done.16, bf16[4,1024]{1,0:T(4,128)(2,1)S(1)} %copy-done.19, ...), custom_call_target="tpu_custom_call" | custom-call | flops 1000000000 | bytes 1048576 | tf_op jit(solution)/shard_map/scan/pallas_call | solution.py:292
  15.5 0.0 copy-start.10
  15.5 0.8 copy-done.10
  16.3 11.8 %all-to-all-start = ((f32[64,2,1024]{2,1,0:T(2,128)}), f32[64,2,1024]{2,1,0:T(2,128)S(1)}, u32[]{:S(2)}, u32[]{:S(2)}) async-start(f32[64,2,1024]{2,1,0:T(2,128)} %copy-done.10), calls=%async_computation | async-start | bytes 1048576 | tf_op jit(solution)/shard_map/all_to_all | solution.py:300
  28.1 0.1 pad_add_fusion.index_ref
  28.2 11.2 %all-to-all-done.seen_ref = f32[64,2,1024]{2,1,0:T(2,128)S(1)} async-done(((f32[64,2,1024]{2,1,0:T(2,128)}), f32[64,2,1024]{2,1,0:T(2,128)S(1)}, u32[]{:S(2)}, u32[]{:S(2)}) %all-to-all-start) | async-done | bytes 524320 | tf_op jit(solution)/shard_map/all_to_all | solution.py:300
  39.3 1.0 copy-done.11
  40.4 2.1 %mix.1 = (bf16[128,1024]{1,0:T(8,128)(2,1)S(1)}, bf16[128,1024]{1,0:T(8,128)(2,1)S(1)}) custom-call(s32[2]{0:T(128)S(1)} %pad_add_fusion.index_ref, f32[64,2,1024]{2,1,0:T(2,128)S(1)} %all-to-all-done.seen_ref, f32[256,1024]{1,0:T(8,128)S(1)} %get-tuple-element.18.h_ref, f32[256,1024]{1,0:T(8,128)S(1)} %get-tuple-element.19.a_ref, ...), custom_call_target="tpu_custom_call" | custom-call | flops 100000000 | bytes 1048576 | tf_op jit(solution)/shard_map/mix/pallas_call | solution.py:309
  42.5 3.1 %collective-permute-start.1 = (bf16[128,1024]{1,0:T(8,128)(2,1)S(1)}, bf16[128,1024]{1,0:T(8,128)(2,1)S(1)}, u32[]{:S(2)}, u32[]{:S(2)}) collective-permute-start(bf16[128,1024]{1,0:T(8,128)(2,1)S(1)} %get-tuple-element.22), channel_id=1, source_target_pairs={{0,1},{1,0},{2,3},{3,2},{4,5},{5,4},{6,7},{7,6},{8,9},{9,8},{10,11... | collective-permute-start | bytes 786440 | tf_op jit(solution)/shard_map/ppermute | solution.py:312
  45.7 0.0 copy-done.22
  45.7 0.0 copy-done.23
  45.7 0.6 route.1
  46.3 0.0 copy-start.6
  46.3 0.8 copy-done.6
  47.1 0.0 copy-done.9
  47.1 4.1 %project.1.acc_ref = f32[128,2048]{1,0:T(8,128)S(1)} custom-call(s32[2]{0:T(128)S(1)} %pad_add_fusion.index_ref, bf16[128,1024]{1,0:T(8,128)(2,1)S(1)} %get-tuple-element.23.mine_ref, bf16[2048,2048]{1,0:T(8,128)(2,1)} %w_ref.3, bf16[128,2048]{1,0:T(8,128)(2,1)S(1)} %copy-done.9), custom_call_target="tpu_custom_call" | custom-call | flops 1000000000 | bytes 1048576 | tf_op jit(solution)/shard_map/project/pallas_call | solution.py:314
  51.3 0.0 collective-permute-done.1.other_ref
  51.3 0.0 copy-done.15
  51.3 7.0 %dispatch.1 = (bf16[128,2048]{1,0:T(8,128)(2,1)S(1)}, bf16[512,2048]{1,0:T(8,128)(2,1)S(1)}, bf16[512,2048]{1,0:T(8,128)(2,1)}) custom-call(s32[2]{0:T(128)S(1)} %pad_add_fusion.index_ref, bf16[128,1024]{1,0:T(8,128)(2,1)S(1)} %collective-permute-done.1.other_ref, bf16[2048,2048]{1,0:T(8,128)(2,1)} %w_ref.3, f32[128,2048]{1,0:T(8,128)S(1)} %project.1.acc_ref, ...), custom_call_target="tpu_custom_call" | custom-call | flops 2000000000 | bytes 1048576 | tf_op jit(solution)/shard_map/dispatch/pallas_call | solution.py:317
  58.3 0.8 copy-done.12
  59.1 2.2 %reshape.24 = bf16[128,4,2048]{2,1,0:T(4,128)(2,1)} reshape(bf16[512,2048]{1,0:T(8,128)(2,1)S(1)} %get-tuple-element.27) | data formatting | bytes 4194304 | tf_op jit(solution)/shard_map/reshape | solution.py:326
  61.3 3.7 %all-to-all-start.1 = ((bf16[128,4,2048]{2,1,0:T(4,128)(2,1)}), bf16[128,4,2048]{2,1,0:T(4,128)(2,1)S(1)}, u32[]{:S(2)}, u32[]{:S(2)}) async-start(bf16[128,4,2048]{2,1,0:T(4,128)(2,1)} %reshape.24), calls=%async_computation.1 | async-start | bytes 4194304 | tf_op jit(solution)/shard_map/all_to_all | solution.py:327
  65.0 4.1 %reshape.28 = bf16[128,4,2048]{2,1,0:T(4,128)(2,1)} reshape(bf16[512,2048]{1,0:T(8,128)(2,1)} %get-tuple-element.28) | data formatting | bytes 4194304 | tf_op jit(solution)/shard_map/reshape | solution.py:326
  69.1 26.3 %all-to-all-done.1 = bf16[128,4,2048]{2,1,0:T(4,128)(2,1)S(1)} async-done(((bf16[128,4,2048]{2,1,0:T(4,128)(2,1)}), bf16[128,4,2048]{2,1,0:T(4,128)(2,1)S(1)}, u32[]{:S(2)}, u32[]{:S(2)}) %all-to-all-start.1) | async-done | bytes 2097184 | tf_op jit(solution)/shard_map/all_to_all | solution.py:327
  95.4 1.3 copy-done.24
  96.8 5.5 %all-to-all-start.3 = ((bf16[128,4,2048]{2,1,0:T(4,128)(2,1)}), bf16[128,4,2048]{2,1,0:T(4,128)(2,1)}, u32[]{:S(2)}, u32[]{:S(2)}) async-start(bf16[128,4,2048]{2,1,0:T(4,128)(2,1)} %reshape.28), calls=%async_computation.3 | async-start | bytes 4194304 | tf_op jit(solution)/shard_map/all_to_all | solution.py:327
  102.2 2.5 %reshape.25.x_ref = bf16[512,2048]{1,0:T(8,128)(2,1)S(1)} reshape(bf16[128,4,2048]{2,1,0:T(4,128)(2,1)} %copy-done.24) | data formatting | bytes 4194304 | tf_op jit(solution)/shard_map/reshape | solution.py:328
  104.8 6.6 %expert.2 = bf16[512,2048]{1,0:T(8,128)(2,1)S(1)} custom-call(bf16[512,2048]{1,0:T(8,128)(2,1)S(1)} %reshape.25.x_ref, bf16[1,2048,512]{2,1,0:T(8,128)(2,1)} %gate_ref.7, bf16[1,2048,512]{2,1,0:T(8,128)(2,1)} %up_ref.5, bf16[1,512,2048]{2,1,0:T(8,128)(2,1)} %down_ref.5), custom_call_target="tpu_custom_call" | custom-call | flops 3000000000 | bytes 1048576 | tf_op jit(solution)/shard_map/expert/pallas_call | solution.py:335
  111.4 0.0 copy-start.2
  111.4 1.4 copy-done.2
  112.8 4.1 %reshape.26 = bf16[128,4,2048]{2,1,0:T(4,128)(2,1)} reshape(bf16[512,2048]{1,0:T(8,128)(2,1)} %copy-done.2) | data formatting | bytes 4194304 | tf_op jit(solution)/shard_map/reshape | solution.py:326
  116.9 15.6 %all-to-all-done.3 = bf16[128,4,2048]{2,1,0:T(4,128)(2,1)} async-done(((bf16[128,4,2048]{2,1,0:T(4,128)(2,1)}), bf16[128,4,2048]{2,1,0:T(4,128)(2,1)}, u32[]{:S(2)}, u32[]{:S(2)}) %all-to-all-start.3) | async-done | bytes 2097184 | tf_op jit(solution)/shard_map/all_to_all | solution.py:327
  132.5 5.5 %all-to-all-start.2 = ((bf16[128,4,2048]{2,1,0:T(4,128)(2,1)}), bf16[128,4,2048]{2,1,0:T(4,128)(2,1)}, u32[]{:S(2)}, u32[]{:S(2)}) async-start(bf16[128,4,2048]{2,1,0:T(4,128)(2,1)} %reshape.26), calls=%async_computation.2 | async-start | bytes 4194304 | tf_op jit(solution)/shard_map/all_to_all | solution.py:327
  138.0 2.5 %reshape.29.x_ref = bf16[512,2048]{1,0:T(8,128)(2,1)S(1)} reshape(bf16[128,4,2048]{2,1,0:T(4,128)(2,1)} %all-to-all-done.3) | data formatting | bytes 4194304 | tf_op jit(solution)/shard_map/reshape | solution.py:328
  140.5 6.6 %expert.3 = bf16[512,2048]{1,0:T(8,128)(2,1)S(1)} custom-call(bf16[512,2048]{1,0:T(8,128)(2,1)S(1)} %reshape.29.x_ref, bf16[1,2048,512]{2,1,0:T(8,128)(2,1)} %gate_ref.7, bf16[1,2048,512]{2,1,0:T(8,128)(2,1)} %up_ref.5, bf16[1,512,2048]{2,1,0:T(8,128)(2,1)} %down_ref.5), custom_call_target="tpu_custom_call" | custom-call | flops 3000000000 | bytes 1048576 | tf_op jit(solution)/shard_map/expert/pallas_call | solution.py:335
  147.1 0.0 copy-start.3
  147.1 1.4 copy-done.3
  148.5 4.1 %reshape.30 = bf16[128,4,2048]{2,1,0:T(4,128)(2,1)} reshape(bf16[512,2048]{1,0:T(8,128)(2,1)} %copy-done.3) | data formatting | bytes 4194304 | tf_op jit(solution)/shard_map/reshape | solution.py:326
  152.6 15.6 %all-to-all-done.2 = bf16[128,4,2048]{2,1,0:T(4,128)(2,1)} async-done(((bf16[128,4,2048]{2,1,0:T(4,128)(2,1)}), bf16[128,4,2048]{2,1,0:T(4,128)(2,1)}, u32[]{:S(2)}, u32[]{:S(2)}) %all-to-all-start.2) | async-done | bytes 2097184 | tf_op jit(solution)/shard_map/all_to_all | solution.py:327
  168.2 5.6 %all-to-all-start.4 = ((bf16[128,4,2048]{2,1,0:T(4,128)(2,1)}), bf16[128,4,2048]{2,1,0:T(4,128)(2,1)}, u32[]{:S(2)}, u32[]{:S(2)}) async-start(bf16[128,4,2048]{2,1,0:T(4,128)(2,1)} %reshape.30), calls=%async_computation.4 | async-start | bytes 4194304 | tf_op jit(solution)/shard_map/all_to_all | solution.py:327
  173.8 0.0 copy-done.4
  173.9 0.0 copy-start.5
  173.9 1.6 copy-done.5
  175.5 1.0 copy-done.13
  176.5 2.7 %shared.1.base_ref = f32[128,2048]{1,0:T(8,128)S(1)} custom-call(bf16[128,2048]{1,0:T(8,128)(2,1)S(1)} %copy-done.13, bf16[2048,512]{1,0:T(8,128)(2,1)S(1)} %copy-done.4, bf16[2048,512]{1,0:T(8,128)(2,1)S(1)} %copy-done.5, bf16[512,2048]{1,0:T(8,128)(2,1)} %down_ref.3), custom_call_target="tpu_custom_call" | custom-call | flops 1000000000 | bytes 1048576 | tf_op jit(solution)/shard_map/shared/pallas_call | solution.py:331
  179.2 2.5 %reshape.27.back_ref = bf16[512,2048]{1,0:T(8,128)(2,1)S(1)} reshape(bf16[128,4,2048]{2,1,0:T(4,128)(2,1)} %all-to-all-done.2) | data formatting | bytes 4194304 | tf_op jit(solution)/shard_map/reshape | solution.py:328
  181.8 0.0 copy-start.7
  181.8 1.0 copy-done.7
  182.8 0.7 gather.1.base_ref
  183.5 0.0 copy-start
  183.5 1.0 copy-done
  184.5 19.6 %all-to-all-done.4 = bf16[128,4,2048]{2,1,0:T(4,128)(2,1)} async-done(((bf16[128,4,2048]{2,1,0:T(4,128)(2,1)}), bf16[128,4,2048]{2,1,0:T(4,128)(2,1)}, u32[]{:S(2)}, u32[]{:S(2)}) %all-to-all-start.4) | async-done | bytes 2097184 | tf_op jit(solution)/shard_map/all_to_all | solution.py:327
  204.1 2.6 %reshape.31.back_ref = bf16[512,2048]{1,0:T(8,128)(2,1)S(1)} reshape(bf16[128,4,2048]{2,1,0:T(4,128)(2,1)} %all-to-all-done.4) | data formatting | bytes 4194304 | tf_op jit(solution)/shard_map/reshape | solution.py:328
  206.8 1.0 copy-done.8
  207.8 1.8 finish.1
  (20 shorter events, 0.0 us)
Async XLA Ops:
  0.7 4.7 %collective-permute-start = (bf16[3,1024]{1,0:T(4,128)(2,1)S(1)}, bf16[3,1024]{1,0:T(4,128)(2,1)S(1)}, u32[]{:S(2)}, u32[]{:S(2)}) collective-permute-start(bf16[3,1024]{1,0:T(4,128)(2,1)S(1)} %slice.3), channel_id=1, source_target_pairs={{0,2},{2,4},{4,6},{6,8},{8,10},{10,12},{12,14},{14,16},{16,18},{18... | collective-permute-start | bytes 18440 | tf_op jit(solution)/shard_map/ppermute | solution.py:288
  5.4 1.0 copy-start.16
  6.5 1.0 copy-start.17
  7.5 1.0 copy-start.18
  8.6 0.7 copy-start.19
  9.3 0.7 copy-start.20
  9.9 0.7 copy-start.21
  15.5 0.8 copy-start.10
  16.3 29.4 %copy-start.22 = (s32[128,4]{0,1:T(4,128)S(1)}, s32[128,4]{0,1:T(4,128)}, u32[]{:S(2)}) copy-start(s32[128,4]{0,1:T(4,128)} %param.29) | copy-start | bytes 6148
  16.3 29.4 %copy-start.23 = (f32[128,4]{0,1:T(4,128)S(1)}, f32[128,4]{0,1:T(4,128)}, u32[]{:S(2)}) copy-start(f32[128,4]{0,1:T(4,128)} %param.30) | copy-start | bytes 6148
  16.3 30.8 %copy-start.9 = (bf16[128,2048]{1,0:T(8,128)(2,1)S(1)}, bf16[128,2048]{1,0:T(8,128)(2,1)}, u32[]{:S(2)}) copy-start(bf16[128,2048]{1,0:T(8,128)(2,1)} %res_ref.1) | copy-start | bytes 1572868
  16.3 23.0 %all-to-all-start = ((f32[64,2,1024]{2,1,0:T(2,128)}), f32[64,2,1024]{2,1,0:T(2,128)S(1)}, u32[]{:S(2)}, u32[]{:S(2)}) async-start(f32[64,2,1024]{2,1,0:T(2,128)} %copy-done.10), calls=%async_computation | async-start | bytes 1048576 | tf_op jit(solution)/shard_map/all_to_all | solution.py:300
  39.3 1.0 copy-start.11
  42.5 8.8 %collective-permute-start.1 = (bf16[128,1024]{1,0:T(8,128)(2,1)S(1)}, bf16[128,1024]{1,0:T(8,128)(2,1)S(1)}, u32[]{:S(2)}, u32[]{:S(2)}) collective-permute-start(bf16[128,1024]{1,0:T(8,128)(2,1)S(1)} %get-tuple-element.22), channel_id=1, source_target_pairs={{0,1},{1,0},{2,3},{3,2},{4,5},{5,4},{6,7},{7,6},{8,9},{9,8},{10,11... | collective-permute-start | bytes 786440 | tf_op jit(solution)/shard_map/ppermute | solution.py:312
  46.3 0.8 copy-start.6
  47.1 4.2 %copy-start.15 = (f32[2048]{0:T(1024)S(1)}, f32[2048]{0:T(1024)}, u32[]{:S(2)}) copy-start(f32[2048]{0:T(1024)} %param.28) | copy-start | bytes 24580
  58.3 0.8 copy-start.12
  61.3 34.1 %all-to-all-start.1 = ((bf16[128,4,2048]{2,1,0:T(4,128)(2,1)}), bf16[128,4,2048]{2,1,0:T(4,128)(2,1)S(1)}, u32[]{:S(2)}, u32[]{:S(2)}) async-start(bf16[128,4,2048]{2,1,0:T(4,128)(2,1)} %reshape.24), calls=%async_computation.1 | async-start | bytes 4194304 | tf_op jit(solution)/shard_map/all_to_all | solution.py:327
  95.4 1.3 copy-start.24
  96.8 35.7 %all-to-all-start.3 = ((bf16[128,4,2048]{2,1,0:T(4,128)(2,1)}), bf16[128,4,2048]{2,1,0:T(4,128)(2,1)}, u32[]{:S(2)}, u32[]{:S(2)}) async-start(bf16[128,4,2048]{2,1,0:T(4,128)(2,1)} %reshape.28), calls=%async_computation.3 | async-start | bytes 4194304 | tf_op jit(solution)/shard_map/all_to_all | solution.py:327
  111.4 1.4 copy-start.2
  132.5 35.7 %all-to-all-start.2 = ((bf16[128,4,2048]{2,1,0:T(4,128)(2,1)}), bf16[128,4,2048]{2,1,0:T(4,128)(2,1)}, u32[]{:S(2)}, u32[]{:S(2)}) async-start(bf16[128,4,2048]{2,1,0:T(4,128)(2,1)} %reshape.26), calls=%async_computation.2 | async-start | bytes 4194304 | tf_op jit(solution)/shard_map/all_to_all | solution.py:327
  147.1 1.4 copy-start.3
  152.6 21.2 %copy-start.4 = (bf16[2048,512]{1,0:T(8,128)(2,1)S(1)}, bf16[2048,512]{1,0:T(8,128)(2,1)}, u32[]{:S(2)}) copy-start(bf16[2048,512]{1,0:T(8,128)(2,1)} %gate_ref.5) | copy-start | bytes 6291460
  168.2 35.9 %all-to-all-start.4 = ((bf16[128,4,2048]{2,1,0:T(4,128)(2,1)}), bf16[128,4,2048]{2,1,0:T(4,128)(2,1)}, u32[]{:S(2)}, u32[]{:S(2)}) async-start(bf16[128,4,2048]{2,1,0:T(4,128)(2,1)} %reshape.30), calls=%async_computation.4 | async-start | bytes 4194304 | tf_op jit(solution)/shard_map/all_to_all | solution.py:327
  173.9 1.6 copy-start.5
  175.5 1.0 copy-start.13
  181.8 1.0 copy-start.7
  183.5 1.0 copy-start
  184.5 22.2 %copy-start.14 = (f32[2048]{0:T(1024)S(1)}, f32[2048]{0:T(1024)}, u32[]{:S(2)}) copy-start(f32[2048]{0:T(1024)} %param.37) | copy-start | bytes 24580
  204.1 2.6 %copy-start.1 = (f32[128,2048]{1,0:T(8,128)S(1)}, f32[128,2048]{1,0:T(8,128)}, u32[]{:S(2)}) copy-start(f32[128,2048]{1,0:T(8,128)} %copy-done) | copy-start | bytes 3145732
  206.7 1.0 copy-start.8

commit v2 on v1

v2 whole, which is shorter than its diff:
```python
import functools

import jax
import jax.numpy as jnp
from jax import lax
from jax.experimental import pallas as pl
from jax.experimental.pallas import tpu as pltpu
from jax.sharding import PartitionSpec as P

ALPHA = 8.0**0.25
RATE_C = 8.0
NORM_EPS = 1e-05
CAP = 8
BLOCK = 256
LANES = 8
F32 = jnp.float32
BF16 = jnp.bfloat16
VMEM = pl.BlockSpec(memory_space=pltpu.VMEM)
SMEM = pl.BlockSpec(memory_space=pltpu.SMEM)
HBM = pl.BlockSpec(memory_space=pltpu.HBM)


def call(
    kernel, out_shape, in_specs, flops, scratch=(), name=None, out_specs=None, grid=(), limit=16
):
    if out_specs is None:
        out_specs = jax.tree.map(lambda _: VMEM, out_shape)
    return pl.pallas_call(
        kernel,
        out_shape=out_shape,
        in_specs=in_specs,
        out_specs=out_specs,
        grid=grid,
        scratch_shapes=list(scratch),
        compiler_params=pltpu.CompilerParams(vmem_limit_bytes=limit * 2**20),
        cost_estimate=pl.CostEstimate(flops=flops, bytes_accessed=2**20, transcendentals=0),
        name=name,
    )


def shape(dims, dtype):
    return jax.ShapeDtypeStruct(dims, dtype)


def log1p_unit(u):
    s = u / (2.0 + u)
    q = s * s
    total = jnp.full_like(s, 1.0 / 17.0)
    for k in (15, 13, 11, 9, 7, 5, 3, 1):
        total = total * q + 1.0 / k
    return 2.0 * s * total


def minus_expm1(y):
    total = jnp.full_like(y, 1.0 / 362880.0)
    for k in (40320, 5040, 720, 120, 24, 6, 2, 1):
        total = total * y + 1.0 / k
    return jnp.where(y > -0.5, -y * total, 1.0 - jnp.exp(y))


def strided(ref, start, stride):
    parts = [ref[c, pl.ds(start, LANES, stride=stride), :] for c in range(ref.shape[0])]
    return jnp.concatenate(parts, axis=1)


def layer_norm(values, gains):
    center = values - jnp.mean(values, axis=-1, keepdims=True)
    spread = jnp.mean(center * center, axis=-1, keepdims=True)
    return center * lax.rsqrt(spread + NORM_EPS) * gains


def fetch(pairs, sems):
    copies = [pltpu.make_async_copy(a, b, sems.at[i]) for i, (a, b) in enumerate(pairs)]
    for copy in copies:
        copy.start()
    return copies


def elements(conv, recur, gain, slope, moved):
    log_decay = slope * jax.nn.sigmoid(recur) + moved
    update = jnp.sqrt(minus_expm1(2.0 * log_decay)) * jax.nn.sigmoid(gain) * conv
    return jnp.exp(log_decay), update


def scan_kernel(
    halo_ref, x_hbm, taps_hbm, rmap_hbm, imap_hbm, rate_hbm, shift_hbm, gate_hbm, routes_hbm,
    weight_hbm, tot_hbm, p_hbm, q_hbm, g_hbm, c_hbm,
    x_ref, taps_ref, rmap_ref, imap_ref, rate_ref, shift_ref, gate_ref, routes_ref, weight_ref,
    tot_ref, p_ref, q_ref, g_ref, c_ref, ext, cv, rg, ig, sh, hs, rs, sems, outs,
):
    copies = fetch(
        [
            (x_hbm, x_ref),
            (shift_hbm, shift_ref),
            (taps_hbm, taps_ref),
            (rate_hbm, rate_ref),
            (rmap_hbm, rmap_ref),
            (imap_hbm, imap_ref),
            (gate_hbm, gate_ref),
            (routes_hbm, routes_ref),
            (weight_hbm, weight_ref),
        ],
        sems,
    )
    tokens, channels = x_ref.shape
    steps = tokens // LANES
    heads, width = rmap_ref.shape[:2]
    reach = taps_ref.shape[0] - 1
    pad = 8 - reach
    for copy in copies[:4]:
        copy.wait()
    for c in range(ext.shape[0]):
        cols = slice(c * 128, (c + 1) * 128)
        ext[c, pl.ds(pad, reach), :] = halo_ref[:, cols].astype(F32)
        ext[c, pl.ds(8, tokens), :] = x_ref[:, cols].astype(F32)
    taps = [taps_ref[pl.ds(j, 1), :].astype(F32) for j in range(reach + 1)]
    full = jnp.concatenate([shift_ref[...], jnp.zeros((128 - heads, tokens), F32)], axis=0)
    sh[...] = jnp.transpose(full)
    logit = -rate_ref[...]
    slope = -RATE_C * (jnp.maximum(logit, 0.0) + log1p_unit(jnp.exp(-jnp.abs(logit))))

    def conv(t, _):
        total = jnp.zeros((LANES, channels), F32)
        for j in range(reach + 1):
            total = total + taps[j] * strided(ext, t + pad + j, steps)
        cv[pl.ds(pl.multiple_of(t * LANES, LANES), LANES), :] = total.astype(BF16).astype(F32)
        return 0

    lax.fori_loop(0, steps, conv, 0, unroll=4)
    for copy in copies[4:6]:
        copy.wait()
    for k in range(heads):
        cols = slice(k * width, (k + 1) * width)
        block = cv[:, cols].astype(BF16)
        rg[:, cols] = jnp.dot(block, rmap_ref[k], preferred_element_type=F32)
        ig[:, cols] = jnp.dot(block, imap_ref[k], preferred_element_type=F32)

    def step(t, carry):
        rows = pl.ds(pl.multiple_of(t * LANES, LANES), LANES)
        moved = sh[pl.ds(t, LANES, stride=steps), :]
        out = []
        for k in range(heads):
            h, run = carry[k]
            cols = slice(k * width, (k + 1) * width)
            decay, update = elements(
                cv[rows, cols], rg[rows, cols], ig[rows, cols], slope[:, cols], moved[:, k : k + 1]
            )
            h = decay * h + update
            run = decay * run
            for j in range(width // 128):
                at, part = k * (width // 128) + j, slice(j * 128, (j + 1) * 128)
                hs[at, pl.ds(t, LANES, stride=steps), :] = h[:, part]
                rs[at, pl.ds(t, LANES, stride=steps), :] = run[:, part]
            out.append((h, run))
        return tuple(out)

    start = tuple(
        (jnp.zeros((LANES, width), F32), jnp.ones((LANES, width), F32)) for _ in range(heads)
    )
    last = lax.fori_loop(0, steps, step, start, unroll=2)
    row = lax.broadcasted_iota(jnp.int32, (LANES, width), 0)
    enter, scale = [], []
    for k in range(heads):
        cols = slice(k * width, (k + 1) * width)
        h, a = last[k]
        for d in (1, 2, 4):
            hp, ap = pltpu.roll(h, d, 0), pltpu.roll(a, d, 0)
            h = jnp.where(row >= d, a * hp + h, h)
            a = jnp.where(row >= d, a * ap, a)
        enter.append(jnp.where(row >= 1, pltpu.roll(h, 1, 0), 0.0))
        scale.append(jnp.where(row >= 1, pltpu.roll(a, 1, 0), 1.0))
        both = jnp.concatenate([a[LANES - 1 :], h[LANES - 1 :]], axis=0)
        tot_ref[:, :, cols] = jnp.broadcast_to(both[None], (tot_ref.shape[0], 2, width))
    out_copies = [pltpu.make_async_copy(tot_ref, tot_hbm, outs.at[0])]
    out_copies[0].start()
    for copy in copies[6:]:
        copy.wait()
    enter, scale = jnp.concatenate(enter, axis=1), jnp.concatenate(scale, axis=1)
    block = 16
    for chunk in range(LANES):
        head, by = enter[chunk : chunk + 1], scale[chunk : chunk + 1]

        def put(i, _):
            rows = pl.ds(pl.multiple_of(chunk * steps + i * block, block), block)
            gate = jax.nn.gelu(gate_ref[rows, :].astype(F32), approximate=True)
            for c in range(hs.shape[0]):
                cols = slice(c * 128, (c + 1) * 128)
                run = rs[c, rows, :]
                p_ref[rows, cols] = (hs[c, rows, :] + run * head[:, cols]) * gate[:, cols]
                q_ref[rows, cols] = run * by[:, cols] * gate[:, cols]
            return 0

        lax.fori_loop(0, steps // block, put, 0)
    route(routes_ref, weight_ref, g_ref, c_ref)
    for i, (ref, hbm) in enumerate(
        ((p_ref, p_hbm), (q_ref, q_hbm), (g_ref, g_hbm), (c_ref, c_hbm))
    ):
        copy = pltpu.make_async_copy(ref, hbm, outs.at[i + 1])
        copy.start()
        out_copies.append(copy)
    for copy in out_copies:
        copy.wait()


def mix_kernel(index_ref, seen_ref, p_ref, q_ref, mine_ref, theirs_ref):
    tokens, channels = p_ref.shape
    here, side = index_ref[0], index_ref[1]

    def fold(i, c):
        pair = seen_ref[i]
        return pair[0:1] * c + pair[1:2]

    carried = lax.fori_loop(0, here, fold, jnp.zeros((1, channels), F32))
    half = tokens // 2
    block = 16

    def put(i, _):
        at = pl.multiple_of(i * block, block)
        for ref, part in ((theirs_ref, 1 - side), (mine_ref, side)):
            rows = pl.ds(pl.multiple_of(part * half + at, block), block)
            ref[pl.ds(at, block), :] = (p_ref[rows, :] + q_ref[rows, :] * carried).astype(BF16)
        return 0

    lax.fori_loop(0, half // block, put, 0, unroll=2)


def route(routes_ref, weight_ref, g_ref, c_ref):
    fanout, rows = routes_ref.shape
    slots = g_ref.shape[0]
    experts = slots // CAP
    expert = lax.broadcasted_iota(jnp.int32, (experts, rows), 0)
    member = jnp.zeros((experts, rows), F32)
    weight = jnp.zeros((experts, rows), F32)
    for k in range(fanout):
        hit = expert == routes_ref[pl.ds(k, 1), :]
        member = member + jnp.where(hit, 1.0, 0.0)
        weight = weight + jnp.where(hit, weight_ref[pl.ds(k, 1), :], 0.0)
    earlier = (
        lax.broadcasted_iota(jnp.int32, (rows, rows), 0)
        < lax.broadcasted_iota(jnp.int32, (rows, rows), 1)
    )
    rank = jnp.dot(
        member.astype(BF16), jnp.where(earlier, 1.0, 0.0).astype(BF16), preferred_element_type=F32
    )
    rank = jnp.where(member > 0.0, rank, -1.0).astype(BF16)
    high = weight.astype(BF16)
    low = (weight - high.astype(F32)).astype(BF16)
    slot = lax.broadcasted_iota(jnp.int32, (BLOCK, experts), 0)
    spread_at = lax.broadcasted_iota(jnp.int32, (BLOCK, experts), 1)
    place = (lax.broadcasted_iota(jnp.int32, (BLOCK, rows), 0) % CAP).astype(F32)
    for b in range(slots // BLOCK):
        spread = jnp.where((slot + b * BLOCK) // CAP == spread_at, 1.0, 0.0).astype(BF16)

        def to_slots(values):
            return jnp.dot(spread, values, preferred_element_type=F32)

        chosen = to_slots(rank) == place
        g_ref[pl.ds(b * BLOCK, BLOCK), :] = jnp.where(chosen, 1.0, 0.0).astype(BF16)
        c_ref[b, :rows] = jnp.transpose(jnp.where(chosen, to_slots(high), 0.0)).astype(BF16)
        c_ref[b, rows:] = jnp.transpose(jnp.where(chosen, to_slots(low), 0.0)).astype(BF16)


def project_kernel(index_ref, mine_ref, w_ref, res_ref, out_ref):
    depth = mine_ref.shape[1]
    rows = pl.ds(pl.multiple_of(index_ref[1] * depth, depth), depth)
    out_ref[...] = ALPHA * res_ref[...].astype(F32) + jnp.dot(
        mine_ref[...], w_ref[rows, :], preferred_element_type=F32
    )


def dispatch_kernel(index_ref, other_ref, w_ref, acc_ref, gain_ref, g_ref, normed_ref, out_ref):
    @pl.when(pl.program_id(0) == 0)
    def _():
        depth = other_ref.shape[1]
        rows = pl.ds(pl.multiple_of((1 - index_ref[1]) * depth, depth), depth)
        values = acc_ref[...] + jnp.dot(other_ref[...], w_ref[rows, :], preferred_element_type=F32)
        normed_ref[...] = layer_norm(values, gain_ref[...]).astype(BF16)

    out_ref[...] = jnp.dot(
        g_ref[...], normed_ref[...], preferred_element_type=F32
    ).astype(BF16)


def hidden_of(x, gate, up):
    return (
        jax.nn.silu(jnp.dot(x, gate, preferred_element_type=F32))
        * jnp.dot(x, up, preferred_element_type=F32)
    ).astype(BF16)


def shared_kernel(x_ref, gate_ref, up_ref, down_ref, out_ref):
    x = x_ref[...]
    hidden = hidden_of(x, gate_ref[...], up_ref[...])
    out_ref[...] = ALPHA * x.astype(F32) + jnp.dot(
        hidden, down_ref[...], preferred_element_type=F32
    )


def expert_kernel(x_ref, gate_ref, up_ref, down_ref, out_ref):
    hidden = hidden_of(x_ref[...], gate_ref[0], up_ref[0])
    out_ref[...] = jnp.dot(hidden, down_ref[0], preferred_element_type=F32).astype(BF16)


def finish_kernel(base_ref, c_ref, back_ref, gain_ref, out_ref, acc):
    i = pl.program_id(0)
    part = jnp.dot(c_ref[i], back_ref[...], preferred_element_type=F32)
    rows = part.shape[0] // 2
    part = part[:rows] + part[rows:]

    @pl.when(i == 0)
    def _():
        acc[...] = base_ref[...] + part

    @pl.when(i > 0)
    def _():
        acc[...] += part

    @pl.when(i == pl.num_programs(0) - 1)
    def _():
        out_ref[...] = layer_norm(acc[...], gain_ref[...]).astype(BF16)


def on_device(
    gate_pre, conv_in, conv_taps, recur_map, input_map, rate_logit, decay_shift, out_weight,
    residual, gain_mix, routes, route_weight, shared_gate, shared_up, shared_down, expert_gate,
    expert_up, expert_down, gain_out,
):
    tokens, channels = conv_in.shape
    reach = conv_taps.shape[0] - 1
    sp, tp = lax.axis_size("sp"), lax.axis_size("tp")
    experts = sp * tp
    rows = tokens // tp
    model = out_weight.shape[1]
    slots = experts * CAP
    blocks = slots // BLOCK
    sem = pltpu.SemaphoreType.DMA
    index = jnp.stack([lax.axis_index("sp"), lax.axis_index("tp")]).astype(jnp.int32)
    before = lax.ppermute(conv_in[tokens - reach :], "sp", [(i, i + 1) for i in range(sp - 1)])
    before, index = lax.optimization_barrier((before, index))
    grid = shape((tokens, channels), F32)
    big = pltpu.VMEM((tokens, channels), F32)
    lanes = pltpu.VMEM((channels // 128, tokens, 128), F32)
    operands = (
        conv_in, conv_taps, recur_map, input_map, rate_logit[None], decay_shift.T, gate_pre,
        routes.T, route_weight.T,
    )
    made = (
        shape((sp, 2, channels), F32), grid, grid, shape((slots, rows), BF16),
        shape((blocks, 2 * rows, BLOCK), BF16),
    )
    totals, p, q, g, c = call(
        scan_kernel,
        made,
        [VMEM] + [HBM] * len(operands),
        10**9,
        [pltpu.VMEM(x.shape, x.dtype) for x in operands + made]
        + [pltpu.VMEM((channels // 128, tokens + 8, 128), F32), big, big, big]
        + [pltpu.VMEM((tokens, 128), F32), lanes, lanes, sem((len(operands),)), sem((len(made),))],
        name="scan",
        out_specs=(HBM,) * len(made),
        limit=62,
    )(before, *operands)
    seen = lax.all_to_all(totals, "sp", 0, 0, tiled=True)
    piece = shape((rows, channels), BF16)
    mine, theirs = call(mix_kernel, (piece, piece), [SMEM] + [VMEM] * 3, 10**8, name="mix")(
        index, seen, p, q
    )
    other = lax.ppermute(theirs, "tp", [(0, 1), (1, 0)])
    wide = shape((rows, model), F32)
    acc = call(project_kernel, wide, [SMEM] + [VMEM] * 3, 10**9, name="project")(
        index, mine, out_weight, residual
    )
    strip = pl.BlockSpec((BLOCK, model), lambda i: (i, 0))
    normed, outgoing = call(
        dispatch_kernel,
        (shape((rows, model), BF16), shape((slots, model), BF16)),
        [SMEM] + [VMEM] * 4 + [pl.BlockSpec((BLOCK, rows), lambda i: (i, 0))],
        2 * 10**9,
        name="dispatch",
        out_specs=(VMEM, strip),
        grid=(blocks,),
    )(index, other, out_weight, acc, gain_mix[None], g)

    def exchanged(x):
        x = x.reshape(experts, CAP, model)
        x = lax.all_to_all(x, ("sp", "tp"), split_axis=0, concat_axis=0, tiled=True)
        return x.reshape(slots, model)

    received = exchanged(outgoing)
    results = call(
        expert_kernel,
        shape((slots, model), BF16),
        [strip] + [VMEM] * 3,
        6 * 10**9,
        name="expert",
        out_specs=strip,
        grid=(blocks,),
    )(received, expert_gate, expert_up, expert_down)
    normed, results = lax.optimization_barrier((normed, results))
    base = call(shared_kernel, wide, [VMEM] * 4, 10**10, name="shared")(
        normed, shared_gate, shared_up, shared_down
    )
    base, results = lax.optimization_barrier((base, results))
    back = exchanged(results)
    return call(
        finish_kernel,
        shape((rows, model), BF16),
        [VMEM, VMEM, strip, VMEM],
        10**9,
        [pltpu.VMEM((rows, model), F32)],
        name="finish",
        grid=(blocks,),
    )(base, c, back, gain_out[None])


def solution(mesh):
    return jax.shard_map(
        on_device,
        mesh=mesh,
        in_specs=(
            P("sp", "tp"),
            P("sp", "tp"),
            P(None, "tp"),
            P("tp", None, None),
            P("tp", None, None),
            P("tp"),
            P("sp", "tp"),
            P(),
            P(("sp", "tp"), None),
            P(),
            P(("sp", "tp"), None),
            P(("sp", "tp"), None),
            P(),
            P(),
            P(),
            P(("sp", "tp"), None, None),
            P(("sp", "tp"), None, None),
            P(("sp", "tp"), None, None),
            P(),
        ),
        out_specs=P(("sp", "tp"), None),
        check_vma=False,
    )
```

time: 211 us -> 180 us (0.85)
  blocking collectives: 0 us -> 136 us
  waiting for transfers between devices: 89 us -> 0.7 us
  local copies, waits for them, and re-layouts: 44 us -> 7.21 us
  starting transfers between devices: 39 us -> 7.05 us
  Pallas kernels: 37.2 us -> 27.7 us
    all_to_all x0 -> x3, blocking collectives: none -> 136 us  [the longest x2 113 us: exchanged(): x = lax.all_to_all(x, ('sp', 'tp'), split_axis=0, concat_axis=0, tiled=True)]
    all_to_all x5 -> x0, waiting for transfers between devices: 88.2 us -> none  [the longest x4 77.1 us: exchanged(): x = lax.all_to_all(x, ('sp', 'tp'), split_axis=0, concat_axis=0, tiled=True)]
    all_to_all x5 -> x0, starting transfers between devices: 32 us -> none  [the longest x4 20.2 us: exchanged(): x = lax.all_to_all(x, ('sp', 'tp'), split_axis=0, concat_axis=0, tiled=True)]
    reshape x8 -> x0, local copies, waits for them, and re-layouts: 24.8 us -> none  [the longest x4 14.6 us: exchanged(): x = x.reshape(experts, CAP // PARTS, model)]
    unnamed x50 -> x30, local copies, waits for them, and re-layouts: 18.5 us -> 6.49 us
    pallas_call x9 -> x6, Pallas kernels: 33 us -> 26.4 us  [the longest x1 10.4 us: on_device(): call(scan_kernel, made, [VMEM] + [HBM] * len(operands), 10 ** 9, [pltpu.V...]
    pallas_call x1, Pallas kernels: 4.13 us -> 1.28 us  [on_device(): call(project_kernel, wide, [SMEM] + [VMEM] * 3, 10 ** 9, name='project')]
  transfers between devices with their start and end apart: 7 -> 2, of which waited for: 6 -> 1; matrix products, arithmetic and copies ran while one was open for 10% -> 0% of each run, Pallas kernels for 10% -> 1%
where the time goes in v2:
time: 180 us; the launch traced here: 179 us
  blocking collectives  136 us (76%)
  Pallas kernels  27.7 us (15%)
  local copies, waits for them, and re-layouts  7.21 us (4%)
  starting transfers between devices  7.05 us (4%)
    all_to_all x2, blocking collectives, exchanged(): x = lax.all_to_all(x, ('sp', 'tp'), split_axis=0, concat_axis=0, tiled=True)  113 us
    all_to_all x1, blocking collectives, on_device(): seen = lax.all_to_all(totals, 'sp', 0, 0, tiled=True)  23 us
    pallas_call x1, Pallas kernels, on_device(): call(scan_kernel, made, [VMEM] + [HBM] * len(operands), 10 ** 9, [pltpu.V...  10.4 us
    pallas_call x1, Pallas kernels, on_device(): call(expert_kernel, shape((slots, model), BF16), [strip] + [VMEM] * 3, 6...  7.53 us
    unnamed x30, local copies, waits for them, and re-layouts  6.49 us
    ppermute x1, starting transfers between devices, on_device(): lax.ppermute(conv_in[tokens - reach:], 'sp', [(i, i + 1) for i in range(s...  3.92 us
  transfers between devices with their start and end apart: 2, of which 1 were waited for; matrix products, arithmetic and copies ran while one was open for 0% of the time, Pallas kernels for 1%

profile of v2, /device:TPU:1, one launch (start us, length us, event | category | flops | bytes accessed | tf_op | source)
XLA Modules:
  0.0 179.3 jit_solution(510824589109643153)
XLA Ops:
  0.0 0.7 slice.3
  0.7 3.9 %collective-permute-start = (bf16[3,1024]{1,0:T(4,128)(2,1)S(1)}, bf16[3,1024]{1,0:T(4,128)(2,1)S(1)}, u32[]{:S(2)}, u32[]{:S(2)}) collective-permute-start(bf16[3,1024]{1,0:T(4,128)(2,1)S(1)} %slice.3), channel_id=1, source_target_pairs={{0,2},{2,4},{4,6},{6,8},{8,10},{10,12},{12,14},{14,16},{16,18},{18... | collective-permute-start | bytes 18440 | tf_op jit(solution)/shard_map/ppermute | solution.py:338
  4.7 0.1 pad_add_fusion.index_ref
  4.7 0.7 collective-permute-done.halo_ref
  5.4 0.0 copy-start.14
  5.4 0.6 copy-done.14
  6.0 10.4 %scan.1 = (f32[64,2,1024]{2,1,0:T(2,128)}, f32[256,1024]{1,0:T(8,128)}, f32[256,1024]{1,0:T(8,128)}, bf16[1024,128]{1,0:T(8,128)(2,1)}, bf16[4,256,256]{2,1,0:T(8,128)(2,1)}) custom-call(bf16[3,1024]{1,0:T(4,128)(2,1)} %copy-done.14, bf16[256,1024]{1,0:T(8,128)(2,1)} %x_hbm.1, bf16[4,1024]{1,0:T(4,128)(2,1)} %taps_hbm.1, bf16[4,256,256]{2,1,0:T(8,128)(2,1)} %rmap_hbm.1, ...), custom_call_target="tpu_custom_call" | custom-call | flops 1000000000 | bytes 1048576 | tf_op jit(solution)/shard_map/scan/pallas_call | solution.py:351
  16.4 0.0 copy-start.3
  16.5 23.0 %all_to_all.15.seen_ref = f32[64,2,1024]{2,1,0:T(2,128)S(1)} all-to-all(f32[64,2,1024]{2,1,0:T(2,128)} %get-tuple-element.22), channel_id=1, replica_groups=mesh['sp'=64,'tp'=2] {'sp'}, dimensions={0} | all-to-all | bytes 1048576 | tf_op jit(solution)/shard_map/all_to_all | solution.py:363
  39.5 0.0 copy-start.1
  39.5 1.2 copy-done.1
  40.7 0.0 copy-start.2
  40.7 1.2 copy-done.2
  41.9 0.7 mix.1
  42.6 3.1 %collective-permute-start.1 = (bf16[128,1024]{1,0:T(8,128)(2,1)S(1)}, bf16[128,1024]{1,0:T(8,128)(2,1)S(1)}, u32[]{:S(2)}, u32[]{:S(2)}) collective-permute-start(bf16[128,1024]{1,0:T(8,128)(2,1)S(1)} %get-tuple-element.25), channel_id=1, source_target_pairs={{0,1},{1,0},{2,3},{3,2},{4,5},{5,4},{6,7},{7,6},{8,9},{9,8},{10,11... | collective-permute-start | bytes 786440 | tf_op jit(solution)/shard_map/ppermute | solution.py:368
  45.7 0.0 copy-done.3
  45.8 0.0 copy-start
  45.8 3.4 %copy-done = bf16[2048,2048]{1,0:T(8,128)(2,1)S(1)} copy-done((bf16[2048,2048]{1,0:T(8,128)(2,1)S(1)}, bf16[2048,2048]{1,0:T(8,128)(2,1)}, u32[]{:S(2)}) %copy-start) | copy-done | bytes 8388632
  49.1 0.0 copy-start.5
  49.1 0.0 copy-start.7
  49.1 1.3 project.1.acc_ref
  50.4 0.0 collective-permute-done.1.other_ref
  50.4 0.0 copy-done.5
  50.4 0.0 copy-done.7
  50.5 3.4 %dispatch.1 = (bf16[128,2048]{1,0:T(8,128)(2,1)S(1)}, bf16[1024,2048]{1,0:T(8,128)(2,1)S(1)}) custom-call(s32[2]{0:T(128)S(1)} %pad_add_fusion.index_ref, bf16[128,1024]{1,0:T(8,128)(2,1)S(1)} %collective-permute-done.1.other_ref, bf16[2048,2048]{1,0:T(8,128)(2,1)S(1)} %copy-done, f32[128,2048]{1,0:T(8,128)S(1)} %project.1.acc_ref, f32[1,2048]{1,0:T(1,128)S(1)} %bitcast.17, ...), custom_call_target="tpu_custom_call" | custom-call | flops 2000000000 | bytes 1048576 | tf_op jit(solution)/shard_map/dispatch/pallas_call | solution.py:374
  53.8 0.0 copy-start.8
  53.8 0.0 copy-start.9
  53.8 0.0 copy-start.10
  53.9 56.4 %all_to_all.16 = bf16[128,8,2048]{2,1,0:T(8,128)(2,1)S(1)} all-to-all(bf16[128,8,2048]{2,1,0:T(8,128)(2,1)S(1)} %bitcast.13), channel_id=1, replica_groups=mesh['sp'=64,'tp'=2] {'sp','tp'}, dimensions={0} | all-to-all | bytes 8388608 | tf_op jit(solution)/shard_map/all_to_all | solution.py:386
  110.2 0.0 copy-done.8
  110.2 0.0 copy-done.9
  110.2 0.0 copy-done.10
  110.2 0.0 copy-start.11
  110.3 0.0 copy-start.12
  110.3 0.0 copy-start.13
  110.3 7.5 %expert.1 = bf16[1024,2048]{1,0:T(8,128)(2,1)S(1)} custom-call(bf16[1024,2048]{1,0:T(8,128)(2,1)S(1)} %bitcast.15, bf16[1,2048,512]{2,1,0:T(8,128)(2,1)S(1)} %copy-done.8, bf16[1,2048,512]{2,1,0:T(8,128)(2,1)S(1)} %copy-done.9, bf16[1,512,2048]{2,1,0:T(8,128)(2,1)S(1)} %copy-done.10), custom_call_target="tpu_custom_call" | custom-call | flops 6000000000 | bytes 1048576 | tf_op jit(solution)/shard_map/expert/pallas_call | solution.py:390
  117.8 0.0 copy-done.11
  117.8 0.0 copy-done.12
  117.8 0.0 copy-done.13
  117.8 1.1 shared.1.base_ref
  119.0 0.0 copy-start.4
  119.0 0.0 copy-start.6
  119.0 57.0 %all_to_all.17 = bf16[128,8,2048]{2,1,0:T(8,128)(2,1)S(1)} all-to-all(bf16[128,8,2048]{2,1,0:T(8,128)(2,1)S(1)} %bitcast.14), channel_id=1, replica_groups=mesh['sp'=64,'tp'=2] {'sp','tp'}, dimensions={0} | all-to-all | bytes 8388608 | tf_op jit(solution)/shard_map/all_to_all | solution.py:386
  176.0 0.0 copy-done.4
  176.0 0.0 copy-done.6
  176.0 3.4 %finish.1 = bf16[128,2048]{1,0:T(8,128)(2,1)} custom-call(f32[128,2048]{1,0:T(8,128)S(1)} %shared.1.base_ref, bf16[4,256,256]{2,1,0:T(8,128)(2,1)S(1)} %copy-done.4, bf16[1024,2048]{1,0:T(8,128)(2,1)S(1)} %bitcast.12, f32[1,2048]{1,0:T(1,128)S(1)} %bitcast.16), custom_call_target="tpu_custom_call" | custom-call | flops 1000000000 | bytes 1048576 | tf_op jit(solution)/shard_map/finish/pallas_call | solution.py:405
Async XLA Ops:
  0.7 4.7 %collective-permute-start = (bf16[3,1024]{1,0:T(4,128)(2,1)S(1)}, bf16[3,1024]{1,0:T(4,128)(2,1)S(1)}, u32[]{:S(2)}, u32[]{:S(2)}) collective-permute-start(bf16[3,1024]{1,0:T(4,128)(2,1)S(1)} %slice.3), channel_id=1, source_target_pairs={{0,2},{2,4},{4,6},{6,8},{8,10},{10,12},{12,14},{14,16},{16,18},{18... | collective-permute-start | bytes 18440 | tf_op jit(solution)/shard_map/ppermute | solution.py:338
  5.4 0.6 copy-start.14
  16.4 29.3 %copy-start.3 = (bf16[128,2048]{1,0:T(8,128)(2,1)S(1)}, bf16[128,2048]{1,0:T(8,128)(2,1)}, u32[]{:S(2)}) copy-start(bf16[128,2048]{1,0:T(8,128)(2,1)} %res_ref.1) | copy-start | bytes 1572868
  39.5 1.2 copy-start.1
  40.7 1.2 copy-start.2
  42.6 7.8 %collective-permute-start.1 = (bf16[128,1024]{1,0:T(8,128)(2,1)S(1)}, bf16[128,1024]{1,0:T(8,128)(2,1)S(1)}, u32[]{:S(2)}, u32[]{:S(2)}) collective-permute-start(bf16[128,1024]{1,0:T(8,128)(2,1)S(1)} %get-tuple-element.25), channel_id=1, source_target_pairs={{0,1},{1,0},{2,3},{3,2},{4,5},{5,4},{6,7},{7,6},{8,9},{9,8},{10,11... | collective-permute-start | bytes 786440 | tf_op jit(solution)/shard_map/ppermute | solution.py:368
  45.8 3.4 %copy-start = (bf16[2048,2048]{1,0:T(8,128)(2,1)S(1)}, bf16[2048,2048]{1,0:T(8,128)(2,1)}, u32[]{:S(2)}) copy-start(bf16[2048,2048]{1,0:T(8,128)(2,1)} %w_ref.3) | copy-start | bytes 25165828
  49.1 1.3 copy-start.5
  49.1 1.3 copy-start.7
  53.8 56.4 %copy-start.8 = (bf16[1,2048,512]{2,1,0:T(8,128)(2,1)S(1)}, bf16[1,2048,512]{2,1,0:T(8,128)(2,1)}, u32[]{:S(2)}) copy-start(bf16[1,2048,512]{2,1,0:T(8,128)(2,1)} %gate_ref.2) | copy-start | bytes 6291460
  53.8 56.4 %copy-start.9 = (bf16[1,2048,512]{2,1,0:T(8,128)(2,1)S(1)}, bf16[1,2048,512]{2,1,0:T(8,128)(2,1)}, u32[]{:S(2)}) copy-start(bf16[1,2048,512]{2,1,0:T(8,128)(2,1)} %up_ref.2) | copy-start | bytes 6291460
  53.8 56.4 %copy-start.10 = (bf16[1,512,2048]{2,1,0:T(8,128)(2,1)S(1)}, bf16[1,512,2048]{2,1,0:T(8,128)(2,1)}, u32[]{:S(2)}) copy-start(bf16[1,512,2048]{2,1,0:T(8,128)(2,1)} %down_ref.2) | copy-start | bytes 6291460
  110.2 7.6 %copy-start.11 = (bf16[2048,512]{1,0:T(8,128)(2,1)S(1)}, bf16[2048,512]{1,0:T(8,128)(2,1)}, u32[]{:S(2)}) copy-start(bf16[2048,512]{1,0:T(8,128)(2,1)} %gate_ref.3) | copy-start | bytes 6291460
  110.3 7.6 %copy-start.12 = (bf16[2048,512]{1,0:T(8,128)(2,1)S(1)}, bf16[2048,512]{1,0:T(8,128)(2,1)}, u32[]{:S(2)}) copy-start(bf16[2048,512]{1,0:T(8,128)(2,1)} %up_ref.3) | copy-start | bytes 6291460
  110.3 7.6 %copy-start.13 = (bf16[512,2048]{1,0:T(8,128)(2,1)S(1)}, bf16[512,2048]{1,0:T(8,128)(2,1)}, u32[]{:S(2)}) copy-start(bf16[512,2048]{1,0:T(8,128)(2,1)} %down_ref.3) | copy-start | bytes 6291460
  119.0 57.0 %copy-start.4 = (bf16[4,256,256]{2,1,0:T(8,128)(2,1)S(1)}, bf16[4,256,256]{2,1,0:T(8,128)(2,1)}, u32[]{:S(2)}) copy-start(bf16[4,256,256]{2,1,0:T(8,128)(2,1)} %get-tuple-element.33.c_ref) | copy-start | bytes 1572868
  119.0 57.0 %copy-start.6 = (f32[2048]{0:T(1024)S(1)}, f32[2048]{0:T(1024)}, u32[]{:S(2)}) copy-start(f32[2048]{0:T(1024)} %param.37) | copy-start | bytes 24580

commit v3 on v2

v3 whole, which is shorter than its diff:
```python
import functools

import jax
import jax.numpy as jnp
from jax import lax
from jax.experimental import pallas as pl
from jax.experimental.pallas import tpu as pltpu
from jax.sharding import PartitionSpec as P

ALPHA = 8.0**0.25
RATE_C = 8.0
NORM_EPS = 1e-05
TINY = 1e-36
CAP = 8
BLOCK = 256
LANES = 8
F32 = jnp.float32
BF16 = jnp.bfloat16
VMEM = pl.BlockSpec(memory_space=pltpu.VMEM)
SMEM = pl.BlockSpec(memory_space=pltpu.SMEM)
HBM = pl.BlockSpec(memory_space=pltpu.HBM)


def call(
    kernel, out_shape, in_specs, flops, scratch=(), name=None, out_specs=None, grid=(), limit=16
):
    if out_specs is None:
        out_specs = jax.tree.map(lambda _: VMEM, out_shape)
    return pl.pallas_call(
        kernel,
        out_shape=out_shape,
        in_specs=in_specs,
        out_specs=out_specs,
        grid=grid,
        scratch_shapes=list(scratch),
        compiler_params=pltpu.CompilerParams(vmem_limit_bytes=limit * 2**20),
        cost_estimate=pl.CostEstimate(flops=flops, bytes_accessed=2**20, transcendentals=0),
        name=name,
    )


def shape(dims, dtype):
    return jax.ShapeDtypeStruct(dims, dtype)


def log1p_unit(u):
    s = u / (2.0 + u)
    q = s * s
    total = jnp.full_like(s, 1.0 / 17.0)
    for k in (15, 13, 11, 9, 7, 5, 3, 1):
        total = total * q + 1.0 / k
    return 2.0 * s * total


def minus_expm1_twice(x, decay):
    y = 2.0 * x
    total = jnp.full_like(y, 1.0 / 720.0)
    for k in (120, 24, 6, 2, 1):
        total = total * y + 1.0 / k
    return jnp.where(y > -0.125, -y * total, 1.0 - decay * decay)


def sigmoid(x):
    return 0.5 * jnp.tanh(0.5 * x) + 0.5


def layer_norm(values, gains):
    center = values - jnp.mean(values, axis=-1, keepdims=True)
    spread = jnp.mean(center * center, axis=-1, keepdims=True)
    return center * lax.rsqrt(spread + NORM_EPS) * gains


def fetch(pairs, sems):
    copies = [pltpu.make_async_copy(a, b, sems.at[i]) for i, (a, b) in enumerate(pairs)]
    for copy in copies:
        copy.start()
    return copies


def elements(conv, recur, gain, slope, moved):
    log_decay = slope * sigmoid(recur) + moved
    decay = jnp.exp(log_decay)
    power = minus_expm1_twice(log_decay, decay)
    return decay, power * lax.rsqrt(jnp.maximum(power, TINY)) * sigmoid(gain) * conv


def scan_kernel(
    halo_ref, x_hbm, taps_hbm, rmap_hbm, imap_hbm, rate_hbm, shift_hbm, tot_hbm, run_hbm, edge_hbm,
    x_ref, taps_ref, rmap_ref, imap_ref, rate_ref, shift_ref, tot_ref, run_ref, edge_ref,
    ext, cv, rg, ig, sh, sems, outs,
):
    copies = fetch(
        [
            (x_hbm, x_ref),
            (taps_hbm, taps_ref),
            (shift_hbm, shift_ref),
            (rate_hbm, rate_ref),
            (rmap_hbm, rmap_ref),
            (imap_hbm, imap_ref),
        ],
        sems,
    )
    tokens, channels = x_ref.shape
    steps = tokens // LANES
    stride = steps + 8
    heads, width = rmap_ref.shape[:2]
    reach = taps_ref.shape[0] - 1
    pad = 8 - reach
    for copy in copies[:2]:
        copy.wait()
    for c in range(channels // 128):
        cols = slice(c * 128, (c + 1) * 128)
        x = x_ref[:, cols].astype(F32)
        ext[c, pl.ds(pad, reach), :] = halo_ref[:, cols].astype(F32)
        for i in range(LANES):
            if i > 0:
                ext[c, pl.ds(stride * i, 8), :] = x[steps * i - 8 : steps * i]
            ext[c, pl.ds(stride * i + 8, steps), :] = x[steps * i : steps * (i + 1)]
        taps = [taps_ref[pl.ds(j, 1), cols].astype(F32) for j in range(reach + 1)]
        window = [ext[c, pl.ds(pad + j, LANES, stride=stride), :] for j in range(reach)]
        for t in range(steps):
            window.append(ext[c, pl.ds(8 + t, LANES, stride=stride), :])
            total = taps[0] * window[0]
            for j in range(1, reach + 1):
                total = total + taps[j] * window[j]
            window = window[1:]
            cv[pl.ds(t * LANES, LANES), cols] = total.astype(BF16).astype(F32)
    for copy in copies[2:]:
        copy.wait()
    for k in range(heads):
        cols = slice(k * width, (k + 1) * width)
        block = cv[:, cols].astype(BF16)
        rg[:, cols] = jnp.dot(block, rmap_ref[k], preferred_element_type=F32)
        ig[:, cols] = jnp.dot(block, imap_ref[k], preferred_element_type=F32)
    full = jnp.concatenate([shift_ref[...], jnp.zeros((128 - heads, tokens), F32)], axis=0)
    full = jnp.transpose(full)
    for i in range(LANES):
        sh[pl.ds(stride * i, steps), :] = full[steps * i : steps * (i + 1)]
    logit = -rate_ref[...]
    slope = -RATE_C * (jnp.maximum(logit, 0.0) + log1p_unit(jnp.exp(-jnp.abs(logit))))

    def step(t, carry):
        rows = pl.ds(pl.multiple_of(t * LANES, LANES), LANES)
        moved = sh[pl.ds(t, LANES, stride=stride), :]
        out = []
        for k in range(heads):
            h, run = carry[k]
            cols = slice(k * width, (k + 1) * width)
            decay, update = elements(
                cv[rows, cols], rg[rows, cols], ig[rows, cols], slope[:, cols], moved[:, k : k + 1]
            )
            h = decay * h + update
            run = decay * run
            run_ref[0, rows, cols] = h
            run_ref[1, rows, cols] = run
            out.append((h, run))
        return tuple(out)

    last = tuple(
        (jnp.zeros((LANES, width), F32), jnp.ones((LANES, width), F32)) for _ in range(heads)
    )
    sent = []
    for part in range(4):
        span = steps // 4
        last = lax.fori_loop(part * span, (part + 1) * span, step, last, unroll=2)
        rows = pl.ds(part * span * LANES, span * LANES)
        copy = pltpu.make_async_copy(run_ref.at[:, rows, :], run_hbm.at[:, rows, :], outs.at[part])
        copy.start()
        sent.append(copy)
    row = lax.broadcasted_iota(jnp.int32, (LANES, width), 0)
    for k in range(heads):
        cols = slice(k * width, (k + 1) * width)
        h, a = last[k]
        for d in (1, 2, 4):
            hp, ap = pltpu.roll(h, d, 0), pltpu.roll(a, d, 0)
            h = jnp.where(row >= d, a * hp + h, h)
            a = jnp.where(row >= d, a * ap, a)
        both = jnp.concatenate([a[LANES - 1 :], h[LANES - 1 :]], axis=0)
        tot_ref[:, :, cols] = jnp.broadcast_to(both[None], (tot_ref.shape[0], 2, width))
        edge_ref[0, :, cols] = jnp.where(row >= 1, pltpu.roll(h, 1, 0), 0.0)
        edge_ref[1, :, cols] = jnp.where(row >= 1, pltpu.roll(a, 1, 0), 1.0)
    sent += [
        pltpu.make_async_copy(tot_ref, tot_hbm, outs.at[4]),
        pltpu.make_async_copy(edge_ref, edge_hbm, outs.at[5]),
    ]
    for copy in sent[4:]:
        copy.start()
    for copy in sent:
        copy.wait()


def side_kernel(
    gate_hbm, routes_hbm, weight_hbm, run_hbm, edge_hbm, mixed_hbm, g_hbm, c_hbm,
    gate_ref, routes_ref, weight_ref, run_ref, edge_ref, mixed_ref, g_ref, c_ref, hs, rs, sems, outs,
):
    copies = fetch(
        [
            (routes_hbm, routes_ref),
            (weight_hbm, weight_ref),
            (gate_hbm, gate_ref),
            (run_hbm, run_ref),
            (edge_hbm, edge_ref),
        ],
        sems,
    )
    for copy in copies[:2]:
        copy.wait()
    route(routes_ref, weight_ref, g_ref, c_ref)
    for copy in copies[2:]:
        copy.wait()
    _, tokens, channels = run_ref.shape
    steps = tokens // LANES
    stride = steps + 8

    def step(t, _):
        rows = pl.ds(pl.multiple_of(t * LANES, LANES), LANES)
        run = run_ref[1, rows, :]
        own = run_ref[0, rows, :] + run * edge_ref[0]
        run = run * edge_ref[1]
        for c in range(hs.shape[0]):
            cols = slice(c * 128, (c + 1) * 128)
            hs[c, pl.ds(t, LANES, stride=stride), :] = own[:, cols]
            rs[c, pl.ds(t, LANES, stride=stride), :] = run[:, cols]
        return 0

    lax.fori_loop(0, steps, step, 0, unroll=2)
    block = 16

    def put(i, _):
        rows = pl.ds(pl.multiple_of(i * block, block), block)
        per = steps // block
        source = pl.ds(pl.multiple_of((i // per) * stride + (i % per) * block, 8), block)
        gate = jax.nn.gelu(gate_ref[rows, :].astype(F32), approximate=True)
        for c in range(hs.shape[0]):
            cols = slice(c * 128, (c + 1) * 128)
            mixed_ref[0, rows, cols] = hs[c, source, :] * gate[:, cols]
            mixed_ref[1, rows, cols] = rs[c, source, :] * gate[:, cols]
        return 0

    lax.fori_loop(0, tokens // block, put, 0)
    sent = [
        pltpu.make_async_copy(ref, hbm, outs.at[i])
        for i, (ref, hbm) in enumerate(((mixed_ref, mixed_hbm), (g_ref, g_hbm), (c_ref, c_hbm)))
    ]
    for copy in sent:
        copy.start()
    for copy in sent:
        copy.wait()


def mix_kernel(index_ref, seen_ref, mixed_ref, mine_ref, theirs_ref):
    _, tokens, channels = mixed_ref.shape
    here, side = index_ref[0], index_ref[1]

    def fold(i, c):
        pair = seen_ref[i]
        return pair[0:1] * c + pair[1:2]

    carried = lax.fori_loop(0, here, fold, jnp.zeros((1, channels), F32))
    half = tokens // 2
    block = 16

    def put(i, _):
        at = pl.multiple_of(i * block, block)
        for ref, part in ((theirs_ref, 1 - side), (mine_ref, side)):
            rows = pl.ds(pl.multiple_of(part * half + at, block), block)
            ref[pl.ds(at, block), :] = (mixed_ref[0, rows, :] + mixed_ref[1, rows, :] * carried).astype(
                BF16
            )
        return 0

    lax.fori_loop(0, half // block, put, 0, unroll=2)


def route(routes_ref, weight_ref, g_ref, c_ref):
    fanout, rows = routes_ref.shape
    slots = g_ref.shape[0]
    experts = slots // CAP
    expert = lax.broadcasted_iota(jnp.int32, (experts, rows), 0)
    member = jnp.zeros((experts, rows), F32)
    weight = jnp.zeros((experts, rows), F32)
    for k in range(fanout):
        hit = expert == routes_ref[pl.ds(k, 1), :]
        member = member + jnp.where(hit, 1.0, 0.0)
        weight = weight + jnp.where(hit, weight_ref[pl.ds(k, 1), :], 0.0)
    earlier = (
        lax.broadcasted_iota(jnp.int32, (rows, rows), 0)
        < lax.broadcasted_iota(jnp.int32, (rows, rows), 1)
    )
    rank = jnp.dot(
        member.astype(BF16), jnp.where(earlier, 1.0, 0.0).astype(BF16), preferred_element_type=F32
    )
    rank = jnp.where(member > 0.0, rank, -1.0).astype(BF16)
    high = weight.astype(BF16)
    low = (weight - high.astype(F32)).astype(BF16)
    slot = lax.broadcasted_iota(jnp.int32, (BLOCK, experts), 0)
    spread_at = lax.broadcasted_iota(jnp.int32, (BLOCK, experts), 1)
    place = (lax.broadcasted_iota(jnp.int32, (BLOCK, rows), 0) % CAP).astype(F32)
    for b in range(slots // BLOCK):
        spread = jnp.where((slot + b * BLOCK) // CAP == spread_at, 1.0, 0.0).astype(BF16)

        def to_slots(values):
            return jnp.dot(spread, values, preferred_element_type=F32)

        chosen = to_slots(rank) == place
        g_ref[pl.ds(b * BLOCK, BLOCK), :] = jnp.where(chosen, 1.0, 0.0).astype(BF16)
        cols = slice(b * BLOCK, (b + 1) * BLOCK)
        c_ref[:rows, cols] = jnp.transpose(jnp.where(chosen, to_slots(high), 0.0)).astype(BF16)
        c_ref[rows:, cols] = jnp.transpose(jnp.where(chosen, to_slots(low), 0.0)).astype(BF16)


def project_kernel(index_ref, mine_ref, res_ref, w_hbm, out_ref, rest_ref, own_ref, sems):
    depth = mine_ref.shape[1]
    side = index_ref[1]
    cut = depth // 4
    pairs = []
    for base, ref in ((side, own_ref), (1 - side, rest_ref)):
        for j in range(4):
            rows = pl.ds(pl.multiple_of(base * depth + j * cut, cut), cut)
            pairs.append((w_hbm.at[rows, :], ref.at[pl.ds(j * cut, cut), :]))
    copies = fetch(pairs, sems)
    out_ref[...] = ALPHA * res_ref[...].astype(F32)
    for j in range(4):
        copies[j].wait()
        rows = slice(j * cut, (j + 1) * cut)
        out_ref[...] += jnp.dot(mine_ref[:, rows], own_ref[rows, :], preferred_element_type=F32)
    for copy in copies[4:]:
        copy.wait()


def dispatch_kernel(other_ref, w_ref, acc_ref, gain_ref, g_ref, normed_ref, out_ref):
    values = acc_ref[...] + jnp.dot(other_ref[...], w_ref[...], preferred_element_type=F32)
    normed = layer_norm(values, gain_ref[...]).astype(BF16)
    normed_ref[...] = normed

    def put(i, _):
        at = pl.ds(pl.multiple_of(i * BLOCK, BLOCK), BLOCK)
        out_ref[at, :] = jnp.dot(
            g_ref[at, :], normed_ref[...], preferred_element_type=F32
        ).astype(BF16)
        return 0

    lax.fori_loop(0, out_ref.shape[0] // BLOCK, put, 0)


def hidden_of(x, gate, up):
    return (
        jax.nn.silu(jnp.dot(x, gate, preferred_element_type=F32))
        * jnp.dot(x, up, preferred_element_type=F32)
    ).astype(BF16)


def shared_kernel(x_ref, gate_ref, up_ref, down_ref, out_ref):
    x = x_ref[...]
    hidden = hidden_of(x, gate_ref[...], up_ref[...])
    out_ref[...] = ALPHA * x.astype(F32) + jnp.dot(
        hidden, down_ref[...], preferred_element_type=F32
    )


def expert_kernel(x_ref, gate_ref, up_ref, down_ref, out_ref):
    def step(i, _):
        rows = pl.ds(pl.multiple_of(i * BLOCK, BLOCK), BLOCK)
        hidden = hidden_of(x_ref[rows, :], gate_ref[0], up_ref[0])
        out_ref[rows, :] = jnp.dot(hidden, down_ref[0], preferred_element_type=F32).astype(BF16)
        return 0

    lax.fori_loop(0, x_ref.shape[0] // BLOCK, step, 0)


def finish_kernel(base_ref, c_ref, back_ref, gain_ref, out_ref, acc):
    rows = base_ref.shape[0]
    width = 512
    for j in range(base_ref.shape[1] // width):
        cols = slice(j * width, (j + 1) * width)
        part = jnp.dot(c_ref[...], back_ref[:, cols], preferred_element_type=F32)
        acc[:, cols] = base_ref[:, cols] + part[:rows] + part[rows:]
    out_ref[...] = layer_norm(acc[...], gain_ref[...]).astype(BF16)


def on_device(
    gate_pre, conv_in, conv_taps, recur_map, input_map, rate_logit, decay_shift, out_weight,
    residual, gain_mix, routes, route_weight, shared_gate, shared_up, shared_down, expert_gate,
    expert_up, expert_down, gain_out,
):
    tokens, channels = conv_in.shape
    reach = conv_taps.shape[0] - 1
    sp, tp = lax.axis_size("sp"), lax.axis_size("tp")
    experts = sp * tp
    rows = tokens // tp
    model = out_weight.shape[1]
    slots = experts * CAP
    sem = pltpu.SemaphoreType.DMA
    index = jnp.stack([lax.axis_index("sp"), lax.axis_index("tp")]).astype(jnp.int32)
    before = lax.ppermute(conv_in[tokens - reach :], "sp", [(i, i + 1) for i in range(sp - 1)])
    before, index = lax.optimization_barrier((before, index))
    pair = shape((2, tokens, channels), F32)
    big = pltpu.VMEM((tokens, channels), F32)
    apart = tokens + 8 * LANES
    lanes = pltpu.VMEM((channels // 128, apart, 128), F32)

    def staged(kernel, first, operands, made, flops, scratch, name):
        held = [pltpu.VMEM(x.shape, x.dtype) for x in tuple(operands) + made]
        return call(
            kernel,
            made,
            [VMEM] * len(first) + [HBM] * len(operands),
            flops,
            held + scratch,
            name=name,
            out_specs=(HBM,) * len(made),
            limit=62,
        )(*first, *operands)

    totals, local, edge = staged(
        scan_kernel,
        (before,),
        (conv_in, conv_taps, recur_map, input_map, rate_logit[None], decay_shift.T),
        (shape((sp, 2, channels), F32), pair, shape((2, LANES, channels), F32)),
        10**9,
        [lanes, big, big, big, pltpu.VMEM((apart, 128), F32), sem((6,)), sem((6,))],
        "scan",
    )
    seen = lax.all_to_all(totals, "sp", 0, 0, tiled=True)
    parts, g, c = staged(
        side_kernel,
        (),
        (gate_pre, routes.T, route_weight.T, local, edge),
        (pair, shape((slots, rows), BF16), shape((2 * rows, slots), BF16)),
        10**10,
        [lanes, lanes, sem((5,)), sem((3,))],
        "side",
    )
    piece = shape((rows, channels), BF16)
    mine, theirs = call(
        mix_kernel, (piece, piece), [SMEM, VMEM, VMEM], 10**8, name="mix", limit=8
    )(index, seen, parts)
    other = lax.ppermute(theirs, "tp", [(0, 1), (1, 0)])
    wide = shape((rows, model), F32)
    strip = (channels, model)
    acc, weight = call(
        project_kernel,
        (wide, shape(strip, BF16)),
        [SMEM, VMEM, VMEM, HBM],
        10**9,
        [pltpu.VMEM(strip, BF16), sem((8,))],
        name="project",
        limit=46,
    )(index, mine, residual, out_weight)
    normed, outgoing = call(
        dispatch_kernel,
        (shape((rows, model), BF16), shape((slots, model), BF16)),
        [VMEM] * 5,
        2 * 10**9,
        name="dispatch",
    )(other, weight, acc, gain_mix[None], g)

    def exchanged(x):
        x = x.reshape(experts, CAP, model)
        x = lax.all_to_all(x, ("sp", "tp"), split_axis=0, concat_axis=0, tiled=True)
        return x.reshape(slots, model)

    received = exchanged(outgoing)
    results = call(
        expert_kernel, shape((slots, model), BF16), [VMEM] * 4, 6 * 10**9, name="expert"
    )(received, expert_gate, expert_up, expert_down)
    normed, results = lax.optimization_barrier((normed, results))
    base = call(shared_kernel, wide, [VMEM] * 4, 10**10, name="shared")(
        normed, shared_gate, shared_up, shared_down
    )
    base, results = lax.optimization_barrier((base, results))
    back = exchanged(results)
    return call(
        finish_kernel,
        shape((rows, model), BF16),
        [VMEM] * 4,
        10**9,
        [pltpu.VMEM((rows, model), F32)],
        name="finish",
    )(base, c, back, gain_out[None])


def solution(mesh):
    return jax.shard_map(
        on_device,
        mesh=mesh,
        in_specs=(
            P("sp", "tp"),
            P("sp", "tp"),
            P(None, "tp"),
            P("tp", None, None),
            P("tp", None, None),
            P("tp"),
            P("sp", "tp"),
            P(),
            P(("sp", "tp"), None),
            P(),
            P(("sp", "tp"), None),
            P(("sp", "tp"), None),
            P(),
            P(),
            P(),
            P(("sp", "tp"), None, None),
            P(("sp", "tp"), None, None),
            P(("sp", "tp"), None, None),
            P(),
        ),
        out_specs=P(("sp", "tp"), None),
        check_vma=False,
    )
```

time: 180 us -> 172 us (0.956)
  blocking collectives: 136 us -> 113 us
  starting transfers between devices: 7.05 us -> 18.7 us
  waiting for transfers between devices: 0.7 us -> 7.24 us
  local copies, waits for them, and re-layouts: 7.21 us -> 2.97 us
    all_to_all x1 -> x0, blocking collectives: 23 us -> none  [on_device(): seen = lax.all_to_all(totals, 'sp', 0, 0, tiled=True)]
    all_to_all x0 -> x1, starting transfers between devices: none -> 11.6 us  [on_device(): seen = lax.all_to_all(totals, 'sp', 0, 0, tiled=True)]
    all_to_all x0 -> x1, waiting for transfers between devices: none -> 6.54 us  [on_device(): seen = lax.all_to_all(totals, 'sp', 0, 0, tiled=True)]
    unnamed x30 -> x26, local copies, waits for them, and re-layouts: 6.49 us -> 2.25 us
    pallas_call x5 -> x6, Pallas kernels: 23.2 us -> 25.3 us  [the longest x2 10.8 us: staged(): call(kernel, made, [VMEM] * len(first) + [HBM] * len(operands), flops, he...]
  transfers between devices with their start and end apart: 2 -> 3, of which waited for: 1 -> 2; matrix products, arithmetic and copies ran while one was open for 0% -> 0% of each run, Pallas kernels for 1% -> 5%
where the time goes in v3:
time: 172 us
  blocking collectives  113 us (66%)
  Pallas kernels  29.1 us (17%)
  starting transfers between devices  18.7 us (11%)
  waiting for transfers between devices  7.24 us (4%)
  local copies, waits for them, and re-layouts  2.97 us (2%)
    all_to_all x2, blocking collectives, exchanged(): x = lax.all_to_all(x, ('sp', 'tp'), split_axis=0, concat_axis=0, tiled=True)  113 us
    all_to_all x1, starting transfers between devices, on_device(): seen = lax.all_to_all(totals, 'sp', 0, 0, tiled=True)  11.6 us
    pallas_call x2, Pallas kernels, staged(): call(kernel, made, [VMEM] * len(first) + [HBM] * len(operands), flops, he...  10.8 us
    pallas_call x1, Pallas kernels, on_device(): call(expert_kernel, shape((slots, model), BF16), [VMEM] * 4, 6 * 10 ** 9,...  7.5 us
    all_to_all x1, waiting for transfers between devices, on_device(): seen = lax.all_to_all(totals, 'sp', 0, 0, tiled=True)  6.54 us
    pallas_call x1, Pallas kernels, on_device(): call(project_kernel, (wide, shape(strip, BF16)), [SMEM, VMEM, VMEM, HBM],...  4.02 us
    ppermute x1, starting transfers between devices, on_device(): lax.ppermute(conv_in[tokens - reach:], 'sp', [(i, i + 1) for i in range(s...  3.92 us
  transfers between devices with their start and end apart: 3, of which 2 were waited for; matrix products, arithmetic and copies ran while one was open for 0% of the time, Pallas kernels for 5%

profile of v3, /device:TPU:1, one launch (start us, length us, event | category | flops | bytes accessed | tf_op | source)
XLA Modules:
  0.0 171.7 jit_solution(14636736331873847277)
XLA Ops:
  0.0 0.7 slice.3
  0.7 3.9 %collective-permute-start = (bf16[3,1024]{1,0:T(4,128)(2,1)S(1)}, bf16[3,1024]{1,0:T(4,128)(2,1)S(1)}, u32[]{:S(2)}, u32[]{:S(2)}) collective-permute-start(bf16[3,1024]{1,0:T(4,128)(2,1)S(1)} %slice.3), channel_id=1, source_target_pairs={{0,2},{2,4},{4,6},{6,8},{8,10},{10,12},{12,14},{14,16},{16,18},{18... | collective-permute-start | bytes 18440 | tf_op jit(solution)/shard_map/ppermute | solution.py:395
  4.7 0.1 pad_add_fusion.index_ref
  4.7 0.7 collective-permute-done.halo_ref
  5.4 0.0 copy-start.12
  5.4 0.6 copy-done.12
  6.0 6.1 %scan.1 = (f32[64,2,1024]{2,1,0:T(2,128)}, f32[2,256,1024]{2,1,0:T(8,128)}, f32[2,8,1024]{2,1,0:T(8,128)}) custom-call(bf16[3,1024]{1,0:T(4,128)(2,1)} %copy-done.12, bf16[256,1024]{1,0:T(8,128)(2,1)} %x_hbm.1, bf16[4,1024]{1,0:T(4,128)(2,1)} %taps_hbm.1, bf16[4,256,256]{2,1,0:T(8,128)(2,1)} %rmap_hbm.1, bf16[4,256,256]{2,1,0:T(8,128)(2,1)} %imap_hbm.1, ...), custom_call_target="tpu_custom_call" | custom-call | flops 1000000000 | bytes 1048576 | tf_op jit(solution)/shard_map/scan/pallas_call | solution.py:404
  12.1 11.6 %all-to-all-start = ((f32[64,2,1024]{2,1,0:T(2,128)}), f32[64,2,1024]{2,1,0:T(2,128)S(1)}, u32[]{:S(2)}, u32[]{:S(2)}) async-start(f32[64,2,1024]{2,1,0:T(2,128)} %get-tuple-element.25), calls=%async_computation | async-start | bytes 1048576 | tf_op jit(solution)/shard_map/all_to_all | solution.py:424
  23.8 0.0 copy-start.1
  23.8 4.7 %side.1 = (f32[2,256,1024]{2,1,0:T(8,128)}, bf16[1024,128]{1,0:T(8,128)(2,1)}, bf16[256,1024]{1,0:T(8,128)(2,1)}) custom-call(bf16[256,1024]{1,0:T(8,128)(2,1)} %gate_hbm.1, s32[4,128]{1,0:T(4,128)} %bitcast.20, f32[4,128]{1,0:T(4,128)} %bitcast.21, f32[2,256,1024]{2,1,0:T(8,128)} %get-tuple-element.26.run_hbm, f32[2,8,1024]{2,1,0:T(8,128)} %get-tuple-element.27.edge_hbm), custom_call_target="tpu_custom_call" | custom-call | flops 10000000000 | bytes 1048576 | tf_op jit(solution)/shard_map/side/pallas_call | solution.py:404
  28.5 6.5 %all-to-all-done.seen_ref = f32[64,2,1024]{2,1,0:T(2,128)S(1)} async-done(((f32[64,2,1024]{2,1,0:T(2,128)}), f32[64,2,1024]{2,1,0:T(2,128)S(1)}, u32[]{:S(2)}, u32[]{:S(2)}) %all-to-all-start) | async-done | bytes 524320 | tf_op jit(solution)/shard_map/all_to_all | solution.py:424
  35.1 0.0 copy-start
  35.1 1.6 copy-done
  36.7 0.7 mix.1
  37.3 3.1 %collective-permute-start.1 = (bf16[128,1024]{1,0:T(8,128)(2,1)S(1)}, bf16[128,1024]{1,0:T(8,128)(2,1)S(1)}, u32[]{:S(2)}, u32[]{:S(2)}) collective-permute-start(bf16[128,1024]{1,0:T(8,128)(2,1)S(1)} %get-tuple-element.29), channel_id=1, source_target_pairs={{0,1},{1,0},{2,3},{3,2},{4,5},{5,4},{6,7},{7,6},{8,9},{9,8},{10,11... | collective-permute-start | bytes 786440 | tf_op jit(solution)/shard_map/ppermute | solution.py:438
  40.5 0.0 copy-done.1
  40.5 0.0 copy-start.10
  40.5 0.0 copy-start.11
  40.5 4.0 %project.1 = (f32[128,2048]{1,0:T(8,128)S(1)}, bf16[1024,2048]{1,0:T(8,128)(2,1)S(1)}) custom-call(s32[2]{0:T(128)S(1)} %pad_add_fusion.index_ref, bf16[128,1024]{1,0:T(8,128)(2,1)S(1)} %get-tuple-element.30.mine_ref, bf16[128,2048]{1,0:T(8,128)(2,1)S(1)} %copy-done.1, bf16[2048,2048]{1,0:T(8,128)(2,1)} %w_hbm.1), custom_call_target="tpu_custom_call" | custom-call | flops 1000000000 | bytes 1048576 | tf_op jit(solution)/shard_map/project/pallas_call | solution.py:441
  44.5 0.0 collective-permute-done.1.other_ref
  44.5 0.0 copy-done.10
  44.5 0.0 copy-done.11
  44.5 2.7 %dispatch.1 = (bf16[128,2048]{1,0:T(8,128)(2,1)S(1)}, bf16[1024,2048]{1,0:T(8,128)(2,1)S(1)}) custom-call(bf16[128,1024]{1,0:T(8,128)(2,1)S(1)} %collective-permute-done.1.other_ref, bf16[1024,2048]{1,0:T(8,128)(2,1)S(1)} %get-tuple-element.31.w_ref, f32[128,2048]{1,0:T(8,128)S(1)} %get-tuple-element.32.acc_ref, f32[1,2048]{1,0:T(1,128)S(1)} %bitcast.17, ...), custom_call_target="tpu_custom_call" | custom-call | flops 2000000000 | bytes 1048576 | tf_op jit(solution)/shard_map/dispatch/pallas_call | solution.py:450
  47.2 0.0 copy-start.4
  47.2 0.0 copy-start.5
  47.3 0.0 copy-start.6
  47.3 56.4 %all_to_all.15 = bf16[128,8,2048]{2,1,0:T(8,128)(2,1)S(1)} all-to-all(bf16[128,8,2048]{2,1,0:T(8,128)(2,1)S(1)} %bitcast.13), channel_id=1, replica_groups=mesh['sp'=64,'tp'=2] {'sp','tp'}, dimensions={0} | all-to-all | bytes 8388608 | tf_op jit(solution)/shard_map/all_to_all | solution.py:460
  103.7 0.0 copy-done.4
  103.7 0.0 copy-done.5
  103.7 0.0 copy-done.6
  103.7 0.0 copy-start.7
  103.7 0.0 copy-start.8
  103.7 0.0 copy-start.9
  103.7 7.5 %expert.1 = bf16[1024,2048]{1,0:T(8,128)(2,1)S(1)} custom-call(bf16[1024,2048]{1,0:T(8,128)(2,1)S(1)} %bitcast.15, bf16[1,2048,512]{2,1,0:T(8,128)(2,1)S(1)} %copy-done.4, bf16[1,2048,512]{2,1,0:T(8,128)(2,1)S(1)} %copy-done.5, bf16[1,512,2048]{2,1,0:T(8,128)(2,1)S(1)} %copy-done.6), custom_call_target="tpu_custom_call" | custom-call | flops 6000000000 | bytes 1048576 | tf_op jit(solution)/shard_map/expert/pallas_call | solution.py:464
  111.2 0.0 copy-done.7
  111.2 0.0 copy-done.8
  111.2 0.0 copy-done.9
  111.2 1.1 shared.1.base_ref
  112.3 0.0 copy-start.2
  112.4 0.0 copy-start.3
  112.4 57.0 %all_to_all.16 = bf16[128,8,2048]{2,1,0:T(8,128)(2,1)S(1)} all-to-all(bf16[128,8,2048]{2,1,0:T(8,128)(2,1)S(1)} %bitcast.14), channel_id=1, replica_groups=mesh['sp'=64,'tp'=2] {'sp','tp'}, dimensions={0} | all-to-all | bytes 8388608 | tf_op jit(solution)/shard_map/all_to_all | solution.py:460
  169.4 0.0 copy-done.2
  169.4 0.0 copy-done.3
  169.4 2.3 %finish.1 = bf16[128,2048]{1,0:T(8,128)(2,1)} custom-call(f32[128,2048]{1,0:T(8,128)S(1)} %shared.1.base_ref, bf16[256,1024]{1,0:T(8,128)(2,1)S(1)} %copy-done.2, bf16[1024,2048]{1,0:T(8,128)(2,1)S(1)} %bitcast.12, f32[1,2048]{1,0:T(1,128)S(1)} %bitcast.16), custom_call_target="tpu_custom_call" | custom-call | flops 1000000000 | bytes 1048576 | tf_op jit(solution)/shard_map/finish/pallas_call | solution.py:473
Async XLA Ops:
  0.7 4.7 %collective-permute-start = (bf16[3,1024]{1,0:T(4,128)(2,1)S(1)}, bf16[3,1024]{1,0:T(4,128)(2,1)S(1)}, u32[]{:S(2)}, u32[]{:S(2)}) collective-permute-start(bf16[3,1024]{1,0:T(4,128)(2,1)S(1)} %slice.3), channel_id=1, source_target_pairs={{0,2},{2,4},{4,6},{6,8},{8,10},{10,12},{12,14},{14,16},{16,18},{18... | collective-permute-start | bytes 18440 | tf_op jit(solution)/shard_map/ppermute | solution.py:395
  5.4 0.6 copy-start.12
  12.1 22.9 %all-to-all-start = ((f32[64,2,1024]{2,1,0:T(2,128)}), f32[64,2,1024]{2,1,0:T(2,128)S(1)}, u32[]{:S(2)}, u32[]{:S(2)}) async-start(f32[64,2,1024]{2,1,0:T(2,128)} %get-tuple-element.25), calls=%async_computation | async-start | bytes 1048576 | tf_op jit(solution)/shard_map/all_to_all | solution.py:424
  23.8 16.7 %copy-start.1 = (bf16[128,2048]{1,0:T(8,128)(2,1)S(1)}, bf16[128,2048]{1,0:T(8,128)(2,1)}, u32[]{:S(2)}) copy-start(bf16[128,2048]{1,0:T(8,128)(2,1)} %res_ref.1) | copy-start | bytes 1572868
  35.1 1.6 copy-start
  37.3 7.2 %collective-permute-start.1 = (bf16[128,1024]{1,0:T(8,128)(2,1)S(1)}, bf16[128,1024]{1,0:T(8,128)(2,1)S(1)}, u32[]{:S(2)}, u32[]{:S(2)}) collective-permute-start(bf16[128,1024]{1,0:T(8,128)(2,1)S(1)} %get-tuple-element.29), channel_id=1, source_target_pairs={{0,1},{1,0},{2,3},{3,2},{4,5},{5,4},{6,7},{7,6},{8,9},{9,8},{10,11... | collective-permute-start | bytes 786440 | tf_op jit(solution)/shard_map/ppermute | solution.py:438
  40.5 4.0 %copy-start.10 = (f32[2048]{0:T(1024)S(1)}, f32[2048]{0:T(1024)}, u32[]{:S(2)}) copy-start(f32[2048]{0:T(1024)} %param.28) | copy-start | bytes 24580
  40.5 4.1 %copy-start.11 = (bf16[1024,128]{1,0:T(8,128)(2,1)S(1)}, bf16[1024,128]{1,0:T(8,128)(2,1)}, u32[]{:S(2)}) copy-start(bf16[1024,128]{1,0:T(8,128)(2,1)} %get-tuple-element.33.g_ref) | copy-start | bytes 786436
  47.2 56.4 %copy-start.4 = (bf16[1,2048,512]{2,1,0:T(8,128)(2,1)S(1)}, bf16[1,2048,512]{2,1,0:T(8,128)(2,1)}, u32[]{:S(2)}) copy-start(bf16[1,2048,512]{2,1,0:T(8,128)(2,1)} %gate_ref.2) | copy-start | bytes 6291460
  47.2 56.4 %copy-start.5 = (bf16[1,2048,512]{2,1,0:T(8,128)(2,1)S(1)}, bf16[1,2048,512]{2,1,0:T(8,128)(2,1)}, u32[]{:S(2)}) copy-start(bf16[1,2048,512]{2,1,0:T(8,128)(2,1)} %up_ref.2) | copy-start | bytes 6291460
  47.3 56.4 %copy-start.6 = (bf16[1,512,2048]{2,1,0:T(8,128)(2,1)S(1)}, bf16[1,512,2048]{2,1,0:T(8,128)(2,1)}, u32[]{:S(2)}) copy-start(bf16[1,512,2048]{2,1,0:T(8,128)(2,1)} %down_ref.2) | copy-start | bytes 6291460
  103.7 7.5 %copy-start.7 = (bf16[2048,512]{1,0:T(8,128)(2,1)S(1)}, bf16[2048,512]{1,0:T(8,128)(2,1)}, u32[]{:S(2)}) copy-start(bf16[2048,512]{1,0:T(8,128)(2,1)} %gate_ref.3) | copy-start | bytes 6291460
  103.7 7.5 %copy-start.8 = (bf16[2048,512]{1,0:T(8,128)(2,1)S(1)}, bf16[2048,512]{1,0:T(8,128)(2,1)}, u32[]{:S(2)}) copy-start(bf16[2048,512]{1,0:T(8,128)(2,1)} %up_ref.3) | copy-start | bytes 6291460
  103.7 7.5 %copy-start.9 = (bf16[512,2048]{1,0:T(8,128)(2,1)S(1)}, bf16[512,2048]{1,0:T(8,128)(2,1)}, u32[]{:S(2)}) copy-start(bf16[512,2048]{1,0:T(8,128)(2,1)} %down_ref.3) | copy-start | bytes 6291460
  112.3 57.0 %copy-start.2 = (bf16[256,1024]{1,0:T(8,128)(2,1)S(1)}, bf16[256,1024]{1,0:T(8,128)(2,1)}, u32[]{:S(2)}) copy-start(bf16[256,1024]{1,0:T(8,128)(2,1)} %get-tuple-element.39.c_ref) | copy-start | bytes 1572868
  112.4 57.0 %copy-start.3 = (f32[2048]{0:T(1024)S(1)}, f32[2048]{0:T(1024)}, u32[]{:S(2)}) copy-start(f32[2048]{0:T(1024)} %param.37) | copy-start | bytes 24580

commit v4 on v3

--- a/solution.py
+++ b/solution.py
@@ -151,8 +151,10 @@
             )
             h = decay * h + update
             run = decay * run
-            run_ref[0, rows, cols] = h
-            run_ref[1, rows, cols] = run
+            for j in range(width // 128):
+                lane = slice(j * 128, (j + 1) * 128)
+                run_ref[0, k * (width // 128) + j, rows, :] = h[:, lane]
+                run_ref[1, k * (width // 128) + j, rows, :] = run[:, lane]
             out.append((h, run))
         return tuple(out)
 
@@ -164,10 +166,13 @@
         span = steps // 4
         last = lax.fori_loop(part * span, (part + 1) * span, step, last, unroll=2)
         rows = pl.ds(part * span * LANES, span * LANES)
-        copy = pltpu.make_async_copy(run_ref.at[:, rows, :], run_hbm.at[:, rows, :], outs.at[part])
+        copy = pltpu.make_async_copy(
+            run_ref.at[:, :, rows, :], run_hbm.at[:, :, rows, :], outs.at[part]
+        )
         copy.start()
         sent.append(copy)
     row = lax.broadcasted_iota(jnp.int32, (LANES, width), 0)
+    ends = [[], []]
     for k in range(heads):
         cols = slice(k * width, (k + 1) * width)
         h, a = last[k]
@@ -175,10 +180,15 @@
             hp, ap = pltpu.roll(h, d, 0), pltpu.roll(a, d, 0)
             h = jnp.where(row >= d, a * hp + h, h)
             a = jnp.where(row >= d, a * ap, a)
-        both = jnp.concatenate([a[LANES - 1 :], h[LANES - 1 :]], axis=0)
-        tot_ref[:, :, cols] = jnp.broadcast_to(both[None], (tot_ref.shape[0], 2, width))
+        for j in range(width // 128):
+            lane = slice(j * 128, (j + 1) * 128)
+            ends[0].append(jnp.log(jnp.maximum(a[LANES - 1 :, lane], TINY)))
+            ends[1].append(h[LANES - 1 :, lane])
         edge_ref[0, :, cols] = jnp.where(row >= 1, pltpu.roll(h, 1, 0), 0.0)
         edge_ref[1, :, cols] = jnp.where(row >= 1, pltpu.roll(a, 1, 0), 1.0)
+    both = jnp.concatenate(ends[0] + ends[1], axis=0).astype(BF16)
+    for i in range(tot_ref.shape[0]):
+        tot_ref[i] = both
     sent += [
         pltpu.make_async_copy(tot_ref, tot_hbm, outs.at[4]),
         pltpu.make_async_copy(edge_ref, edge_hbm, outs.at[5]),
@@ -191,7 +201,7 @@
 
 def side_kernel(
     gate_hbm, routes_hbm, weight_hbm, run_hbm, edge_hbm, mixed_hbm, g_hbm, c_hbm,
-    gate_ref, routes_ref, weight_ref, run_ref, edge_ref, mixed_ref, g_ref, c_ref, hs, rs, sems, outs,
+    gate_ref, routes_ref, weight_ref, run_ref, edge_ref, mixed_ref, g_ref, c_ref, sems, outs,
 ):
     copies = fetch(
         [
@@ -208,57 +218,55 @@
     route(routes_ref, weight_ref, g_ref, c_ref)
     for copy in copies[2:]:
         copy.wait()
-    _, tokens, channels = run_ref.shape
+    tokens, channels = gate_ref.shape
     steps = tokens // LANES
-    stride = steps + 8
-
-    def step(t, _):
-        rows = pl.ds(pl.multiple_of(t * LANES, LANES), LANES)
-        run = run_ref[1, rows, :]
-        own = run_ref[0, rows, :] + run * edge_ref[0]
-        run = run * edge_ref[1]
-        for c in range(hs.shape[0]):
-            cols = slice(c * 128, (c + 1) * 128)
-            hs[c, pl.ds(t, LANES, stride=stride), :] = own[:, cols]
-            rs[c, pl.ds(t, LANES, stride=stride), :] = run[:, cols]
-        return 0
-
-    lax.fori_loop(0, steps, step, 0, unroll=2)
     block = 16
+    per = steps // block
 
     def put(i, _):
         rows = pl.ds(pl.multiple_of(i * block, block), block)
-        per = steps // block
-        source = pl.ds(pl.multiple_of((i // per) * stride + (i % per) * block, 8), block)
+        chunk = i // per
+        source = pl.ds(chunk + (i % per) * (block * LANES), block, stride=LANES)
         gate = jax.nn.gelu(gate_ref[rows, :].astype(F32), approximate=True)
-        for c in range(hs.shape[0]):
+        enter, scale = edge_ref[0, pl.ds(chunk, 1), :], edge_ref[1, pl.ds(chunk, 1), :]
+        for c in range(channels // 128):
             cols = slice(c * 128, (c + 1) * 128)
-            mixed_ref[0, rows, cols] = hs[c, source, :] * gate[:, cols]
-            mixed_ref[1, rows, cols] = rs[c, source, :] * gate[:, cols]
+            run = run_ref[1, c, source, :]
+            mixed_ref[0, rows, cols] = (run_ref[0, c, source, :] + run * enter[:, cols]) * gate[:, cols]
+            mixed_ref[1, rows, cols] = run * scale[:, cols] * gate[:, cols]
         return 0
 
-    lax.fori_loop(0, tokens // block, put, 0)
-    sent = [
-        pltpu.make_async_copy(ref, hbm, outs.at[i])
-        for i, (ref, hbm) in enumerate(((mixed_ref, mixed_hbm), (g_ref, g_hbm), (c_ref, c_hbm)))
-    ]
-    for copy in sent:
+    pairs = [(g_ref, g_hbm), (c_ref, c_hbm)]
+    sent = fetch(pairs, outs)
+    quarter = tokens // 4
+    for part in range(4):
+        lax.fori_loop(part * quarter // block, (part + 1) * quarter // block, put, 0)
+        rows = pl.ds(part * quarter, quarter)
+        copy = pltpu.make_async_copy(
+            mixed_ref.at[:, rows, :], mixed_hbm.at[pl.ds(0, 2), rows, :], outs.at[2 + part]
+        )
         copy.start()
+        sent.append(copy)
     for copy in sent:
         copy.wait()
 
 
-def mix_kernel(index_ref, seen_ref, mixed_ref, mine_ref, theirs_ref):
+def mix_kernel(
+    index_ref, seen_ref, mixed_hbm, w_hbm, mine_ref, theirs_ref, w_ref, mixed_ref, sems
+):
     _, tokens, channels = mixed_ref.shape
     here, side = index_ref[0], index_ref[1]
-
-    def fold(i, c):
-        pair = seen_ref[i]
-        return pair[0:1] * c + pair[1:2]
-
-    carried = lax.fori_loop(0, here, fold, jnp.zeros((1, channels), F32))
+    depth = w_ref.shape[0]
+    own = pl.ds(pl.multiple_of(side * depth, depth), depth)
+    copies = fetch([(mixed_hbm.at[pl.ds(0, 2)], mixed_ref), (w_hbm.at[own, :], w_ref)], sems)
+    carried = jnp.zeros((LANES, 128), F32)
+    for i in range(seen_ref.shape[0]):
+        pair = seen_ref[i].astype(F32)
+        carried = jnp.where(i < here, jnp.exp(pair[:LANES]) * carried + pair[LANES:], carried)
+    carried = jnp.concatenate([carried[i : i + 1] for i in range(LANES)], axis=1)
     half = tokens // 2
     block = 16
+    copies[0].wait()
 
     def put(i, _):
         at = pl.multiple_of(i * block, block)
@@ -270,6 +278,7 @@
         return 0
 
     lax.fori_loop(0, half // block, put, 0, unroll=2)
+    copies[1].wait()
 
 
 def route(routes_ref, weight_ref, g_ref, c_ref):
@@ -309,23 +318,14 @@
         c_ref[rows:, cols] = jnp.transpose(jnp.where(chosen, to_slots(low), 0.0)).astype(BF16)
 
 
-def project_kernel(index_ref, mine_ref, res_ref, w_hbm, out_ref, rest_ref, own_ref, sems):
+def project_kernel(index_ref, mine_ref, res_ref, own_ref, w_hbm, out_ref, rest_ref, sems):
     depth = mine_ref.shape[1]
-    side = index_ref[1]
-    cut = depth // 4
-    pairs = []
-    for base, ref in ((side, own_ref), (1 - side, rest_ref)):
-        for j in range(4):
-            rows = pl.ds(pl.multiple_of(base * depth + j * cut, cut), cut)
-            pairs.append((w_hbm.at[rows, :], ref.at[pl.ds(j * cut, cut), :]))
-    copies = fetch(pairs, sems)
-    out_ref[...] = ALPHA * res_ref[...].astype(F32)
-    for j in range(4):
-        copies[j].wait()
-        rows = slice(j * cut, (j + 1) * cut)
-        out_ref[...] += jnp.dot(mine_ref[:, rows], own_ref[rows, :], preferred_element_type=F32)
-    for copy in copies[4:]:
-        copy.wait()
+    rest = pl.ds(pl.multiple_of((1 - index_ref[1]) * depth, depth), depth)
+    copies = fetch([(w_hbm.at[rest, :], rest_ref)], sems)
+    out_ref[...] = ALPHA * res_ref[...].astype(F32) + jnp.dot(
+        mine_ref[...], own_ref[...], preferred_element_type=F32
+    )
+    copies[0].wait()
 
 
 def dispatch_kernel(other_ref, w_ref, acc_ref, gain_ref, g_ref, normed_ref, out_ref):
@@ -333,14 +333,7 @@
     normed = layer_norm(values, gain_ref[...]).astype(BF16)
     normed_ref[...] = normed
 
-    def put(i, _):
-        at = pl.ds(pl.multiple_of(i * BLOCK, BLOCK), BLOCK)
-        out_ref[at, :] = jnp.dot(
-            g_ref[at, :], normed_ref[...], preferred_element_type=F32
-        ).astype(BF16)
-        return 0
-
-    lax.fori_loop(0, out_ref.shape[0] // BLOCK, put, 0)
+    out_ref[...] = jnp.dot(g_ref[...], normed, preferred_element_type=F32).astype(BF16)
 
 
 def hidden_of(x, gate, up):
@@ -359,13 +352,15 @@
 
 
 def expert_kernel(x_ref, gate_ref, up_ref, down_ref, out_ref):
+    block = 2 * BLOCK
+
     def step(i, _):
-        rows = pl.ds(pl.multiple_of(i * BLOCK, BLOCK), BLOCK)
+        rows = pl.ds(pl.multiple_of(i * block, block), block)
         hidden = hidden_of(x_ref[rows, :], gate_ref[0], up_ref[0])
         out_ref[rows, :] = jnp.dot(hidden, down_ref[0], preferred_element_type=F32).astype(BF16)
         return 0
 
-    lax.fori_loop(0, x_ref.shape[0] // BLOCK, step, 0)
+    lax.fori_loop(0, x_ref.shape[0] // block, step, 0)
 
 
 def finish_kernel(base_ref, c_ref, back_ref, gain_ref, out_ref, acc):
@@ -394,13 +389,16 @@
     index = jnp.stack([lax.axis_index("sp"), lax.axis_index("tp")]).astype(jnp.int32)
     before = lax.ppermute(conv_in[tokens - reach :], "sp", [(i, i + 1) for i in range(sp - 1)])
     before, index = lax.optimization_barrier((before, index))
-    pair = shape((2, tokens, channels), F32)
+    padded = shape((8, tokens, channels), F32)
     big = pltpu.VMEM((tokens, channels), F32)
     apart = tokens + 8 * LANES
     lanes = pltpu.VMEM((channels // 128, apart, 128), F32)
 
     def staged(kernel, first, operands, made, flops, scratch, name):
-        held = [pltpu.VMEM(x.shape, x.dtype) for x in tuple(operands) + made]
+        held = [
+            pltpu.VMEM((2,) + x.shape[1:] if x is padded else x.shape, x.dtype)
+            for x in tuple(operands) + made
+        ]
         return call(
             kernel,
             made,
@@ -416,7 +414,11 @@
         scan_kernel,
         (before,),
         (conv_in, conv_taps, recur_map, input_map, rate_logit[None], decay_shift.T),
-        (shape((sp, 2, channels), F32), pair, shape((2, LANES, channels), F32)),
+        (
+            shape((sp, 2 * LANES, 128), BF16),
+            shape((2, channels // 128, tokens, 128), F32),
+            shape((2, LANES, channels), F32),
+        ),
         10**9,
         [lanes, big, big, big, pltpu.VMEM((apart, 128), F32), sem((6,)), sem((6,))],
         "scan",
@@ -426,34 +428,41 @@
         side_kernel,
         (),
         (gate_pre, routes.T, route_weight.T, local, edge),
-        (pair, shape((slots, rows), BF16), shape((2 * rows, slots), BF16)),
+        (padded, shape((slots, rows), BF16), shape((2 * rows, slots), BF16)),
         10**10,
-        [lanes, lanes, sem((5,)), sem((3,))],
+        [sem((5,)), sem((6,))],
         "side",
     )
     piece = shape((rows, channels), BF16)
-    mine, theirs = call(
-        mix_kernel, (piece, piece), [SMEM, VMEM, VMEM], 10**8, name="mix", limit=8
-    )(index, seen, parts)
+    strip = shape((channels, model), BF16)
+    mine, theirs, own = call(
+        mix_kernel,
+        (piece, piece, strip),
+        [SMEM, VMEM, HBM, HBM],
+        10**8,
+        [pltpu.VMEM((2, tokens, channels), F32), sem((2,))],
+        name="mix",
+        limit=46,
+    )(index, seen, parts, out_weight)
     other = lax.ppermute(theirs, "tp", [(0, 1), (1, 0)])
     wide = shape((rows, model), F32)
-    strip = (channels, model)
-    acc, weight = call(
+    acc, rest = call(
         project_kernel,
-        (wide, shape(strip, BF16)),
-        [SMEM, VMEM, VMEM, HBM],
+        (wide, strip),
+        [SMEM, VMEM, VMEM, VMEM, HBM],
         10**9,
-        [pltpu.VMEM(strip, BF16), sem((8,))],
+        [sem((1,))],
         name="project",
-        limit=46,
-    )(index, mine, residual, out_weight)
+        limit=40,
+    )(index, mine, residual, own, out_weight)
     normed, outgoing = call(
         dispatch_kernel,
         (shape((rows, model), BF16), shape((slots, model), BF16)),
         [VMEM] * 5,
         2 * 10**9,
         name="dispatch",
-    )(other, weight, acc, gain_mix[None], g)
+        limit=24,
+    )(other, rest, acc, gain_mix[None], g)
 
     def exchanged(x):
         x = x.reshape(experts, CAP, model)
@@ -462,7 +471,7 @@
 
     received = exchanged(outgoing)
     results = call(
-        expert_kernel, shape((slots, model), BF16), [VMEM] * 4, 6 * 10**9, name="expert"
+        expert_kernel, shape((slots, model), BF16), [VMEM] * 4, 6 * 10**9, name="expert", limit=24
     )(received, expert_gate, expert_up, expert_down)
     normed, results = lax.optimization_barrier((normed, results))
     base = call(shared_kernel, wide, [VMEM] * 4, 10**10, name="shared")(

time: 172 us -> 170 us (0.988)
    pallas_call x2, Pallas kernels: 4.69 us -> 6.7 us  [the longest x1 3.38 us: on_device(): call(mix_kernel, (piece, piece, strip), [SMEM, VMEM, HBM, HBM], 10 ** 8,...]
  transfers between devices with their start and end apart: 3 -> 3, of which waited for: 2 -> 2; matrix products, arithmetic and copies ran while one was open for 0% -> 0% of each run, Pallas kernels for 5% -> 4%
where the time goes in v4:
time: 170 us; the launch traced here: 169 us
  blocking collectives  113 us (66%)
  Pallas kernels  28.8 us (17%)
  starting transfers between devices  18.9 us (11%)
  waiting for transfers between devices  6.63 us (4%)
    all_to_all x2, blocking collectives, exchanged(): x = lax.all_to_all(x, ('sp', 'tp'), split_axis=0, concat_axis=0, tiled=True)  113 us
    all_to_all x1, starting transfers between devices, on_device(): seen = lax.all_to_all(totals, 'sp', 0, 0, tiled=True)  11.6 us
    pallas_call x2, Pallas kernels, staged(): call(kernel, made, [VMEM] * len(first) + [HBM] * len(operands), flops, he...  9.6 us
    pallas_call x1, Pallas kernels, on_device(): call(expert_kernel, shape((slots, model), BF16), [VMEM] * 4, 6 * 10 ** 9,...  6.84 us
    all_to_all x1, waiting for transfers between devices, on_device(): seen = lax.all_to_all(totals, 'sp', 0, 0, tiled=True)  5.93 us
    ppermute x1, starting transfers between devices, on_device(): lax.ppermute(conv_in[tokens - reach:], 'sp', [(i, i + 1) for i in range(s...  3.92 us
  transfers between devices with their start and end apart: 3, of which 2 were waited for; matrix products, arithmetic and copies ran while one was open for 0% of the time, Pallas kernels for 4%

profile of v4, /device:TPU:1, one launch (start us, length us, event | category | flops | bytes accessed | tf_op | source)
XLA Modules:
  0.0 169.3 jit_solution(9291293660088070563)
XLA Ops:
  0.0 0.7 slice.3
  0.7 3.9 %collective-permute-start = (bf16[3,1024]{1,0:T(4,128)(2,1)S(1)}, bf16[3,1024]{1,0:T(4,128)(2,1)S(1)}, u32[]{:S(2)}, u32[]{:S(2)}) collective-permute-start(bf16[3,1024]{1,0:T(4,128)(2,1)S(1)} %slice.3), channel_id=1, source_target_pairs={{0,2},{2,4},{4,6},{6,8},{8,10},{10,12},{12,14},{14,16},{16,18},{18... | collective-permute-start | bytes 18440 | tf_op jit(solution)/shard_map/ppermute | solution.py:390
  4.7 0.1 pad_add_fusion.index_ref
  4.7 0.7 collective-permute-done.halo_ref
  5.4 0.0 copy-start.11
  5.4 0.6 copy-done.11
  6.0 6.1 %scan.1 = (bf16[64,16,128]{2,1,0:T(8,128)(2,1)}, f32[2,8,256,128]{3,2,1,0:T(8,128)}, f32[2,8,1024]{2,1,0:T(8,128)}) custom-call(bf16[3,1024]{1,0:T(4,128)(2,1)} %copy-done.11, bf16[256,1024]{1,0:T(8,128)(2,1)} %x_hbm.1, bf16[4,1024]{1,0:T(4,128)(2,1)} %taps_hbm.1, bf16[4,256,256]{2,1,0:T(8,128)(2,1)} %rmap_hbm.1, bf16[4,256,256]{2,1,0:T(8,128)(2,1)} %imap_hbm.1, ...), custom_call_target="tpu_custom_call" | custom-call | flops 1000000000 | bytes 1048576 | tf_op jit(solution)/shard_map/scan/pallas_call | solution.py:402
  12.1 11.6 %all-to-all-start = ((bf16[64,16,128]{2,1,0:T(8,128)(2,1)}), bf16[64,16,128]{2,1,0:T(8,128)(2,1)S(1)}, u32[]{:S(2)}, u32[]{:S(2)}) async-start(bf16[64,16,128]{2,1,0:T(8,128)(2,1)} %get-tuple-element.26), calls=%async_computation | async-start | bytes 524288 | tf_op jit(solution)/shard_map/all_to_all | solution.py:426
  23.8 3.5 %side.1 = (f32[8,256,1024]{2,1,0:T(8,128)}, bf16[1024,128]{1,0:T(8,128)(2,1)}, bf16[256,1024]{1,0:T(8,128)(2,1)}) custom-call(bf16[256,1024]{1,0:T(8,128)(2,1)} %gate_hbm.1, s32[4,128]{1,0:T(4,128)} %bitcast.20, f32[4,128]{1,0:T(4,128)} %bitcast.21, f32[2,8,256,128]{3,2,1,0:T(8,128)} %get-tuple-element.27.run_hbm, f32[2,8,1024]{2,1,0:T(8,128)} %get-tuple-element.28.edge_hbm), custom_call_target="tpu_custom_call" | custom-call | flops 10000000000 | bytes 1048576 | tf_op jit(solution)/shard_map/side/pallas_call | solution.py:402
  27.3 5.9 %all-to-all-done.seen_ref = bf16[64,16,128]{2,1,0:T(8,128)(2,1)S(1)} async-done(((bf16[64,16,128]{2,1,0:T(8,128)(2,1)}), bf16[64,16,128]{2,1,0:T(8,128)(2,1)S(1)}, u32[]{:S(2)}, u32[]{:S(2)}) %all-to-all-start) | async-done | bytes 262176 | tf_op jit(solution)/shard_map/all_to_all | solution.py:426
  33.2 0.0 copy-start.1
  33.2 3.4 %mix.1 = (bf16[128,1024]{1,0:T(8,128)(2,1)S(1)}, bf16[128,1024]{1,0:T(8,128)(2,1)S(1)}, bf16[1024,2048]{1,0:T(8,128)(2,1)S(1)}) custom-call(s32[2]{0:T(128)S(1)} %pad_add_fusion.index_ref, bf16[64,16,128]{2,1,0:T(8,128)(2,1)S(1)} %all-to-all-done.seen_ref, f32[8,256,1024]{2,1,0:T(8,128)} %get-tuple-element.29.mixed_hbm, bf16[2048,2048]{1,0:T(8,128)(2,1)} %w_hbm.3), custom_call_target="tpu_custom_call" | custom-call | flops 100000000 | bytes 1048576 | tf_op jit(solution)/shard_map/mix/pallas_call | solution.py:438
  36.6 3.3 %collective-permute-start.1 = (bf16[128,1024]{1,0:T(8,128)(2,1)S(1)}, bf16[128,1024]{1,0:T(8,128)(2,1)S(1)}, u32[]{:S(2)}, u32[]{:S(2)}) collective-permute-start(bf16[128,1024]{1,0:T(8,128)(2,1)S(1)} %get-tuple-element.30), channel_id=1, source_target_pairs={{0,1},{1,0},{2,3},{3,2},{4,5},{5,4},{6,7},{7,6},{8,9},{9,8},{10,11... | collective-permute-start | bytes 786440 | tf_op jit(solution)/shard_map/ppermute | solution.py:447
  39.9 0.0 copy-done.1
  39.9 0.0 copy-start.9
  39.9 0.0 copy-start.10
  39.9 3.3 %project.1 = (f32[128,2048]{1,0:T(8,128)S(1)}, bf16[1024,2048]{1,0:T(8,128)(2,1)S(1)}) custom-call(s32[2]{0:T(128)S(1)} %pad_add_fusion.index_ref, bf16[128,1024]{1,0:T(8,128)(2,1)S(1)} %get-tuple-element.31.mine_ref, bf16[128,2048]{1,0:T(8,128)(2,1)S(1)} %copy-done.1, bf16[1024,2048]{1,0:T(8,128)(2,1)S(1)} %get-tuple-element.32.own_ref, ...), custom_call_target="tpu_custom_call" | custom-call | flops 1000000000 | bytes 1048576 | tf_op jit(solution)/shard_map/project/pallas_call | solution.py:449
  43.3 0.0 collective-permute-done.1.other_ref
  43.3 0.0 copy-done.9
  43.3 0.0 copy-done.10
  43.3 2.2 %dispatch.1 = (bf16[128,2048]{1,0:T(8,128)(2,1)S(1)}, bf16[1024,2048]{1,0:T(8,128)(2,1)S(1)}) custom-call(bf16[128,1024]{1,0:T(8,128)(2,1)S(1)} %collective-permute-done.1.other_ref, bf16[1024,2048]{1,0:T(8,128)(2,1)S(1)} %get-tuple-element.33.w_ref, f32[128,2048]{1,0:T(8,128)S(1)} %get-tuple-element.34.acc_ref, f32[1,2048]{1,0:T(1,128)S(1)} %bitcast.17, ...), custom_call_target="tpu_custom_call" | custom-call | flops 2000000000 | bytes 1048576 | tf_op jit(solution)/shard_map/dispatch/pallas_call | solution.py:458
  45.5 0.0 copy-start.3
  45.5 0.0 copy-start.4
  45.6 0.0 copy-start.5
  45.6 56.3 %all_to_all.15 = bf16[128,8,2048]{2,1,0:T(8,128)(2,1)S(1)} all-to-all(bf16[128,8,2048]{2,1,0:T(8,128)(2,1)S(1)} %bitcast.13), channel_id=1, replica_groups=mesh['sp'=64,'tp'=2] {'sp','tp'}, dimensions={0} | all-to-all | bytes 8388608 | tf_op jit(solution)/shard_map/all_to_all | solution.py:469
  101.9 0.0 copy-done.3
  101.9 0.0 copy-done.4
  101.9 0.0 copy-done.5
  101.9 0.0 copy-start.6
  101.9 0.0 copy-start.7
  101.9 0.0 copy-start.8
  101.9 6.8 %expert.1 = bf16[1024,2048]{1,0:T(8,128)(2,1)S(1)} custom-call(bf16[1024,2048]{1,0:T(8,128)(2,1)S(1)} %bitcast.15, bf16[1,2048,512]{2,1,0:T(8,128)(2,1)S(1)} %copy-done.3, bf16[1,2048,512]{2,1,0:T(8,128)(2,1)S(1)} %copy-done.4, bf16[1,512,2048]{2,1,0:T(8,128)(2,1)S(1)} %copy-done.5), custom_call_target="tpu_custom_call" | custom-call | flops 6000000000 | bytes 1048576 | tf_op jit(solution)/shard_map/expert/pallas_call | solution.py:473
  108.8 0.0 copy-done.6
  108.8 0.0 copy-done.7
  108.8 0.0 copy-done.8
  108.8 1.1 shared.1.base_ref
  109.9 0.0 copy-start
  109.9 0.0 copy-start.2
  109.9 57.0 %all_to_all.16 = bf16[128,8,2048]{2,1,0:T(8,128)(2,1)S(1)} all-to-all(bf16[128,8,2048]{2,1,0:T(8,128)(2,1)S(1)} %bitcast.14), channel_id=1, replica_groups=mesh['sp'=64,'tp'=2] {'sp','tp'}, dimensions={0} | all-to-all | bytes 8388608 | tf_op jit(solution)/shard_map/all_to_all | solution.py:469
  166.9 0.0 copy-done
  166.9 0.0 copy-done.2
  166.9 2.3 %finish.1 = bf16[128,2048]{1,0:T(8,128)(2,1)} custom-call(f32[128,2048]{1,0:T(8,128)S(1)} %shared.1.base_ref, bf16[256,1024]{1,0:T(8,128)(2,1)S(1)} %copy-done, bf16[1024,2048]{1,0:T(8,128)(2,1)S(1)} %bitcast.12, f32[1,2048]{1,0:T(1,128)S(1)} %bitcast.16), custom_call_target="tpu_custom_call" | custom-call | flops 1000000000 | bytes 1048576 | tf_op jit(solution)/shard_map/finish/pallas_call | solution.py:482
Async XLA Ops:
  0.7 4.7 %collective-permute-start = (bf16[3,1024]{1,0:T(4,128)(2,1)S(1)}, bf16[3,1024]{1,0:T(4,128)(2,1)S(1)}, u32[]{:S(2)}, u32[]{:S(2)}) collective-permute-start(bf16[3,1024]{1,0:T(4,128)(2,1)S(1)} %slice.3), channel_id=1, source_target_pairs={{0,2},{2,4},{4,6},{6,8},{8,10},{10,12},{12,14},{14,16},{16,18},{18... | collective-permute-start | bytes 18440 | tf_op jit(solution)/shard_map/ppermute | solution.py:390
  5.4 0.6 copy-start.11
  12.1 21.1 %all-to-all-start = ((bf16[64,16,128]{2,1,0:T(8,128)(2,1)}), bf16[64,16,128]{2,1,0:T(8,128)(2,1)S(1)}, u32[]{:S(2)}, u32[]{:S(2)}) async-start(bf16[64,16,128]{2,1,0:T(8,128)(2,1)} %get-tuple-element.26), calls=%async_computation | async-start | bytes 524288 | tf_op jit(solution)/shard_map/all_to_all | solution.py:426
  33.2 6.7 %copy-start.1 = (bf16[128,2048]{1,0:T(8,128)(2,1)S(1)}, bf16[128,2048]{1,0:T(8,128)(2,1)}, u32[]{:S(2)}) copy-start(bf16[128,2048]{1,0:T(8,128)(2,1)} %res_ref.1) | copy-start | bytes 1572868
  36.6 6.7 %collective-permute-start.1 = (bf16[128,1024]{1,0:T(8,128)(2,1)S(1)}, bf16[128,1024]{1,0:T(8,128)(2,1)S(1)}, u32[]{:S(2)}, u32[]{:S(2)}) collective-permute-start(bf16[128,1024]{1,0:T(8,128)(2,1)S(1)} %get-tuple-element.30), channel_id=1, source_target_pairs={{0,1},{1,0},{2,3},{3,2},{4,5},{5,4},{6,7},{7,6},{8,9},{9,8},{10,11... | collective-permute-start | bytes 786440 | tf_op jit(solution)/shard_map/ppermute | solution.py:447
  39.9 3.3 %copy-start.9 = (f32[2048]{0:T(1024)S(1)}, f32[2048]{0:T(1024)}, u32[]{:S(2)}) copy-start(f32[2048]{0:T(1024)} %param.28) | copy-start | bytes 24580
  39.9 3.3 %copy-start.10 = (bf16[1024,128]{1,0:T(8,128)(2,1)S(1)}, bf16[1024,128]{1,0:T(8,128)(2,1)}, u32[]{:S(2)}) copy-start(bf16[1024,128]{1,0:T(8,128)(2,1)} %get-tuple-element.35.g_ref) | copy-start | bytes 786436
  45.5 56.3 %copy-start.3 = (bf16[1,2048,512]{2,1,0:T(8,128)(2,1)S(1)}, bf16[1,2048,512]{2,1,0:T(8,128)(2,1)}, u32[]{:S(2)}) copy-start(bf16[1,2048,512]{2,1,0:T(8,128)(2,1)} %gate_ref.2) | copy-start | bytes 6291460
  45.5 56.3 %copy-start.4 = (bf16[1,2048,512]{2,1,0:T(8,128)(2,1)S(1)}, bf16[1,2048,512]{2,1,0:T(8,128)(2,1)}, u32[]{:S(2)}) copy-start(bf16[1,2048,512]{2,1,0:T(8,128)(2,1)} %up_ref.2) | copy-start | bytes 6291460
  45.6 56.3 %copy-start.5 = (bf16[1,512,2048]{2,1,0:T(8,128)(2,1)S(1)}, bf16[1,512,2048]{2,1,0:T(8,128)(2,1)}, u32[]{:S(2)}) copy-start(bf16[1,512,2048]{2,1,0:T(8,128)(2,1)} %down_ref.2) | copy-start | bytes 6291460
  101.9 6.9 %copy-start.6 = (bf16[2048,512]{1,0:T(8,128)(2,1)S(1)}, bf16[2048,512]{1,0:T(8,128)(2,1)}, u32[]{:S(2)}) copy-start(bf16[2048,512]{1,0:T(8,128)(2,1)} %gate_ref.3) | copy-start | bytes 6291460
  101.9 6.9 %copy-start.7 = (bf16[2048,512]{1,0:T(8,128)(2,1)S(1)}, bf16[2048,512]{1,0:T(8,128)(2,1)}, u32[]{:S(2)}) copy-start(bf16[2048,512]{1,0:T(8,128)(2,1)} %up_ref.3) | copy-start | bytes 6291460
  101.9 6.9 %copy-start.8 = (bf16[512,2048]{1,0:T(8,128)(2,1)S(1)}, bf16[512,2048]{1,0:T(8,128)(2,1)}, u32[]{:S(2)}) copy-start(bf16[512,2048]{1,0:T(8,128)(2,1)} %down_ref.3) | copy-start | bytes 6291460
  109.9 57.0 %copy-start = (bf16[256,1024]{1,0:T(8,128)(2,1)S(1)}, bf16[256,1024]{1,0:T(8,128)(2,1)}, u32[]{:S(2)}) copy-start(bf16[256,1024]{1,0:T(8,128)(2,1)} %get-tuple-element.41.c_ref) | copy-start | bytes 1572868
  109.9 57.0 %copy-start.2 = (f32[2048]{0:T(1024)S(1)}, f32[2048]{0:T(1024)}, u32[]{:S(2)}) copy-start(f32[2048]{0:T(1024)} %param.37) | copy-start | bytes 24580

commit v5 on v4

--- a/solution.py
+++ b/solution.py
@@ -13,6 +13,7 @@
 TINY = 1e-36
 CAP = 8
 BLOCK = 256
+PIECES = 8
 LANES = 8
 F32 = jnp.float32
 BF16 = jnp.bfloat16
@@ -257,8 +258,15 @@
     _, tokens, channels = mixed_ref.shape
     here, side = index_ref[0], index_ref[1]
     depth = w_ref.shape[0]
-    own = pl.ds(pl.multiple_of(side * depth, depth), depth)
-    copies = fetch([(mixed_hbm.at[pl.ds(0, 2)], mixed_ref), (w_hbm.at[own, :], w_ref)], sems)
+    cut = depth // PIECES
+    pairs = []
+    for j in range(4):
+        rows = pl.ds(j * (tokens // 4), tokens // 4)
+        pairs.append((mixed_hbm.at[pl.ds(0, 2), rows, :], mixed_ref.at[:, rows, :]))
+    for j in range(PIECES):
+        rows = pl.ds(pl.multiple_of(side * depth + j * cut, cut), cut)
+        pairs.append((w_hbm.at[rows, :], w_ref.at[pl.ds(j * cut, cut), :]))
+    copies = fetch(pairs, sems)
     carried = jnp.zeros((LANES, 128), F32)
     for i in range(seen_ref.shape[0]):
         pair = seen_ref[i].astype(F32)
@@ -266,7 +274,8 @@
     carried = jnp.concatenate([carried[i : i + 1] for i in range(LANES)], axis=1)
     half = tokens // 2
     block = 16
-    copies[0].wait()
+    for copy in copies[:4]:
+        copy.wait()
 
     def put(i, _):
         at = pl.multiple_of(i * block, block)
@@ -278,7 +287,8 @@
         return 0
 
     lax.fori_loop(0, half // block, put, 0, unroll=2)
-    copies[1].wait()
+    for copy in copies[4:]:
+        copy.wait()
 
 
 def route(routes_ref, weight_ref, g_ref, c_ref):
@@ -320,12 +330,17 @@
 
 def project_kernel(index_ref, mine_ref, res_ref, own_ref, w_hbm, out_ref, rest_ref, sems):
     depth = mine_ref.shape[1]
-    rest = pl.ds(pl.multiple_of((1 - index_ref[1]) * depth, depth), depth)
-    copies = fetch([(w_hbm.at[rest, :], rest_ref)], sems)
+    cut = depth // PIECES
+    pairs = []
+    for j in range(PIECES):
+        rows = pl.ds(pl.multiple_of((1 - index_ref[1]) * depth + j * cut, cut), cut)
+        pairs.append((w_hbm.at[rows, :], rest_ref.at[pl.ds(j * cut, cut), :]))
+    copies = fetch(pairs, sems)
     out_ref[...] = ALPHA * res_ref[...].astype(F32) + jnp.dot(
         mine_ref[...], own_ref[...], preferred_element_type=F32
     )
-    copies[0].wait()
+    for copy in copies:
+        copy.wait()
 
 
 def dispatch_kernel(other_ref, w_ref, acc_ref, gain_ref, g_ref, normed_ref, out_ref):
@@ -440,7 +455,7 @@
         (piece, piece, strip),
         [SMEM, VMEM, HBM, HBM],
         10**8,
-        [pltpu.VMEM((2, tokens, channels), F32), sem((2,))],
+        [pltpu.VMEM((2, tokens, channels), F32), sem((4 + PIECES,))],
         name="mix",
         limit=46,
     )(index, seen, parts, out_weight)
@@ -451,7 +466,7 @@
         (wide, strip),
         [SMEM, VMEM, VMEM, VMEM, HBM],
         10**9,
-        [sem((1,))],
+        [sem((PIECES,))],
         name="project",
         limit=40,
     )(index, mine, residual, own, out_weight)

time: 170 us -> 170 us (level)
  no operation moved by 1% of the time
where the time goes in v5:
time: 170 us; the launch traced here: 169 us
  blocking collectives  113 us (66%)
  Pallas kernels  28.9 us (17%)
  starting transfers between devices  18.9 us (11%)
  waiting for transfers between devices  6.63 us (4%)
    all_to_all x2, blocking collectives, exchanged(): x = lax.all_to_all(x, ('sp', 'tp'), split_axis=0, concat_axis=0, tiled=True)  113 us
    all_to_all x1, starting transfers between devices, on_device(): seen = lax.all_to_all(totals, 'sp', 0, 0, tiled=True)  11.6 us
    pallas_call x2, Pallas kernels, staged(): call(kernel, made, [VMEM] * len(first) + [HBM] * len(operands), flops, he...  9.6 us
    pallas_call x1, Pallas kernels, on_device(): call(expert_kernel, shape((slots, model), BF16), [VMEM] * 4, 6 * 10 ** 9,...  6.84 us
    all_to_all x1, waiting for transfers between devices, on_device(): seen = lax.all_to_all(totals, 'sp', 0, 0, tiled=True)  5.93 us
    ppermute x1, starting transfers between devices, on_device(): lax.ppermute(conv_in[tokens - reach:], 'sp', [(i, i + 1) for i in range(s...  3.92 us
    pallas_call x1, Pallas kernels, on_device(): call(mix_kernel, (piece, piece, strip), [SMEM, VMEM, HBM, HBM], 10 ** 8,...  3.42 us
  transfers between devices with their start and end apart: 3, of which 2 were waited for; matrix products, arithmetic and copies ran while one was open for 0% of the time, Pallas kernels for 4%

profile of v5, /device:TPU:1, one launch (start us, length us, event | category | flops | bytes accessed | tf_op | source)
XLA Modules:
  0.0 169.3 jit_solution(8511374790871668478)
XLA Ops:
  0.0 0.7 slice.3
  0.7 3.9 %collective-permute-start = (bf16[3,1024]{1,0:T(4,128)(2,1)S(1)}, bf16[3,1024]{1,0:T(4,128)(2,1)S(1)}, u32[]{:S(2)}, u32[]{:S(2)}) collective-permute-start(bf16[3,1024]{1,0:T(4,128)(2,1)S(1)} %slice.3), channel_id=1, source_target_pairs={{0,2},{2,4},{4,6},{6,8},{8,10},{10,12},{12,14},{14,16},{16,18},{18... | collective-permute-start | bytes 18440 | tf_op jit(solution)/shard_map/ppermute | solution.py:405
  4.7 0.1 pad_add_fusion.index_ref
  4.7 0.7 collective-permute-done.halo_ref
  5.4 0.0 copy-start.11
  5.4 0.6 copy-done.11
  6.0 6.1 %scan.1 = (bf16[64,16,128]{2,1,0:T(8,128)(2,1)}, f32[2,8,256,128]{3,2,1,0:T(8,128)}, f32[2,8,1024]{2,1,0:T(8,128)}) custom-call(bf16[3,1024]{1,0:T(4,128)(2,1)} %copy-done.11, bf16[256,1024]{1,0:T(8,128)(2,1)} %x_hbm.1, bf16[4,1024]{1,0:T(4,128)(2,1)} %taps_hbm.1, bf16[4,256,256]{2,1,0:T(8,128)(2,1)} %rmap_hbm.1, bf16[4,256,256]{2,1,0:T(8,128)(2,1)} %imap_hbm.1, ...), custom_call_target="tpu_custom_call" | custom-call | flops 1000000000 | bytes 1048576 | tf_op jit(solution)/shard_map/scan/pallas_call | solution.py:417
  12.1 11.6 %all-to-all-start = ((bf16[64,16,128]{2,1,0:T(8,128)(2,1)}), bf16[64,16,128]{2,1,0:T(8,128)(2,1)S(1)}, u32[]{:S(2)}, u32[]{:S(2)}) async-start(bf16[64,16,128]{2,1,0:T(8,128)(2,1)} %get-tuple-element.26), calls=%async_computation | async-start | bytes 524288 | tf_op jit(solution)/shard_map/all_to_all | solution.py:441
  23.8 3.5 %side.1 = (f32[8,256,1024]{2,1,0:T(8,128)}, bf16[1024,128]{1,0:T(8,128)(2,1)}, bf16[256,1024]{1,0:T(8,128)(2,1)}) custom-call(bf16[256,1024]{1,0:T(8,128)(2,1)} %gate_hbm.1, s32[4,128]{1,0:T(4,128)} %bitcast.20, f32[4,128]{1,0:T(4,128)} %bitcast.21, f32[2,8,256,128]{3,2,1,0:T(8,128)} %get-tuple-element.27.run_hbm, f32[2,8,1024]{2,1,0:T(8,128)} %get-tuple-element.28.edge_hbm), custom_call_target="tpu_custom_call" | custom-call | flops 10000000000 | bytes 1048576 | tf_op jit(solution)/shard_map/side/pallas_call | solution.py:417
  27.3 5.9 %all-to-all-done.seen_ref = bf16[64,16,128]{2,1,0:T(8,128)(2,1)S(1)} async-done(((bf16[64,16,128]{2,1,0:T(8,128)(2,1)}), bf16[64,16,128]{2,1,0:T(8,128)(2,1)S(1)}, u32[]{:S(2)}, u32[]{:S(2)}) %all-to-all-start) | async-done | bytes 262176 | tf_op jit(solution)/shard_map/all_to_all | solution.py:441
  33.2 0.0 copy-start.1
  33.2 3.4 %mix.1 = (bf16[128,1024]{1,0:T(8,128)(2,1)S(1)}, bf16[128,1024]{1,0:T(8,128)(2,1)S(1)}, bf16[1024,2048]{1,0:T(8,128)(2,1)S(1)}) custom-call(s32[2]{0:T(128)S(1)} %pad_add_fusion.index_ref, bf16[64,16,128]{2,1,0:T(8,128)(2,1)S(1)} %all-to-all-done.seen_ref, f32[8,256,1024]{2,1,0:T(8,128)} %get-tuple-element.29.mixed_hbm, bf16[2048,2048]{1,0:T(8,128)(2,1)} %w_hbm.3), custom_call_target="tpu_custom_call" | custom-call | flops 100000000 | bytes 1048576 | tf_op jit(solution)/shard_map/mix/pallas_call | solution.py:453
  36.7 3.3 %collective-permute-start.1 = (bf16[128,1024]{1,0:T(8,128)(2,1)S(1)}, bf16[128,1024]{1,0:T(8,128)(2,1)S(1)}, u32[]{:S(2)}, u32[]{:S(2)}) collective-permute-start(bf16[128,1024]{1,0:T(8,128)(2,1)S(1)} %get-tuple-element.30), channel_id=1, source_target_pairs={{0,1},{1,0},{2,3},{3,2},{4,5},{5,4},{6,7},{7,6},{8,9},{9,8},{10,11... | collective-permute-start | bytes 786440 | tf_op jit(solution)/shard_map/ppermute | solution.py:462
  40.0 0.0 copy-done.1
  40.0 0.0 copy-start.9
  40.0 0.0 copy-start.10
  40.0 3.3 %project.1 = (f32[128,2048]{1,0:T(8,128)S(1)}, bf16[1024,2048]{1,0:T(8,128)(2,1)S(1)}) custom-call(s32[2]{0:T(128)S(1)} %pad_add_fusion.index_ref, bf16[128,1024]{1,0:T(8,128)(2,1)S(1)} %get-tuple-element.31.mine_ref, bf16[128,2048]{1,0:T(8,128)(2,1)S(1)} %copy-done.1, bf16[1024,2048]{1,0:T(8,128)(2,1)S(1)} %get-tuple-element.32.own_ref, ...), custom_call_target="tpu_custom_call" | custom-call | flops 1000000000 | bytes 1048576 | tf_op jit(solution)/shard_map/project/pallas_call | solution.py:464
  43.3 0.0 collective-permute-done.1.other_ref
  43.3 0.0 copy-done.9
  43.4 0.0 copy-done.10
  43.4 2.2 %dispatch.1 = (bf16[128,2048]{1,0:T(8,128)(2,1)S(1)}, bf16[1024,2048]{1,0:T(8,128)(2,1)S(1)}) custom-call(bf16[128,1024]{1,0:T(8,128)(2,1)S(1)} %collective-permute-done.1.other_ref, bf16[1024,2048]{1,0:T(8,128)(2,1)S(1)} %get-tuple-element.33.w_ref, f32[128,2048]{1,0:T(8,128)S(1)} %get-tuple-element.34.acc_ref, f32[1,2048]{1,0:T(1,128)S(1)} %bitcast.17, ...), custom_call_target="tpu_custom_call" | custom-call | flops 2000000000 | bytes 1048576 | tf_op jit(solution)/shard_map/dispatch/pallas_call | solution.py:473
  45.6 0.0 copy-start.3
  45.6 0.0 copy-start.4
  45.6 0.0 copy-start.5
  45.6 56.3 %all_to_all.15 = bf16[128,8,2048]{2,1,0:T(8,128)(2,1)S(1)} all-to-all(bf16[128,8,2048]{2,1,0:T(8,128)(2,1)S(1)} %bitcast.13), channel_id=1, replica_groups=mesh['sp'=64,'tp'=2] {'sp','tp'}, dimensions={0} | all-to-all | bytes 8388608 | tf_op jit(solution)/shard_map/all_to_all | solution.py:484
  101.9 0.0 copy-done.3
  101.9 0.0 copy-done.4
  101.9 0.0 copy-done.5
  101.9 0.0 copy-start.6
  101.9 0.0 copy-start.7
  102.0 0.0 copy-start.8
  102.0 6.8 %expert.1 = bf16[1024,2048]{1,0:T(8,128)(2,1)S(1)} custom-call(bf16[1024,2048]{1,0:T(8,128)(2,1)S(1)} %bitcast.15, bf16[1,2048,512]{2,1,0:T(8,128)(2,1)S(1)} %copy-done.3, bf16[1,2048,512]{2,1,0:T(8,128)(2,1)S(1)} %copy-done.4, bf16[1,512,2048]{2,1,0:T(8,128)(2,1)S(1)} %copy-done.5), custom_call_target="tpu_custom_call" | custom-call | flops 6000000000 | bytes 1048576 | tf_op jit(solution)/shard_map/expert/pallas_call | solution.py:488
  108.8 0.0 copy-done.6
  108.8 0.0 copy-done.7
  108.8 0.0 copy-done.8
  108.8 1.1 shared.1.base_ref
  110.0 0.0 copy-start
  110.0 0.0 copy-start.2
  110.0 57.0 %all_to_all.16 = bf16[128,8,2048]{2,1,0:T(8,128)(2,1)S(1)} all-to-all(bf16[128,8,2048]{2,1,0:T(8,128)(2,1)S(1)} %bitcast.14), channel_id=1, replica_groups=mesh['sp'=64,'tp'=2] {'sp','tp'}, dimensions={0} | all-to-all | bytes 8388608 | tf_op jit(solution)/shard_map/all_to_all | solution.py:484
  167.0 0.0 copy-done
  167.0 0.0 copy-done.2
  167.0 2.3 %finish.1 = bf16[128,2048]{1,0:T(8,128)(2,1)} custom-call(f32[128,2048]{1,0:T(8,128)S(1)} %shared.1.base_ref, bf16[256,1024]{1,0:T(8,128)(2,1)S(1)} %copy-done, bf16[1024,2048]{1,0:T(8,128)(2,1)S(1)} %bitcast.12, f32[1,2048]{1,0:T(1,128)S(1)} %bitcast.16), custom_call_target="tpu_custom_call" | custom-call | flops 1000000000 | bytes 1048576 | tf_op jit(solution)/shard_map/finish/pallas_call | solution.py:497
Async XLA Ops:
  0.7 4.7 %collective-permute-start = (bf16[3,1024]{1,0:T(4,128)(2,1)S(1)}, bf16[3,1024]{1,0:T(4,128)(2,1)S(1)}, u32[]{:S(2)}, u32[]{:S(2)}) collective-permute-start(bf16[3,1024]{1,0:T(4,128)(2,1)S(1)} %slice.3), channel_id=1, source_target_pairs={{0,2},{2,4},{4,6},{6,8},{8,10},{10,12},{12,14},{14,16},{16,18},{18... | collective-permute-start | bytes 18440 | tf_op jit(solution)/shard_map/ppermute | solution.py:405
  5.4 0.6 copy-start.11
  12.1 21.1 %all-to-all-start = ((bf16[64,16,128]{2,1,0:T(8,128)(2,1)}), bf16[64,16,128]{2,1,0:T(8,128)(2,1)S(1)}, u32[]{:S(2)}, u32[]{:S(2)}) async-start(bf16[64,16,128]{2,1,0:T(8,128)(2,1)} %get-tuple-element.26), calls=%async_computation | async-start | bytes 524288 | tf_op jit(solution)/shard_map/all_to_all | solution.py:441
  33.2 6.8 %copy-start.1 = (bf16[128,2048]{1,0:T(8,128)(2,1)S(1)}, bf16[128,2048]{1,0:T(8,128)(2,1)}, u32[]{:S(2)}) copy-start(bf16[128,2048]{1,0:T(8,128)(2,1)} %res_ref.1) | copy-start | bytes 1572868
  36.7 6.7 %collective-permute-start.1 = (bf16[128,1024]{1,0:T(8,128)(2,1)S(1)}, bf16[128,1024]{1,0:T(8,128)(2,1)S(1)}, u32[]{:S(2)}, u32[]{:S(2)}) collective-permute-start(bf16[128,1024]{1,0:T(8,128)(2,1)S(1)} %get-tuple-element.30), channel_id=1, source_target_pairs={{0,1},{1,0},{2,3},{3,2},{4,5},{5,4},{6,7},{7,6},{8,9},{9,8},{10,11... | collective-permute-start | bytes 786440 | tf_op jit(solution)/shard_map/ppermute | solution.py:462
  40.0 3.4 %copy-start.9 = (f32[2048]{0:T(1024)S(1)}, f32[2048]{0:T(1024)}, u32[]{:S(2)}) copy-start(f32[2048]{0:T(1024)} %param.28) | copy-start | bytes 24580
  40.0 3.4 %copy-start.10 = (bf16[1024,128]{1,0:T(8,128)(2,1)S(1)}, bf16[1024,128]{1,0:T(8,128)(2,1)}, u32[]{:S(2)}) copy-start(bf16[1024,128]{1,0:T(8,128)(2,1)} %get-tuple-element.35.g_ref) | copy-start | bytes 786436
  45.6 56.3 %copy-start.3 = (bf16[1,2048,512]{2,1,0:T(8,128)(2,1)S(1)}, bf16[1,2048,512]{2,1,0:T(8,128)(2,1)}, u32[]{:S(2)}) copy-start(bf16[1,2048,512]{2,1,0:T(8,128)(2,1)} %gate_ref.2) | copy-start | bytes 6291460
  45.6 56.3 %copy-start.4 = (bf16[1,2048,512]{2,1,0:T(8,128)(2,1)S(1)}, bf16[1,2048,512]{2,1,0:T(8,128)(2,1)}, u32[]{:S(2)}) copy-start(bf16[1,2048,512]{2,1,0:T(8,128)(2,1)} %up_ref.2) | copy-start | bytes 6291460
  45.6 56.3 %copy-start.5 = (bf16[1,512,2048]{2,1,0:T(8,128)(2,1)S(1)}, bf16[1,512,2048]{2,1,0:T(8,128)(2,1)}, u32[]{:S(2)}) copy-start(bf16[1,512,2048]{2,1,0:T(8,128)(2,1)} %down_ref.2) | copy-start | bytes 6291460
  101.9 6.9 %copy-start.6 = (bf16[2048,512]{1,0:T(8,128)(2,1)S(1)}, bf16[2048,512]{1,0:T(8,128)(2,1)}, u32[]{:S(2)}) copy-start(bf16[2048,512]{1,0:T(8,128)(2,1)} %gate_ref.3) | copy-start | bytes 6291460
  101.9 6.9 %copy-start.7 = (bf16[2048,512]{1,0:T(8,128)(2,1)S(1)}, bf16[2048,512]{1,0:T(8,128)(2,1)}, u32[]{:S(2)}) copy-start(bf16[2048,512]{1,0:T(8,128)(2,1)} %up_ref.3) | copy-start | bytes 6291460
  102.0 6.9 %copy-start.8 = (bf16[512,2048]{1,0:T(8,128)(2,1)S(1)}, bf16[512,2048]{1,0:T(8,128)(2,1)}, u32[]{:S(2)}) copy-start(bf16[512,2048]{1,0:T(8,128)(2,1)} %down_ref.3) | copy-start | bytes 6291460
  110.0 57.0 %copy-start = (bf16[256,1024]{1,0:T(8,128)(2,1)S(1)}, bf16[256,1024]{1,0:T(8,128)(2,1)}, u32[]{:S(2)}) copy-start(bf16[256,1024]{1,0:T(8,128)(2,1)} %get-tuple-element.41.c_ref) | copy-start | bytes 1572868
  110.0 57.0 %copy-start.2 = (f32[2048]{0:T(1024)S(1)}, f32[2048]{0:T(1024)}, u32[]{:S(2)}) copy-start(f32[2048]{0:T(1024)} %param.37) | copy-start | bytes 24580

commit v6 on v4

--- a/solution.py
+++ b/solution.py
@@ -17,7 +17,6 @@
 F32 = jnp.float32
 BF16 = jnp.bfloat16
 VMEM = pl.BlockSpec(memory_space=pltpu.VMEM)
-SMEM = pl.BlockSpec(memory_space=pltpu.SMEM)
 HBM = pl.BlockSpec(memory_space=pltpu.HBM)
 
 
@@ -85,14 +84,15 @@
 
 
 def scan_kernel(
-    halo_ref, x_hbm, taps_hbm, rmap_hbm, imap_hbm, rate_hbm, shift_hbm, tot_hbm, run_hbm, edge_hbm,
-    x_ref, taps_ref, rmap_ref, imap_ref, rate_ref, shift_ref, tot_ref, run_ref, edge_ref,
+    halo_hbm, x_hbm, taps_hbm, rmap_hbm, imap_hbm, rate_hbm, shift_hbm, tot_hbm, run_hbm, edge_hbm,
+    halo_ref, x_ref, taps_ref, rmap_ref, imap_ref, rate_ref, shift_ref, tot_ref, run_ref, edge_ref,
     ext, cv, rg, ig, sh, sems, outs,
 ):
     copies = fetch(
         [
             (x_hbm, x_ref),
             (taps_hbm, taps_ref),
+            (halo_hbm, halo_ref),
             (shift_hbm, shift_ref),
             (rate_hbm, rate_ref),
             (rmap_hbm, rmap_ref),
@@ -106,7 +106,7 @@
     heads, width = rmap_ref.shape[:2]
     reach = taps_ref.shape[0] - 1
     pad = 8 - reach
-    for copy in copies[:2]:
+    for copy in copies[:3]:
         copy.wait()
     for c in range(channels // 128):
         cols = slice(c * 128, (c + 1) * 128)
@@ -125,7 +125,7 @@
                 total = total + taps[j] * window[j]
             window = window[1:]
             cv[pl.ds(t * LANES, LANES), cols] = total.astype(BF16).astype(F32)
-    for copy in copies[2:]:
+    for copy in copies[3:]:
         copy.wait()
     for k in range(heads):
         cols = slice(k * width, (k + 1) * width)
@@ -252,21 +252,29 @@
 
 
 def mix_kernel(
-    index_ref, seen_ref, mixed_hbm, w_hbm, mine_ref, theirs_ref, w_ref, mixed_ref, sems
+    seen_ref, mixed_hbm, w_hbm, mine_ref, theirs_ref, w_ref, mixed_ref, sems
 ):
     _, tokens, channels = mixed_ref.shape
-    here, side = index_ref[0], index_ref[1]
-    depth = w_ref.shape[0]
-    own = pl.ds(pl.multiple_of(side * depth, depth), depth)
-    copies = fetch([(mixed_hbm.at[pl.ds(0, 2)], mixed_ref), (w_hbm.at[own, :], w_ref)], sems)
+    here, side = lax.axis_index("sp"), lax.axis_index("tp")
+    half = tokens // 2
+    strip = channels // 2
+    pairs = []
+    for j in range(4):
+        rows = pl.ds(j * (tokens // 4), tokens // 4)
+        pairs.append((mixed_hbm.at[pl.ds(0, 2), rows, :], mixed_ref.at[:, rows, :]))
+    for j in range(3):
+        at = (side if j < 2 else 1 - side) * channels + (j % 2) * strip
+        at = pl.multiple_of(at, strip)
+        pairs.append((w_hbm.at[pl.ds(at, strip), :], w_ref.at[pl.ds(j * strip, strip), :]))
+    copies = fetch(pairs, sems)
     carried = jnp.zeros((LANES, 128), F32)
     for i in range(seen_ref.shape[0]):
         pair = seen_ref[i].astype(F32)
         carried = jnp.where(i < here, jnp.exp(pair[:LANES]) * carried + pair[LANES:], carried)
     carried = jnp.concatenate([carried[i : i + 1] for i in range(LANES)], axis=1)
-    half = tokens // 2
     block = 16
-    copies[0].wait()
+    for copy in copies[:4]:
+        copy.wait()
 
     def put(i, _):
         at = pl.multiple_of(i * block, block)
@@ -278,7 +286,8 @@
         return 0
 
     lax.fori_loop(0, half // block, put, 0, unroll=2)
-    copies[1].wait()
+    for copy in copies[4:]:
+        copy.wait()
 
 
 def route(routes_ref, weight_ref, g_ref, c_ref):
@@ -318,18 +327,24 @@
         c_ref[rows:, cols] = jnp.transpose(jnp.where(chosen, to_slots(low), 0.0)).astype(BF16)
 
 
-def project_kernel(index_ref, mine_ref, res_ref, own_ref, w_hbm, out_ref, rest_ref, sems):
+def project_kernel(mine_ref, res_ref, w_ref, w_hbm, out_ref, rest_ref, sems):
     depth = mine_ref.shape[1]
-    rest = pl.ds(pl.multiple_of((1 - index_ref[1]) * depth, depth), depth)
-    copies = fetch([(w_hbm.at[rest, :], rest_ref)], sems)
+    half = depth // 2
+    at = pl.multiple_of((1 - lax.axis_index("tp")) * depth + half, half)
+    copies = fetch([(w_hbm.at[pl.ds(at, half), :], rest_ref)], sems)
     out_ref[...] = ALPHA * res_ref[...].astype(F32) + jnp.dot(
-        mine_ref[...], own_ref[...], preferred_element_type=F32
+        mine_ref[...], w_ref[:depth], preferred_element_type=F32
     )
     copies[0].wait()
 
 
-def dispatch_kernel(other_ref, w_ref, acc_ref, gain_ref, g_ref, normed_ref, out_ref):
-    values = acc_ref[...] + jnp.dot(other_ref[...], w_ref[...], preferred_element_type=F32)
+def dispatch_kernel(other_ref, w_ref, rest_ref, acc_ref, gain_ref, g_ref, normed_ref, out_ref):
+    depth = other_ref.shape[1]
+    values = (
+        acc_ref[...]
+        + jnp.dot(other_ref[:, : depth // 2], w_ref[depth:], preferred_element_type=F32)
+        + jnp.dot(other_ref[:, depth // 2 :], rest_ref[...], preferred_element_type=F32)
+    )
     normed = layer_norm(values, gain_ref[...]).astype(BF16)
     normed_ref[...] = normed
 
@@ -386,15 +401,13 @@
     model = out_weight.shape[1]
     slots = experts * CAP
     sem = pltpu.SemaphoreType.DMA
-    index = jnp.stack([lax.axis_index("sp"), lax.axis_index("tp")]).astype(jnp.int32)
     before = lax.ppermute(conv_in[tokens - reach :], "sp", [(i, i + 1) for i in range(sp - 1)])
-    before, index = lax.optimization_barrier((before, index))
     padded = shape((8, tokens, channels), F32)
     big = pltpu.VMEM((tokens, channels), F32)
     apart = tokens + 8 * LANES
     lanes = pltpu.VMEM((channels // 128, apart, 128), F32)
 
-    def staged(kernel, first, operands, made, flops, scratch, name):
+    def staged(kernel, operands, made, flops, scratch, name):
         held = [
             pltpu.VMEM((2,) + x.shape[1:] if x is padded else x.shape, x.dtype)
             for x in tuple(operands) + made
@@ -402,31 +415,29 @@
         return call(
             kernel,
             made,
-            [VMEM] * len(first) + [HBM] * len(operands),
+            [HBM] * len(operands),
             flops,
             held + scratch,
             name=name,
             out_specs=(HBM,) * len(made),
             limit=62,
-        )(*first, *operands)
+        )(*operands)
 
     totals, local, edge = staged(
         scan_kernel,
-        (before,),
-        (conv_in, conv_taps, recur_map, input_map, rate_logit[None], decay_shift.T),
+        (before, conv_in, conv_taps, recur_map, input_map, rate_logit[None], decay_shift.T),
         (
             shape((sp, 2 * LANES, 128), BF16),
             shape((2, channels // 128, tokens, 128), F32),
             shape((2, LANES, channels), F32),
         ),
         10**9,
-        [lanes, big, big, big, pltpu.VMEM((apart, 128), F32), sem((6,)), sem((6,))],
+        [lanes, big, big, big, pltpu.VMEM((apart, 128), F32), sem((7,)), sem((6,))],
         "scan",
     )
     seen = lax.all_to_all(totals, "sp", 0, 0, tiled=True)
     parts, g, c = staged(
         side_kernel,
-        (),
         (gate_pre, routes.T, route_weight.T, local, edge),
         (padded, shape((slots, rows), BF16), shape((2 * rows, slots), BF16)),
         10**10,
@@ -434,35 +445,34 @@
         "side",
     )
     piece = shape((rows, channels), BF16)
-    strip = shape((channels, model), BF16)
-    mine, theirs, own = call(
+    mine, theirs, most = call(
         mix_kernel,
-        (piece, piece, strip),
-        [SMEM, VMEM, HBM, HBM],
+        (piece, piece, shape((3 * channels // 2, model), BF16)),
+        [VMEM, HBM, HBM],
         10**8,
-        [pltpu.VMEM((2, tokens, channels), F32), sem((2,))],
+        [pltpu.VMEM((2, tokens, channels), F32), sem((7,))],
         name="mix",
-        limit=46,
-    )(index, seen, parts, out_weight)
+        limit=44,
+    )(seen, parts, out_weight)
     other = lax.ppermute(theirs, "tp", [(0, 1), (1, 0)])
     wide = shape((rows, model), F32)
     acc, rest = call(
         project_kernel,
-        (wide, strip),
-        [SMEM, VMEM, VMEM, VMEM, HBM],
+        (wide, shape((channels // 2, model), BF16)),
+        [VMEM, VMEM, VMEM, HBM],
         10**9,
         [sem((1,))],
         name="project",
         limit=40,
-    )(index, mine, residual, own, out_weight)
+    )(mine, residual, most, out_weight)
     normed, outgoing = call(
         dispatch_kernel,
         (shape((rows, model), BF16), shape((slots, model), BF16)),
-        [VMEM] * 5,
+        [VMEM] * 6,
         2 * 10**9,
         name="dispatch",
         limit=24,
-    )(other, rest, acc, gain_mix[None], g)
+    )(other, most, rest, acc, gain_mix[None], g)
 
     def exchanged(x):
         x = x.reshape(experts, CAP, model)

time: 170 us -> 168 us (0.988)
  transfers between devices with their start and end apart: 3 -> 3, of which waited for: 2 -> 2; matrix products, arithmetic and copies ran while one was open for 0% -> 0% of each run, Pallas kernels for 4% -> 3%
where the time goes in v6:
time: 168 us
  blocking collectives  113 us (67%)
  Pallas kernels  27.3 us (16%)
  starting transfers between devices  18.9 us (11%)
  waiting for transfers between devices  6.71 us (4%)
    all_to_all x2, blocking collectives, exchanged(): x = lax.all_to_all(x, ('sp', 'tp'), split_axis=0, concat_axis=0, tiled=True)  113 us
    all_to_all x1, starting transfers between devices, on_device(): seen = lax.all_to_all(totals, 'sp', 0, 0, tiled=True)  11.6 us
    pallas_call x2, Pallas kernels, staged(): call(kernel, made, [HBM] * len(operands), flops, held + scratch, name=nam...  8.92 us
    pallas_call x1, Pallas kernels, on_device(): call(expert_kernel, shape((slots, model), BF16), [VMEM] * 4, 6 * 10 ** 9,...  6.84 us
    all_to_all x1, waiting for transfers between devices, on_device(): seen = lax.all_to_all(totals, 'sp', 0, 0, tiled=True)  5.93 us
    ppermute x1, starting transfers between devices, on_device(): lax.ppermute(conv_in[tokens - reach:], 'sp', [(i, i + 1) for i in range(s...  3.92 us
    pallas_call x1, Pallas kernels, on_device(): call(mix_kernel, (piece, piece, shape((3 * channels // 2, model), BF16)),...  3.61 us
  transfers between devices with their start and end apart: 3, of which 2 were waited for; matrix products, arithmetic and copies ran while one was open for 0% of the time, Pallas kernels for 3%

profile of v6, /device:TPU:1, one launch (start us, length us, event | category | flops | bytes accessed | tf_op | source)
XLA Modules:
  0.0 167.7 jit_solution(10132146273302785903)
XLA Ops:
  0.0 0.7 slice.3
  0.7 3.9 %collective-permute-start = (bf16[3,1024]{1,0:T(4,128)(2,1)S(1)}, bf16[3,1024]{1,0:T(4,128)(2,1)S(1)}, u32[]{:S(2)}, u32[]{:S(2)}) collective-permute-start(bf16[3,1024]{1,0:T(4,128)(2,1)S(1)} %slice.3), channel_id=1, source_target_pairs={{0,2},{2,4},{4,6},{6,8},{8,10},{10,12},{12,14},{14,16},{16,18},{18... | collective-permute-start | bytes 18440 | tf_op jit(solution)/shard_map/ppermute | solution.py:404
  4.7 0.8 collective-permute-done.halo_hbm
  5.4 0.0 copy-start.11
  5.4 0.6 copy-done.11
  6.0 5.4 %scan.1 = (bf16[64,16,128]{2,1,0:T(8,128)(2,1)}, f32[2,8,256,128]{3,2,1,0:T(8,128)}, f32[2,8,1024]{2,1,0:T(8,128)}) custom-call(bf16[3,1024]{1,0:T(4,128)(2,1)} %copy-done.11, bf16[256,1024]{1,0:T(8,128)(2,1)} %x_hbm.1, bf16[4,1024]{1,0:T(4,128)(2,1)} %taps_hbm.1, bf16[4,256,256]{2,1,0:T(8,128)(2,1)} %rmap_hbm.1, bf16[4,256,256]{2,1,0:T(8,128)(2,1)} %imap_hbm.1, ...), custom_call_target="tpu_custom_call" | custom-call | flops 1000000000 | bytes 1048576 | tf_op jit(solution)/shard_map/scan/pallas_call | solution.py:415
  11.4 11.6 %all-to-all-start = ((bf16[64,16,128]{2,1,0:T(8,128)(2,1)}), bf16[64,16,128]{2,1,0:T(8,128)(2,1)S(1)}, u32[]{:S(2)}, u32[]{:S(2)}) async-start(bf16[64,16,128]{2,1,0:T(8,128)(2,1)} %get-tuple-element.22), calls=%async_computation | async-start | bytes 524288 | tf_op jit(solution)/shard_map/all_to_all | solution.py:438
  23.1 3.5 %side.1 = (f32[8,256,1024]{2,1,0:T(8,128)}, bf16[1024,128]{1,0:T(8,128)(2,1)}, bf16[256,1024]{1,0:T(8,128)(2,1)}) custom-call(bf16[256,1024]{1,0:T(8,128)(2,1)} %gate_hbm.1, s32[4,128]{1,0:T(4,128)} %bitcast.18, f32[4,128]{1,0:T(4,128)} %bitcast.19, f32[2,8,256,128]{3,2,1,0:T(8,128)} %get-tuple-element.23.run_hbm, f32[2,8,1024]{2,1,0:T(8,128)} %get-tuple-element.24.edge_hbm), custom_call_target="tpu_custom_call" | custom-call | flops 10000000000 | bytes 1048576 | tf_op jit(solution)/shard_map/side/pallas_call | solution.py:415
  26.6 5.9 %all-to-all-done.seen_ref = bf16[64,16,128]{2,1,0:T(8,128)(2,1)S(1)} async-done(((bf16[64,16,128]{2,1,0:T(8,128)(2,1)}), bf16[64,16,128]{2,1,0:T(8,128)(2,1)S(1)}, u32[]{:S(2)}, u32[]{:S(2)}) %all-to-all-start) | async-done | bytes 262176 | tf_op jit(solution)/shard_map/all_to_all | solution.py:438
  32.5 0.0 copy-start.1
  32.6 3.6 %mix.1 = (bf16[128,1024]{1,0:T(8,128)(2,1)S(1)}, bf16[128,1024]{1,0:T(8,128)(2,1)S(1)}, bf16[1536,2048]{1,0:T(8,128)(2,1)S(1)}) custom-call(bf16[64,16,128]{2,1,0:T(8,128)(2,1)S(1)} %all-to-all-done.seen_ref, f32[8,256,1024]{2,1,0:T(8,128)} %get-tuple-element.25.mixed_hbm, bf16[2048,2048]{1,0:T(8,128)(2,1)} %w_hbm.3), custom_call_target="tpu_custom_call" | custom-call | flops 100000000 | bytes 1048576 | tf_op jit(solution)/shard_map/mix/pallas_call | solution.py:448
  36.2 3.3 %collective-permute-start.1 = (bf16[128,1024]{1,0:T(8,128)(2,1)S(1)}, bf16[128,1024]{1,0:T(8,128)(2,1)S(1)}, u32[]{:S(2)}, u32[]{:S(2)}) collective-permute-start(bf16[128,1024]{1,0:T(8,128)(2,1)S(1)} %get-tuple-element.26), channel_id=1, source_target_pairs={{0,1},{1,0},{2,3},{3,2},{4,5},{5,4},{6,7},{7,6},{8,9},{9,8},{10,11... | collective-permute-start | bytes 786440 | tf_op jit(solution)/shard_map/ppermute | solution.py:457
  39.5 0.0 copy-done.1
  39.5 0.0 copy-start.2
  39.5 0.0 copy-start.4
  39.5 2.2 %project.1 = (f32[128,2048]{1,0:T(8,128)S(1)}, bf16[512,2048]{1,0:T(8,128)(2,1)S(1)}) custom-call(bf16[128,1024]{1,0:T(8,128)(2,1)S(1)} %get-tuple-element.28.mine_ref, bf16[128,2048]{1,0:T(8,128)(2,1)S(1)} %copy-done.1, bf16[1536,2048]{1,0:T(8,128)(2,1)S(1)} %get-tuple-element.27.w_ref, bf16[2048,2048]{1,0:T(8,128)(2,1)} %w_hbm.3), custom_call_target="tpu_custom_call" | custom-call | flops 1000000000 | bytes 1048576 | tf_op jit(solution)/shard_map/project/pallas_call | solution.py:459
  41.7 0.0 collective-permute-done.1.other_ref
  41.7 0.0 copy-done.2
  41.7 0.0 copy-done.4
  41.7 2.2 %dispatch.1 = (bf16[128,2048]{1,0:T(8,128)(2,1)S(1)}, bf16[1024,2048]{1,0:T(8,128)(2,1)S(1)}) custom-call(bf16[128,1024]{1,0:T(8,128)(2,1)S(1)} %collective-permute-done.1.other_ref, bf16[1536,2048]{1,0:T(8,128)(2,1)S(1)} %get-tuple-element.27.w_ref, bf16[512,2048]{1,0:T(8,128)(2,1)S(1)} %get-tuple-element.29.rest_ref, ...), custom_call_target="tpu_custom_call" | custom-call | flops 2000000000 | bytes 1048576 | tf_op jit(solution)/shard_map/dispatch/pallas_call | solution.py:468
  44.0 0.0 copy-start.5
  44.0 0.0 copy-start.6
  44.0 0.0 copy-start.7
  44.0 56.3 %all_to_all.15 = bf16[128,8,2048]{2,1,0:T(8,128)(2,1)S(1)} all-to-all(bf16[128,8,2048]{2,1,0:T(8,128)(2,1)S(1)} %bitcast.11), channel_id=1, replica_groups=mesh['sp'=64,'tp'=2] {'sp','tp'}, dimensions={0} | all-to-all | bytes 8388608 | tf_op jit(solution)/shard_map/all_to_all | solution.py:479
  100.3 0.0 copy-done.5
  100.3 0.0 copy-done.6
  100.3 0.0 copy-done.7
  100.3 0.0 copy-start.8
  100.3 0.0 copy-start.9
  100.3 0.0 copy-start.10
  100.4 6.8 %expert.1 = bf16[1024,2048]{1,0:T(8,128)(2,1)S(1)} custom-call(bf16[1024,2048]{1,0:T(8,128)(2,1)S(1)} %bitcast.13, bf16[1,2048,512]{2,1,0:T(8,128)(2,1)S(1)} %copy-done.5, bf16[1,2048,512]{2,1,0:T(8,128)(2,1)S(1)} %copy-done.6, bf16[1,512,2048]{2,1,0:T(8,128)(2,1)S(1)} %copy-done.7), custom_call_target="tpu_custom_call" | custom-call | flops 6000000000 | bytes 1048576 | tf_op jit(solution)/shard_map/expert/pallas_call | solution.py:483
  107.2 0.0 copy-done.8
  107.2 0.0 copy-done.9
  107.2 0.0 copy-done.10
  107.2 1.1 shared.1.base_ref
  108.3 0.0 copy-start
  108.4 0.0 copy-start.3
  108.4 57.0 %all_to_all.16 = bf16[128,8,2048]{2,1,0:T(8,128)(2,1)S(1)} all-to-all(bf16[128,8,2048]{2,1,0:T(8,128)(2,1)S(1)} %bitcast.12), channel_id=1, replica_groups=mesh['sp'=64,'tp'=2] {'sp','tp'}, dimensions={0} | all-to-all | bytes 8388608 | tf_op jit(solution)/shard_map/all_to_all | solution.py:479
  165.4 0.0 copy-done
  165.4 0.0 copy-done.3
  165.4 2.3 %finish.1 = bf16[128,2048]{1,0:T(8,128)(2,1)} custom-call(f32[128,2048]{1,0:T(8,128)S(1)} %shared.1.base_ref, bf16[256,1024]{1,0:T(8,128)(2,1)S(1)} %copy-done, bf16[1024,2048]{1,0:T(8,128)(2,1)S(1)} %bitcast.10, f32[1,2048]{1,0:T(1,128)S(1)} %bitcast.14), custom_call_target="tpu_custom_call" | custom-call | flops 1000000000 | bytes 1048576 | tf_op jit(solution)/shard_map/finish/pallas_call | solution.py:492
Async XLA Ops:
  0.7 4.7 %collective-permute-start = (bf16[3,1024]{1,0:T(4,128)(2,1)S(1)}, bf16[3,1024]{1,0:T(4,128)(2,1)S(1)}, u32[]{:S(2)}, u32[]{:S(2)}) collective-permute-start(bf16[3,1024]{1,0:T(4,128)(2,1)S(1)} %slice.3), channel_id=1, source_target_pairs={{0,2},{2,4},{4,6},{6,8},{8,10},{10,12},{12,14},{14,16},{16,18},{18... | collective-permute-start | bytes 18440 | tf_op jit(solution)/shard_map/ppermute | solution.py:404
  5.4 0.6 copy-start.11
  11.4 21.1 %all-to-all-start = ((bf16[64,16,128]{2,1,0:T(8,128)(2,1)}), bf16[64,16,128]{2,1,0:T(8,128)(2,1)S(1)}, u32[]{:S(2)}, u32[]{:S(2)}) async-start(bf16[64,16,128]{2,1,0:T(8,128)(2,1)} %get-tuple-element.22), calls=%async_computation | async-start | bytes 524288 | tf_op jit(solution)/shard_map/all_to_all | solution.py:438
  32.5 7.0 %copy-start.1 = (bf16[128,2048]{1,0:T(8,128)(2,1)S(1)}, bf16[128,2048]{1,0:T(8,128)(2,1)}, u32[]{:S(2)}) copy-start(bf16[128,2048]{1,0:T(8,128)(2,1)} %res_ref.1) | copy-start | bytes 1572868
  36.2 5.5 %collective-permute-start.1 = (bf16[128,1024]{1,0:T(8,128)(2,1)S(1)}, bf16[128,1024]{1,0:T(8,128)(2,1)S(1)}, u32[]{:S(2)}, u32[]{:S(2)}) collective-permute-start(bf16[128,1024]{1,0:T(8,128)(2,1)S(1)} %get-tuple-element.26), channel_id=1, source_target_pairs={{0,1},{1,0},{2,3},{3,2},{4,5},{5,4},{6,7},{7,6},{8,9},{9,8},{10,11... | collective-permute-start | bytes 786440 | tf_op jit(solution)/shard_map/ppermute | solution.py:457
  39.5 2.2 %copy-start.2 = (bf16[1024,128]{1,0:T(8,128)(2,1)S(1)}, bf16[1024,128]{1,0:T(8,128)(2,1)}, u32[]{:S(2)}) copy-start(bf16[1024,128]{1,0:T(8,128)(2,1)} %get-tuple-element.31.g_ref) | copy-start | bytes 786436
  39.5 2.2 %copy-start.4 = (f32[2048]{0:T(1024)S(1)}, f32[2048]{0:T(1024)}, u32[]{:S(2)}) copy-start(f32[2048]{0:T(1024)} %param.28) | copy-start | bytes 24580
  44.0 56.3 %copy-start.5 = (bf16[1,2048,512]{2,1,0:T(8,128)(2,1)S(1)}, bf16[1,2048,512]{2,1,0:T(8,128)(2,1)}, u32[]{:S(2)}) copy-start(bf16[1,2048,512]{2,1,0:T(8,128)(2,1)} %gate_ref.2) | copy-start | bytes 6291460
  44.0 56.3 %copy-start.6 = (bf16[1,2048,512]{2,1,0:T(8,128)(2,1)S(1)}, bf16[1,2048,512]{2,1,0:T(8,128)(2,1)}, u32[]{:S(2)}) copy-start(bf16[1,2048,512]{2,1,0:T(8,128)(2,1)} %up_ref.2) | copy-start | bytes 6291460
  44.0 56.3 %copy-start.7 = (bf16[1,512,2048]{2,1,0:T(8,128)(2,1)S(1)}, bf16[1,512,2048]{2,1,0:T(8,128)(2,1)}, u32[]{:S(2)}) copy-start(bf16[1,512,2048]{2,1,0:T(8,128)(2,1)} %down_ref.2) | copy-start | bytes 6291460
  100.3 6.9 %copy-start.8 = (bf16[2048,512]{1,0:T(8,128)(2,1)S(1)}, bf16[2048,512]{1,0:T(8,128)(2,1)}, u32[]{:S(2)}) copy-start(bf16[2048,512]{1,0:T(8,128)(2,1)} %gate_ref.3) | copy-start | bytes 6291460
  100.3 6.9 %copy-start.9 = (bf16[2048,512]{1,0:T(8,128)(2,1)S(1)}, bf16[2048,512]{1,0:T(8,128)(2,1)}, u32[]{:S(2)}) copy-start(bf16[2048,512]{1,0:T(8,128)(2,1)} %up_ref.3) | copy-start | bytes 6291460
  100.3 6.9 %copy-start.10 = (bf16[512,2048]{1,0:T(8,128)(2,1)S(1)}, bf16[512,2048]{1,0:T(8,128)(2,1)}, u32[]{:S(2)}) copy-start(bf16[512,2048]{1,0:T(8,128)(2,1)} %down_ref.3) | copy-start | bytes 6291460
  108.3 57.0 %copy-start = (bf16[256,1024]{1,0:T(8,128)(2,1)S(1)}, bf16[256,1024]{1,0:T(8,128)(2,1)}, u32[]{:S(2)}) copy-start(bf16[256,1024]{1,0:T(8,128)(2,1)} %get-tuple-element.37.c_ref) | copy-start | bytes 1572868
  108.4 57.0 %copy-start.3 = (f32[2048]{0:T(1024)S(1)}, f32[2048]{0:T(1024)}, u32[]{:S(2)}) copy-start(f32[2048]{0:T(1024)} %param.37) | copy-start | bytes 24580

commit v7 on v6

--- a/solution.py
+++ b/solution.py
@@ -309,8 +309,7 @@
         member.astype(BF16), jnp.where(earlier, 1.0, 0.0).astype(BF16), preferred_element_type=F32
     )
     rank = jnp.where(member > 0.0, rank, -1.0).astype(BF16)
-    high = weight.astype(BF16)
-    low = (weight - high.astype(F32)).astype(BF16)
+    weight = weight.astype(BF16)
     slot = lax.broadcasted_iota(jnp.int32, (BLOCK, experts), 0)
     spread_at = lax.broadcasted_iota(jnp.int32, (BLOCK, experts), 1)
     place = (lax.broadcasted_iota(jnp.int32, (BLOCK, rows), 0) % CAP).astype(F32)
@@ -323,8 +322,7 @@
         chosen = to_slots(rank) == place
         g_ref[pl.ds(b * BLOCK, BLOCK), :] = jnp.where(chosen, 1.0, 0.0).astype(BF16)
         cols = slice(b * BLOCK, (b + 1) * BLOCK)
-        c_ref[:rows, cols] = jnp.transpose(jnp.where(chosen, to_slots(high), 0.0)).astype(BF16)
-        c_ref[rows:, cols] = jnp.transpose(jnp.where(chosen, to_slots(low), 0.0)).astype(BF16)
+        c_ref[:, cols] = jnp.transpose(jnp.where(chosen, to_slots(weight), 0.0)).astype(BF16)
 
 
 def project_kernel(mine_ref, res_ref, w_ref, w_hbm, out_ref, rest_ref, sems):
@@ -358,15 +356,9 @@
     ).astype(BF16)
 
 
-def shared_kernel(x_ref, gate_ref, up_ref, down_ref, out_ref):
-    x = x_ref[...]
-    hidden = hidden_of(x, gate_ref[...], up_ref[...])
-    out_ref[...] = ALPHA * x.astype(F32) + jnp.dot(
-        hidden, down_ref[...], preferred_element_type=F32
-    )
-
-
-def expert_kernel(x_ref, gate_ref, up_ref, down_ref, out_ref):
+def expert_kernel(
+    x_ref, gate_ref, up_ref, down_ref, own_ref, sgate_ref, sup_ref, sdown_ref, out_ref, base_ref
+):
     block = 2 * BLOCK
 
     def step(i, _):
@@ -376,16 +368,16 @@
         return 0
 
     lax.fori_loop(0, x_ref.shape[0] // block, step, 0)
-
-
-def finish_kernel(base_ref, c_ref, back_ref, gain_ref, out_ref, acc):
-    rows = base_ref.shape[0]
-    width = 512
-    for j in range(base_ref.shape[1] // width):
-        cols = slice(j * width, (j + 1) * width)
-        part = jnp.dot(c_ref[...], back_ref[:, cols], preferred_element_type=F32)
-        acc[:, cols] = base_ref[:, cols] + part[:rows] + part[rows:]
-    out_ref[...] = layer_norm(acc[...], gain_ref[...]).astype(BF16)
+    x = own_ref[...]
+    hidden = hidden_of(x, sgate_ref[...], sup_ref[...])
+    base_ref[...] = ALPHA * x.astype(F32) + jnp.dot(
+        hidden, sdown_ref[...], preferred_element_type=F32
+    )
+
+
+def finish_kernel(base_ref, c_ref, back_ref, gain_ref, out_ref):
+    values = base_ref[...] + jnp.dot(c_ref[...], back_ref[...], preferred_element_type=F32)
+    out_ref[...] = layer_norm(values, gain_ref[...]).astype(BF16)
 
 
 def on_device(
@@ -439,7 +431,7 @@
     parts, g, c = staged(
         side_kernel,
         (gate_pre, routes.T, route_weight.T, local, edge),
-        (padded, shape((slots, rows), BF16), shape((2 * rows, slots), BF16)),
+        (padded, shape((slots, rows), BF16), shape((rows, slots), BF16)),
         10**10,
         [sem((5,)), sem((6,))],
         "side",
@@ -480,21 +472,22 @@
         return x.reshape(slots, model)
 
     received = exchanged(outgoing)
-    results = call(
-        expert_kernel, shape((slots, model), BF16), [VMEM] * 4, 6 * 10**9, name="expert", limit=24
-    )(received, expert_gate, expert_up, expert_down)
-    normed, results = lax.optimization_barrier((normed, results))
-    base = call(shared_kernel, wide, [VMEM] * 4, 10**10, name="shared")(
-        normed, shared_gate, shared_up, shared_down
-    )
-    base, results = lax.optimization_barrier((base, results))
+    results, base = call(
+        expert_kernel,
+        (shape((slots, model), BF16), wide),
+        [VMEM] * 8,
+        7 * 10**9,
+        name="expert",
+        limit=24,
+    )(
+        received, expert_gate, expert_up, expert_down, normed, shared_gate, shared_up, shared_down
+    )
     back = exchanged(results)
     return call(
         finish_kernel,
         shape((rows, model), BF16),
         [VMEM] * 4,
         10**9,
-        [pltpu.VMEM((rows, model), F32)],
         name="finish",
     )(base, c, back, gain_out[None])
 

time: 168 us -> 167 us (level)
    pallas_call x3 -> x2, Pallas kernels: 10.3 us -> 9.74 us  [the longest x1 7.93 us: on_device(): call(expert_kernel, (shape((slots, model), BF16), wide), [VMEM] * 8, 7 *...]
where the time goes in v7:
time: 167 us
  blocking collectives  113 us (68%)
  Pallas kernels  26.7 us (16%)
  starting transfers between devices  18.9 us (11%)
  waiting for transfers between devices  6.71 us (4%)
    all_to_all x2, blocking collectives, exchanged(): x = lax.all_to_all(x, ('sp', 'tp'), split_axis=0, concat_axis=0, tiled=True)  113 us
    all_to_all x1, starting transfers between devices, on_device(): seen = lax.all_to_all(totals, 'sp', 0, 0, tiled=True)  11.6 us
    pallas_call x2, Pallas kernels, staged(): call(kernel, made, [HBM] * len(operands), flops, held + scratch, name=nam...  8.86 us
    pallas_call x1, Pallas kernels, on_device(): call(expert_kernel, (shape((slots, model), BF16), wide), [VMEM] * 8, 7 *...  7.93 us
    all_to_all x1, waiting for transfers between devices, on_device(): seen = lax.all_to_all(totals, 'sp', 0, 0, tiled=True)  5.93 us
    ppermute x1, starting transfers between devices, on_device(): lax.ppermute(conv_in[tokens - reach:], 'sp', [(i, i + 1) for i in range(s...  3.92 us
    pallas_call x1, Pallas kernels, on_device(): call(mix_kernel, (piece, piece, shape((3 * channels // 2, model), BF16)),...  3.61 us
  transfers between devices with their start and end apart: 3, of which 2 were waited for; matrix products, arithmetic and copies ran while one was open for 0% of the time, Pallas kernels for 3%

profile of v7, /device:TPU:1, one launch (start us, length us, event | category | flops | bytes accessed | tf_op | source)
XLA Modules:
  0.0 167.1 jit_solution(17802326577877994112)
XLA Ops:
  0.0 0.7 slice.3
  0.7 3.9 %collective-permute-start = (bf16[3,1024]{1,0:T(4,128)(2,1)S(1)}, bf16[3,1024]{1,0:T(4,128)(2,1)S(1)}, u32[]{:S(2)}, u32[]{:S(2)}) collective-permute-start(bf16[3,1024]{1,0:T(4,128)(2,1)S(1)} %slice.3), channel_id=1, source_target_pairs={{0,2},{2,4},{4,6},{6,8},{8,10},{10,12},{12,14},{14,16},{16,18},{18... | collective-permute-start | bytes 18440 | tf_op jit(solution)/shard_map/ppermute | solution.py:396
  4.7 0.8 collective-permute-done.halo_hbm
  5.4 0.0 copy-start.11
  5.4 0.6 copy-done.11
  6.0 5.3 %scan.1 = (bf16[64,16,128]{2,1,0:T(8,128)(2,1)}, f32[2,8,256,128]{3,2,1,0:T(8,128)}, f32[2,8,1024]{2,1,0:T(8,128)}) custom-call(bf16[3,1024]{1,0:T(4,128)(2,1)} %copy-done.11, bf16[256,1024]{1,0:T(8,128)(2,1)} %x_hbm.1, bf16[4,1024]{1,0:T(4,128)(2,1)} %taps_hbm.1, bf16[4,256,256]{2,1,0:T(8,128)(2,1)} %rmap_hbm.1, bf16[4,256,256]{2,1,0:T(8,128)(2,1)} %imap_hbm.1, ...), custom_call_target="tpu_custom_call" | custom-call | flops 1000000000 | bytes 1048576 | tf_op jit(solution)/shard_map/scan/pallas_call | solution.py:407
  11.4 11.6 %all-to-all-start = ((bf16[64,16,128]{2,1,0:T(8,128)(2,1)}), bf16[64,16,128]{2,1,0:T(8,128)(2,1)S(1)}, u32[]{:S(2)}, u32[]{:S(2)}) async-start(bf16[64,16,128]{2,1,0:T(8,128)(2,1)} %get-tuple-element.20), calls=%async_computation | async-start | bytes 524288 | tf_op jit(solution)/shard_map/all_to_all | solution.py:430
  23.0 3.5 %side.1 = (f32[8,256,1024]{2,1,0:T(8,128)}, bf16[1024,128]{1,0:T(8,128)(2,1)}, bf16[128,1024]{1,0:T(8,128)(2,1)}) custom-call(bf16[256,1024]{1,0:T(8,128)(2,1)} %gate_hbm.1, s32[4,128]{1,0:T(4,128)} %bitcast.18, f32[4,128]{1,0:T(4,128)} %bitcast.19, f32[2,8,256,128]{3,2,1,0:T(8,128)} %get-tuple-element.21.run_hbm, f32[2,8,1024]{2,1,0:T(8,128)} %get-tuple-element.22.edge_hbm), custom_call_target="tpu_custom_call" | custom-call | flops 10000000000 | bytes 1048576 | tf_op jit(solution)/shard_map/side/pallas_call | solution.py:407
  26.5 5.9 %all-to-all-done.seen_ref = bf16[64,16,128]{2,1,0:T(8,128)(2,1)S(1)} async-done(((bf16[64,16,128]{2,1,0:T(8,128)(2,1)}), bf16[64,16,128]{2,1,0:T(8,128)(2,1)S(1)}, u32[]{:S(2)}, u32[]{:S(2)}) %all-to-all-start) | async-done | bytes 262176 | tf_op jit(solution)/shard_map/all_to_all | solution.py:430
  32.5 0.0 copy-start
  32.5 3.6 %mix.1 = (bf16[128,1024]{1,0:T(8,128)(2,1)S(1)}, bf16[128,1024]{1,0:T(8,128)(2,1)S(1)}, bf16[1536,2048]{1,0:T(8,128)(2,1)S(1)}) custom-call(bf16[64,16,128]{2,1,0:T(8,128)(2,1)S(1)} %all-to-all-done.seen_ref, f32[8,256,1024]{2,1,0:T(8,128)} %get-tuple-element.23.mixed_hbm, bf16[2048,2048]{1,0:T(8,128)(2,1)} %w_hbm.3), custom_call_target="tpu_custom_call" | custom-call | flops 100000000 | bytes 1048576 | tf_op jit(solution)/shard_map/mix/pallas_call | solution.py:440
  36.1 3.3 %collective-permute-start.1 = (bf16[128,1024]{1,0:T(8,128)(2,1)S(1)}, bf16[128,1024]{1,0:T(8,128)(2,1)S(1)}, u32[]{:S(2)}, u32[]{:S(2)}) collective-permute-start(bf16[128,1024]{1,0:T(8,128)(2,1)S(1)} %get-tuple-element.24), channel_id=1, source_target_pairs={{0,1},{1,0},{2,3},{3,2},{4,5},{5,4},{6,7},{7,6},{8,9},{9,8},{10,11... | collective-permute-start | bytes 786440 | tf_op jit(solution)/shard_map/ppermute | solution.py:449
  39.4 0.0 copy-done
  39.4 0.0 copy-start.2
  39.4 0.0 copy-start.4
  39.4 2.2 %project.1 = (f32[128,2048]{1,0:T(8,128)S(1)}, bf16[512,2048]{1,0:T(8,128)(2,1)S(1)}) custom-call(bf16[128,1024]{1,0:T(8,128)(2,1)S(1)} %get-tuple-element.26.mine_ref, bf16[128,2048]{1,0:T(8,128)(2,1)S(1)} %copy-done, bf16[1536,2048]{1,0:T(8,128)(2,1)S(1)} %get-tuple-element.25.w_ref, bf16[2048,2048]{1,0:T(8,128)(2,1)} %w_hbm.3), custom_call_target="tpu_custom_call" | custom-call | flops 1000000000 | bytes 1048576 | tf_op jit(solution)/shard_map/project/pallas_call | solution.py:451
  41.6 0.0 collective-permute-done.1.other_ref
  41.6 0.0 copy-done.2
  41.7 0.0 copy-done.4
  41.7 0.0 copy-start.9
  41.7 0.0 copy-start.10
  41.7 2.2 %dispatch.1 = (bf16[128,2048]{1,0:T(8,128)(2,1)S(1)}, bf16[1024,2048]{1,0:T(8,128)(2,1)S(1)}) custom-call(bf16[128,1024]{1,0:T(8,128)(2,1)S(1)} %collective-permute-done.1.other_ref, bf16[1536,2048]{1,0:T(8,128)(2,1)S(1)} %get-tuple-element.25.w_ref, bf16[512,2048]{1,0:T(8,128)(2,1)S(1)} %get-tuple-element.27.rest_ref, ...), custom_call_target="tpu_custom_call" | custom-call | flops 2000000000 | bytes 1048576 | tf_op jit(solution)/shard_map/dispatch/pallas_call | solution.py:460
  43.9 0.0 copy-start.5
  43.9 0.0 copy-start.6
  44.0 0.0 copy-start.7
  44.0 0.0 copy-start.8
  44.0 56.3 %all_to_all.15 = bf16[128,8,2048]{2,1,0:T(8,128)(2,1)S(1)} all-to-all(bf16[128,8,2048]{2,1,0:T(8,128)(2,1)S(1)} %bitcast.11), channel_id=1, replica_groups=mesh['sp'=64,'tp'=2] {'sp','tp'}, dimensions={0} | all-to-all | bytes 8388608 | tf_op jit(solution)/shard_map/all_to_all | solution.py:471
  100.3 0.0 copy-done.9
  100.3 0.0 copy-done.10
  100.3 0.0 copy-done.5
  100.3 0.0 copy-done.6
  100.3 0.0 copy-done.7
  100.3 0.0 copy-done.8
  100.3 7.9 %expert.1 = (bf16[1024,2048]{1,0:T(8,128)(2,1)S(1)}, f32[128,2048]{1,0:T(8,128)S(1)}) custom-call(bf16[1024,2048]{1,0:T(8,128)(2,1)S(1)} %bitcast.12, bf16[1,2048,512]{2,1,0:T(8,128)(2,1)S(1)} %copy-done.5, bf16[1,2048,512]{2,1,0:T(8,128)(2,1)S(1)} %copy-done.6, bf16[1,512,2048]{2,1,0:T(8,128)(2,1)S(1)} %copy-done.7, ...), custom_call_target="tpu_custom_call" | custom-call | flops 7000000000 | bytes 1048576 | tf_op jit(solution)/shard_map/expert/pallas_call | solution.py:475
  108.3 0.0 copy-start.1
  108.3 0.0 copy-start.3
  108.3 57.0 %all_to_all.16 = bf16[128,8,2048]{2,1,0:T(8,128)(2,1)S(1)} all-to-all(bf16[128,8,2048]{2,1,0:T(8,128)(2,1)S(1)} %bitcast.13), channel_id=1, replica_groups=mesh['sp'=64,'tp'=2] {'sp','tp'}, dimensions={0} | all-to-all | bytes 8388608 | tf_op jit(solution)/shard_map/all_to_all | solution.py:471
  165.3 0.0 copy-done.1
  165.3 0.0 copy-done.3
  165.3 1.8 %finish.1 = bf16[128,2048]{1,0:T(8,128)(2,1)} custom-call(f32[128,2048]{1,0:T(8,128)S(1)} %get-tuple-element.32.base_ref, bf16[128,1024]{1,0:T(8,128)(2,1)S(1)} %copy-done.1, bf16[1024,2048]{1,0:T(8,128)(2,1)S(1)} %bitcast.10, f32[1,2048]{1,0:T(1,128)S(1)} %bitcast.14), custom_call_target="tpu_custom_call" | custom-call | flops 1000000000 | bytes 1048576 | tf_op jit(solution)/shard_map/finish/pallas_call | solution.py:486
Async XLA Ops:
  0.7 4.7 %collective-permute-start = (bf16[3,1024]{1,0:T(4,128)(2,1)S(1)}, bf16[3,1024]{1,0:T(4,128)(2,1)S(1)}, u32[]{:S(2)}, u32[]{:S(2)}) collective-permute-start(bf16[3,1024]{1,0:T(4,128)(2,1)S(1)} %slice.3), channel_id=1, source_target_pairs={{0,2},{2,4},{4,6},{6,8},{8,10},{10,12},{12,14},{14,16},{16,18},{18... | collective-permute-start | bytes 18440 | tf_op jit(solution)/shard_map/ppermute | solution.py:396
  5.4 0.6 copy-start.11
  11.4 21.1 %all-to-all-start = ((bf16[64,16,128]{2,1,0:T(8,128)(2,1)}), bf16[64,16,128]{2,1,0:T(8,128)(2,1)S(1)}, u32[]{:S(2)}, u32[]{:S(2)}) async-start(bf16[64,16,128]{2,1,0:T(8,128)(2,1)} %get-tuple-element.20), calls=%async_computation | async-start | bytes 524288 | tf_op jit(solution)/shard_map/all_to_all | solution.py:430
  32.5 7.0 %copy-start = (bf16[128,2048]{1,0:T(8,128)(2,1)S(1)}, bf16[128,2048]{1,0:T(8,128)(2,1)}, u32[]{:S(2)}) copy-start(bf16[128,2048]{1,0:T(8,128)(2,1)} %res_ref.1) | copy-start | bytes 1572868
  36.1 5.5 %collective-permute-start.1 = (bf16[128,1024]{1,0:T(8,128)(2,1)S(1)}, bf16[128,1024]{1,0:T(8,128)(2,1)S(1)}, u32[]{:S(2)}, u32[]{:S(2)}) collective-permute-start(bf16[128,1024]{1,0:T(8,128)(2,1)S(1)} %get-tuple-element.24), channel_id=1, source_target_pairs={{0,1},{1,0},{2,3},{3,2},{4,5},{5,4},{6,7},{7,6},{8,9},{9,8},{10,11... | collective-permute-start | bytes 786440 | tf_op jit(solution)/shard_map/ppermute | solution.py:449
  39.4 2.2 %copy-start.2 = (bf16[1024,128]{1,0:T(8,128)(2,1)S(1)}, bf16[1024,128]{1,0:T(8,128)(2,1)}, u32[]{:S(2)}) copy-start(bf16[1024,128]{1,0:T(8,128)(2,1)} %get-tuple-element.29.g_ref) | copy-start | bytes 786436
  39.4 2.2 %copy-start.4 = (f32[2048]{0:T(1024)S(1)}, f32[2048]{0:T(1024)}, u32[]{:S(2)}) copy-start(f32[2048]{0:T(1024)} %param.28) | copy-start | bytes 24580
  41.7 58.6 %copy-start.9 = (bf16[2048,512]{1,0:T(8,128)(2,1)S(1)}, bf16[2048,512]{1,0:T(8,128)(2,1)}, u32[]{:S(2)}) copy-start(bf16[2048,512]{1,0:T(8,128)(2,1)} %sup_ref.1) | copy-start | bytes 6291460
  41.7 58.6 %copy-start.10 = (bf16[512,2048]{1,0:T(8,128)(2,1)S(1)}, bf16[512,2048]{1,0:T(8,128)(2,1)}, u32[]{:S(2)}) copy-start(bf16[512,2048]{1,0:T(8,128)(2,1)} %sdown_ref.1) | copy-start | bytes 6291460
  43.9 56.4 %copy-start.5 = (bf16[1,2048,512]{2,1,0:T(8,128)(2,1)S(1)}, bf16[1,2048,512]{2,1,0:T(8,128)(2,1)}, u32[]{:S(2)}) copy-start(bf16[1,2048,512]{2,1,0:T(8,128)(2,1)} %gate_ref.1) | copy-start | bytes 6291460
  43.9 56.3 %copy-start.6 = (bf16[1,2048,512]{2,1,0:T(8,128)(2,1)S(1)}, bf16[1,2048,512]{2,1,0:T(8,128)(2,1)}, u32[]{:S(2)}) copy-start(bf16[1,2048,512]{2,1,0:T(8,128)(2,1)} %up_ref.1) | copy-start | bytes 6291460
  44.0 56.3 %copy-start.7 = (bf16[1,512,2048]{2,1,0:T(8,128)(2,1)S(1)}, bf16[1,512,2048]{2,1,0:T(8,128)(2,1)}, u32[]{:S(2)}) copy-start(bf16[1,512,2048]{2,1,0:T(8,128)(2,1)} %down_ref.1) | copy-start | bytes 6291460
  44.0 56.3 %copy-start.8 = (bf16[2048,512]{1,0:T(8,128)(2,1)S(1)}, bf16[2048,512]{1,0:T(8,128)(2,1)}, u32[]{:S(2)}) copy-start(bf16[2048,512]{1,0:T(8,128)(2,1)} %sgate_ref.1) | copy-start | bytes 6291460
  108.3 57.0 %copy-start.1 = (bf16[128,1024]{1,0:T(8,128)(2,1)S(1)}, bf16[128,1024]{1,0:T(8,128)(2,1)}, u32[]{:S(2)}) copy-start(bf16[128,1024]{1,0:T(8,128)(2,1)} %get-tuple-element.33.c_ref) | copy-start | bytes 786436
  108.3 57.0 %copy-start.3 = (f32[2048]{0:T(1024)S(1)}, f32[2048]{0:T(1024)}, u32[]{:S(2)}) copy-start(f32[2048]{0:T(1024)} %param.37) | copy-start | bytes 24580

commit v8 on v7

--- a/solution.py
+++ b/solution.py
@@ -32,7 +32,7 @@
         out_specs=out_specs,
         grid=grid,
         scratch_shapes=list(scratch),
-        compiler_params=pltpu.CompilerParams(vmem_limit_bytes=limit * 2**20),
+        compiler_params=pltpu.CompilerParams(vmem_limit_bytes=int(limit * 2**20)),
         cost_estimate=pl.CostEstimate(flops=flops, bytes_accessed=2**20, transcendentals=0),
         name=name,
     )
@@ -84,17 +84,13 @@
 
 
 def scan_kernel(
-    halo_hbm, x_hbm, taps_hbm, rmap_hbm, imap_hbm, rate_hbm, shift_hbm, tot_hbm, run_hbm, edge_hbm,
-    halo_ref, x_ref, taps_ref, rmap_ref, imap_ref, rate_ref, shift_ref, tot_ref, run_ref, edge_ref,
+    halo_ref, small_ref, x_hbm, rmap_hbm, imap_hbm, tot_hbm, run_hbm,
+    x_ref, rmap_ref, imap_ref, tot_ref, run_ref,
     ext, cv, rg, ig, sh, sems, outs,
 ):
     copies = fetch(
         [
             (x_hbm, x_ref),
-            (taps_hbm, taps_ref),
-            (halo_hbm, halo_ref),
-            (shift_hbm, shift_ref),
-            (rate_hbm, rate_ref),
             (rmap_hbm, rmap_ref),
             (imap_hbm, imap_ref),
         ],
@@ -104,10 +100,9 @@
     steps = tokens // LANES
     stride = steps + 8
     heads, width = rmap_ref.shape[:2]
-    reach = taps_ref.shape[0] - 1
+    reach = halo_ref.shape[0]
     pad = 8 - reach
-    for copy in copies[:3]:
-        copy.wait()
+    copies[0].wait()
     for c in range(channels // 128):
         cols = slice(c * 128, (c + 1) * 128)
         x = x_ref[:, cols].astype(F32)
@@ -116,7 +111,7 @@
             if i > 0:
                 ext[c, pl.ds(stride * i, 8), :] = x[steps * i - 8 : steps * i]
             ext[c, pl.ds(stride * i + 8, steps), :] = x[steps * i : steps * (i + 1)]
-        taps = [taps_ref[pl.ds(j, 1), cols].astype(F32) for j in range(reach + 1)]
+        taps = [small_ref[pl.ds(j, 1), cols] for j in range(reach + 1)]
         window = [ext[c, pl.ds(pad + j, LANES, stride=stride), :] for j in range(reach)]
         for t in range(steps):
             window.append(ext[c, pl.ds(8 + t, LANES, stride=stride), :])
@@ -125,18 +120,19 @@
                 total = total + taps[j] * window[j]
             window = window[1:]
             cv[pl.ds(t * LANES, LANES), cols] = total.astype(BF16).astype(F32)
-    for copy in copies[3:]:
+    for copy in copies[1:]:
         copy.wait()
     for k in range(heads):
         cols = slice(k * width, (k + 1) * width)
         block = cv[:, cols].astype(BF16)
         rg[:, cols] = jnp.dot(block, rmap_ref[k], preferred_element_type=F32)
         ig[:, cols] = jnp.dot(block, imap_ref[k], preferred_element_type=F32)
-    full = jnp.concatenate([shift_ref[...], jnp.zeros((128 - heads, tokens), F32)], axis=0)
+    lines = [small_ref[pl.ds(reach + 2, 1), k * tokens : (k + 1) * tokens] for k in range(heads)]
+    full = jnp.concatenate(lines + [jnp.zeros((128 - heads, tokens), F32)], axis=0)
     full = jnp.transpose(full)
     for i in range(LANES):
         sh[pl.ds(stride * i, steps), :] = full[steps * i : steps * (i + 1)]
-    logit = -rate_ref[...]
+    logit = -small_ref[pl.ds(reach + 1, 1), :]
     slope = -RATE_C * (jnp.maximum(logit, 0.0) + log1p_unit(jnp.exp(-jnp.abs(logit))))
 
     def step(t, carry):
@@ -184,14 +180,19 @@
             lane = slice(j * 128, (j + 1) * 128)
             ends[0].append(jnp.log(jnp.maximum(a[LANES - 1 :, lane], TINY)))
             ends[1].append(h[LANES - 1 :, lane])
-        edge_ref[0, :, cols] = jnp.where(row >= 1, pltpu.roll(h, 1, 0), 0.0)
-        edge_ref[1, :, cols] = jnp.where(row >= 1, pltpu.roll(a, 1, 0), 1.0)
+        enter = jnp.where(row >= 1, pltpu.roll(h, 1, 0), 0.0)
+        scale = jnp.where(row >= 1, pltpu.roll(a, 1, 0), 1.0)
+        for j in range(width // 128):
+            lane = slice(j * 128, (j + 1) * 128)
+            run_ref[0, k * (width // 128) + j, pl.ds(tokens, LANES), :] = enter[:, lane]
+            run_ref[1, k * (width // 128) + j, pl.ds(tokens, LANES), :] = scale[:, lane]
     both = jnp.concatenate(ends[0] + ends[1], axis=0).astype(BF16)
     for i in range(tot_ref.shape[0]):
         tot_ref[i] = both
+    rows = pl.ds(tokens, LANES)
     sent += [
         pltpu.make_async_copy(tot_ref, tot_hbm, outs.at[4]),
-        pltpu.make_async_copy(edge_ref, edge_hbm, outs.at[5]),
+        pltpu.make_async_copy(run_ref.at[:, :, rows, :], run_hbm.at[:, :, rows, :], outs.at[5]),
     ]
     for copy in sent[4:]:
         copy.start()
@@ -200,8 +201,8 @@
 
 
 def side_kernel(
-    gate_hbm, routes_hbm, weight_hbm, run_hbm, edge_hbm, mixed_hbm, g_hbm, c_hbm,
-    gate_ref, routes_ref, weight_ref, run_ref, edge_ref, mixed_ref, g_ref, c_ref, sems, outs,
+    gate_hbm, routes_hbm, weight_hbm, run_hbm, mixed_hbm, g_hbm, c_hbm,
+    gate_ref, routes_ref, weight_ref, run_ref, mixed_ref, g_ref, c_ref, sems, outs,
 ):
     copies = fetch(
         [
@@ -209,7 +210,6 @@
             (weight_hbm, weight_ref),
             (gate_hbm, gate_ref),
             (run_hbm, run_ref),
-            (edge_hbm, edge_ref),
         ],
         sems,
     )
@@ -228,12 +228,13 @@
         chunk = i // per
         source = pl.ds(chunk + (i % per) * (block * LANES), block, stride=LANES)
         gate = jax.nn.gelu(gate_ref[rows, :].astype(F32), approximate=True)
-        enter, scale = edge_ref[0, pl.ds(chunk, 1), :], edge_ref[1, pl.ds(chunk, 1), :]
+        edge = pl.ds(tokens + chunk, 1)
         for c in range(channels // 128):
             cols = slice(c * 128, (c + 1) * 128)
             run = run_ref[1, c, source, :]
-            mixed_ref[0, rows, cols] = (run_ref[0, c, source, :] + run * enter[:, cols]) * gate[:, cols]
-            mixed_ref[1, rows, cols] = run * scale[:, cols] * gate[:, cols]
+            own = run_ref[0, c, source, :] + run * run_ref[0, c, edge, :]
+            mixed_ref[0, rows, cols] = own * gate[:, cols]
+            mixed_ref[1, rows, cols] = run * run_ref[1, c, edge, :] * gate[:, cols]
         return 0
 
     pairs = [(g_ref, g_hbm), (c_ref, c_hbm)]
@@ -415,25 +416,32 @@
             limit=62,
         )(*operands)
 
-    totals, local, edge = staged(
+    small = jnp.concatenate(
+        [conv_taps.astype(F32), rate_logit[None], decay_shift.T.reshape(1, -1)], axis=0
+    )
+    made = (
+        shape((sp, 2 * LANES, 128), BF16),
+        shape((2, channels // 128, tokens + LANES, 128), F32),
+    )
+    held = (conv_in, recur_map, input_map) + made
+    totals, local = call(
         scan_kernel,
-        (before, conv_in, conv_taps, recur_map, input_map, rate_logit[None], decay_shift.T),
-        (
-            shape((sp, 2 * LANES, 128), BF16),
-            shape((2, channels // 128, tokens, 128), F32),
-            shape((2, LANES, channels), F32),
-        ),
+        made,
+        [VMEM] * 2 + [HBM] * 3,
         10**9,
-        [lanes, big, big, big, pltpu.VMEM((apart, 128), F32), sem((7,)), sem((6,))],
-        "scan",
-    )
+        [pltpu.VMEM(x.shape, x.dtype) for x in held]
+        + [lanes, big, big, big, pltpu.VMEM((apart, 128), F32), sem((3,)), sem((6,))],
+        name="scan",
+        out_specs=(HBM,) * 2,
+        limit=53.5,
+    )(before, small, conv_in, recur_map, input_map)
     seen = lax.all_to_all(totals, "sp", 0, 0, tiled=True)
     parts, g, c = staged(
         side_kernel,
-        (gate_pre, routes.T, route_weight.T, local, edge),
+        (gate_pre, routes.T, route_weight.T, local),
         (padded, shape((slots, rows), BF16), shape((rows, slots), BF16)),
         10**10,
-        [sem((5,)), sem((6,))],
+        [sem((4,)), sem((6,))],
         "side",
     )
     piece = shape((rows, channels), BF16)

time: 167 us -> 167 us (level)
    pallas_call x2 -> x1, Pallas kernels: 8.86 us -> 3.52 us  [staged(): call(kernel, made, [HBM] * len(operands), flops, held + scratch, name=nam...]
    pallas_call x0 -> x1, Pallas kernels: none -> 5.3 us  [on_device(): call(scan_kernel, made, [VMEM] * 2 + [HBM] * 3, 10 ** 9, [pltpu.VMEM(x.sh...]
  transfers between devices with their start and end apart: 3 -> 3, of which waited for: 2 -> 1; matrix products, arithmetic and copies ran while one was open for 0% -> 1% of each run, Pallas kernels for 3% -> 3%
where the time goes in v8:
time: 167 us; the launch traced here: 166 us
  blocking collectives  113 us (68%)
  Pallas kernels  26.6 us (16%)
  starting transfers between devices  17.5 us (10%)
  waiting for transfers between devices  5.95 us (4%)
    all_to_all x2, blocking collectives, exchanged(): x = lax.all_to_all(x, ('sp', 'tp'), split_axis=0, concat_axis=0, tiled=True)  113 us
    all_to_all x1, starting transfers between devices, on_device(): seen = lax.all_to_all(totals, 'sp', 0, 0, tiled=True)  10.9 us
    pallas_call x1, Pallas kernels, on_device(): call(expert_kernel, (shape((slots, model), BF16), wide), [VMEM] * 8, 7 *...  7.93 us
    all_to_all x1, waiting for transfers between devices, on_device(): seen = lax.all_to_all(totals, 'sp', 0, 0, tiled=True)  5.95 us
    pallas_call x1, Pallas kernels, on_device(): call(scan_kernel, made, [VMEM] * 2 + [HBM] * 3, 10 ** 9, [pltpu.VMEM(x.sh...  5.3 us
    ppermute x1, starting transfers between devices, on_device(): lax.ppermute(conv_in[tokens - reach:], 'sp', [(i, i + 1) for i in range(s...  3.92 us
    pallas_call x1, Pallas kernels, on_device(): call(mix_kernel, (piece, piece, shape((3 * channels // 2, model), BF16)),...  3.61 us
    pallas_call x1, Pallas kernels, staged(): call(kernel, made, [HBM] * len(operands), flops, held + scratch, name=nam...  3.52 us
  transfers between devices with their start and end apart: 3, of which 1 were waited for; matrix products, arithmetic and copies ran while one was open for 1% of the time, Pallas kernels for 3%

profile of v8, /device:TPU:1, one launch (start us, length us, event | category | flops | bytes accessed | tf_op | source)
XLA Modules:
  0.0 166.4 jit_solution(2595209864789339228)
XLA Ops:
  0.0 0.7 slice.3
  0.7 3.9 %collective-permute-start = (bf16[3,1024]{1,0:T(4,128)(2,1)S(1)}, bf16[3,1024]{1,0:T(4,128)(2,1)S(1)}, u32[]{:S(2)}, u32[]{:S(2)}) collective-permute-start(bf16[3,1024]{1,0:T(4,128)(2,1)S(1)} %slice.3), channel_id=1, source_target_pairs={{0,2},{2,4},{4,6},{6,8},{8,10},{10,12},{12,14},{14,16},{16,18},{18... | collective-permute-start | bytes 18440 | tf_op jit(solution)/shard_map/ppermute | solution.py:397
  4.7 0.7 copy.20
  5.3 0.7 convert_element_type.3
  6.0 0.7 pad_maximum_fusion.small_ref
  6.8 0.0 collective-permute-done.halo_ref
  6.8 5.3 %scan.1 = (bf16[64,16,128]{2,1,0:T(8,128)(2,1)}, f32[2,8,264,128]{3,2,1,0:T(8,128)}) custom-call(bf16[3,1024]{1,0:T(4,128)(2,1)S(1)} %collective-permute-done.halo_ref, f32[6,1024]{1,0:T(8,128)S(1)} %pad_maximum_fusion.small_ref, bf16[256,1024]{1,0:T(8,128)(2,1)} %x_hbm.1, bf16[4,256,256]{2,1,0:T(8,128)(2,1)} %rmap_hbm.1, bf16[4,256,256]{2,1,0:T(8,128)(2,1)} %imap_hbm.1), custom_call_target="tpu_custom_call" | custom-call | flops 1000000000 | bytes 1048576 | tf_op jit(solution)/shard_map/scan/pallas_call | solution.py:427
  12.1 10.9 %all-to-all-start = ((bf16[64,16,128]{2,1,0:T(8,128)(2,1)}), bf16[64,16,128]{2,1,0:T(8,128)(2,1)S(1)}, u32[]{:S(2)}, u32[]{:S(2)}) async-start(bf16[64,16,128]{2,1,0:T(8,128)(2,1)} %get-tuple-element.19), calls=%async_computation | async-start | bytes 524288 | tf_op jit(solution)/shard_map/all_to_all | solution.py:438
  22.9 3.5 %side.1 = (f32[8,256,1024]{2,1,0:T(8,128)}, bf16[1024,128]{1,0:T(8,128)(2,1)}, bf16[128,1024]{1,0:T(8,128)(2,1)}) custom-call(bf16[256,1024]{1,0:T(8,128)(2,1)} %gate_hbm.1, s32[4,128]{1,0:T(4,128)} %bitcast.22, f32[4,128]{1,0:T(4,128)} %bitcast.23, f32[2,8,264,128]{3,2,1,0:T(8,128)} %get-tuple-element.20.run_hbm), custom_call_target="tpu_custom_call" | custom-call | flops 10000000000 | bytes 1048576 | tf_op jit(solution)/shard_map/side/pallas_call | solution.py:408
  26.5 5.9 %all-to-all-done.seen_ref = bf16[64,16,128]{2,1,0:T(8,128)(2,1)S(1)} async-done(((bf16[64,16,128]{2,1,0:T(8,128)(2,1)}), bf16[64,16,128]{2,1,0:T(8,128)(2,1)S(1)}, u32[]{:S(2)}, u32[]{:S(2)}) %all-to-all-start) | async-done | bytes 262176 | tf_op jit(solution)/shard_map/all_to_all | solution.py:438
  32.4 0.0 copy-start
  32.4 3.6 %mix.1 = (bf16[128,1024]{1,0:T(8,128)(2,1)S(1)}, bf16[128,1024]{1,0:T(8,128)(2,1)S(1)}, bf16[1536,2048]{1,0:T(8,128)(2,1)S(1)}) custom-call(bf16[64,16,128]{2,1,0:T(8,128)(2,1)S(1)} %all-to-all-done.seen_ref, f32[8,256,1024]{2,1,0:T(8,128)} %get-tuple-element.21.mixed_hbm, bf16[2048,2048]{1,0:T(8,128)(2,1)} %w_hbm.3), custom_call_target="tpu_custom_call" | custom-call | flops 100000000 | bytes 1048576 | tf_op jit(solution)/shard_map/mix/pallas_call | solution.py:448
  36.0 2.8 %collective-permute-start.1 = (bf16[128,1024]{1,0:T(8,128)(2,1)S(1)}, bf16[128,1024]{1,0:T(8,128)(2,1)S(1)}, u32[]{:S(2)}, u32[]{:S(2)}) collective-permute-start(bf16[128,1024]{1,0:T(8,128)(2,1)S(1)} %get-tuple-element.22), channel_id=1, source_target_pairs={{0,1},{1,0},{2,3},{3,2},{4,5},{5,4},{6,7},{7,6},{8,9},{9,8},{10,11... | collective-permute-start | bytes 786440 | tf_op jit(solution)/shard_map/ppermute | solution.py:457
  38.8 0.0 copy-done
  38.8 0.0 copy-start.2
  38.8 0.0 copy-start.4
  38.8 2.2 %project.1 = (f32[128,2048]{1,0:T(8,128)S(1)}, bf16[512,2048]{1,0:T(8,128)(2,1)S(1)}) custom-call(bf16[128,1024]{1,0:T(8,128)(2,1)S(1)} %get-tuple-element.24.mine_ref, bf16[128,2048]{1,0:T(8,128)(2,1)S(1)} %copy-done, bf16[1536,2048]{1,0:T(8,128)(2,1)S(1)} %get-tuple-element.23.w_ref, bf16[2048,2048]{1,0:T(8,128)(2,1)} %w_hbm.3), custom_call_target="tpu_custom_call" | custom-call | flops 1000000000 | bytes 1048576 | tf_op jit(solution)/shard_map/project/pallas_call | solution.py:459
  41.0 0.0 collective-permute-done.1.other_ref
  41.0 0.0 copy-done.2
  41.0 0.0 copy-done.4
  41.0 0.0 copy-start.9
  41.0 0.0 copy-start.10
  41.1 2.2 %dispatch.1 = (bf16[128,2048]{1,0:T(8,128)(2,1)S(1)}, bf16[1024,2048]{1,0:T(8,128)(2,1)S(1)}) custom-call(bf16[128,1024]{1,0:T(8,128)(2,1)S(1)} %collective-permute-done.1.other_ref, bf16[1536,2048]{1,0:T(8,128)(2,1)S(1)} %get-tuple-element.23.w_ref, bf16[512,2048]{1,0:T(8,128)(2,1)S(1)} %get-tuple-element.25.rest_ref, ...), custom_call_target="tpu_custom_call" | custom-call | flops 2000000000 | bytes 1048576 | tf_op jit(solution)/shard_map/dispatch/pallas_call | solution.py:468
  43.3 0.0 copy-start.5
  43.3 0.0 copy-start.6
  43.3 0.0 copy-start.7
  43.3 0.0 copy-start.8
  43.4 56.3 %all_to_all.15 = bf16[128,8,2048]{2,1,0:T(8,128)(2,1)S(1)} all-to-all(bf16[128,8,2048]{2,1,0:T(8,128)(2,1)S(1)} %bitcast.14), channel_id=1, replica_groups=mesh['sp'=64,'tp'=2] {'sp','tp'}, dimensions={0} | all-to-all | bytes 8388608 | tf_op jit(solution)/shard_map/all_to_all | solution.py:479
  99.6 0.0 copy-done.9
  99.6 0.0 copy-done.10
  99.7 0.0 copy-done.5
  99.7 0.0 copy-done.6
  99.7 0.0 copy-done.7
  99.7 0.0 copy-done.8
  99.7 7.9 %expert.1 = (bf16[1024,2048]{1,0:T(8,128)(2,1)S(1)}, f32[128,2048]{1,0:T(8,128)S(1)}) custom-call(bf16[1024,2048]{1,0:T(8,128)(2,1)S(1)} %bitcast.15, bf16[1,2048,512]{2,1,0:T(8,128)(2,1)S(1)} %copy-done.5, bf16[1,2048,512]{2,1,0:T(8,128)(2,1)S(1)} %copy-done.6, bf16[1,512,2048]{2,1,0:T(8,128)(2,1)S(1)} %copy-done.7, ...), custom_call_target="tpu_custom_call" | custom-call | flops 7000000000 | bytes 1048576 | tf_op jit(solution)/shard_map/expert/pallas_call | solution.py:483
  107.6 0.0 copy-start.1
  107.6 0.0 copy-start.3
  107.6 57.0 %all_to_all.16 = bf16[128,8,2048]{2,1,0:T(8,128)(2,1)S(1)} all-to-all(bf16[128,8,2048]{2,1,0:T(8,128)(2,1)S(1)} %bitcast.16), channel_id=1, replica_groups=mesh['sp'=64,'tp'=2] {'sp','tp'}, dimensions={0} | all-to-all | bytes 8388608 | tf_op jit(solution)/shard_map/all_to_all | solution.py:479
  164.6 0.0 copy-done.1
  164.6 0.0 copy-done.3
  164.6 1.8 %finish.1 = bf16[128,2048]{1,0:T(8,128)(2,1)} custom-call(f32[128,2048]{1,0:T(8,128)S(1)} %get-tuple-element.30.base_ref, bf16[128,1024]{1,0:T(8,128)(2,1)S(1)} %copy-done.1, bf16[1024,2048]{1,0:T(8,128)(2,1)S(1)} %bitcast.13, f32[1,2048]{1,0:T(1,128)S(1)} %bitcast.17), custom_call_target="tpu_custom_call" | custom-call | flops 1000000000 | bytes 1048576 | tf_op jit(solution)/shard_map/finish/pallas_call | solution.py:494
Async XLA Ops:
  0.7 6.0 %collective-permute-start = (bf16[3,1024]{1,0:T(4,128)(2,1)S(1)}, bf16[3,1024]{1,0:T(4,128)(2,1)S(1)}, u32[]{:S(2)}, u32[]{:S(2)}) collective-permute-start(bf16[3,1024]{1,0:T(4,128)(2,1)S(1)} %slice.3), channel_id=1, source_target_pairs={{0,2},{2,4},{4,6},{6,8},{8,10},{10,12},{12,14},{14,16},{16,18},{18... | collective-permute-start | bytes 18440 | tf_op jit(solution)/shard_map/ppermute | solution.py:397
  12.1 20.3 %all-to-all-start = ((bf16[64,16,128]{2,1,0:T(8,128)(2,1)}), bf16[64,16,128]{2,1,0:T(8,128)(2,1)S(1)}, u32[]{:S(2)}, u32[]{:S(2)}) async-start(bf16[64,16,128]{2,1,0:T(8,128)(2,1)} %get-tuple-element.19), calls=%async_computation | async-start | bytes 524288 | tf_op jit(solution)/shard_map/all_to_all | solution.py:438
  32.4 6.4 %copy-start = (bf16[128,2048]{1,0:T(8,128)(2,1)S(1)}, bf16[128,2048]{1,0:T(8,128)(2,1)}, u32[]{:S(2)}) copy-start(bf16[128,2048]{1,0:T(8,128)(2,1)} %res_ref.1) | copy-start | bytes 1572868
  36.0 5.0 %collective-permute-start.1 = (bf16[128,1024]{1,0:T(8,128)(2,1)S(1)}, bf16[128,1024]{1,0:T(8,128)(2,1)S(1)}, u32[]{:S(2)}, u32[]{:S(2)}) collective-permute-start(bf16[128,1024]{1,0:T(8,128)(2,1)S(1)} %get-tuple-element.22), channel_id=1, source_target_pairs={{0,1},{1,0},{2,3},{3,2},{4,5},{5,4},{6,7},{7,6},{8,9},{9,8},{10,11... | collective-permute-start | bytes 786440 | tf_op jit(solution)/shard_map/ppermute | solution.py:457
  38.8 2.2 %copy-start.2 = (bf16[1024,128]{1,0:T(8,128)(2,1)S(1)}, bf16[1024,128]{1,0:T(8,128)(2,1)}, u32[]{:S(2)}) copy-start(bf16[1024,128]{1,0:T(8,128)(2,1)} %get-tuple-element.27.g_ref) | copy-start | bytes 786436
  38.8 2.2 %copy-start.4 = (f32[2048]{0:T(1024)S(1)}, f32[2048]{0:T(1024)}, u32[]{:S(2)}) copy-start(f32[2048]{0:T(1024)} %param.28) | copy-start | bytes 24580
  41.0 58.6 %copy-start.9 = (bf16[2048,512]{1,0:T(8,128)(2,1)S(1)}, bf16[2048,512]{1,0:T(8,128)(2,1)}, u32[]{:S(2)}) copy-start(bf16[2048,512]{1,0:T(8,128)(2,1)} %sup_ref.1) | copy-start | bytes 6291460
  41.0 58.6 %copy-start.10 = (bf16[512,2048]{1,0:T(8,128)(2,1)S(1)}, bf16[512,2048]{1,0:T(8,128)(2,1)}, u32[]{:S(2)}) copy-start(bf16[512,2048]{1,0:T(8,128)(2,1)} %sdown_ref.1) | copy-start | bytes 6291460
  43.3 56.4 %copy-start.5 = (bf16[1,2048,512]{2,1,0:T(8,128)(2,1)S(1)}, bf16[1,2048,512]{2,1,0:T(8,128)(2,1)}, u32[]{:S(2)}) copy-start(bf16[1,2048,512]{2,1,0:T(8,128)(2,1)} %gate_ref.1) | copy-start | bytes 6291460
  43.3 56.3 %copy-start.6 = (bf16[1,2048,512]{2,1,0:T(8,128)(2,1)S(1)}, bf16[1,2048,512]{2,1,0:T(8,128)(2,1)}, u32[]{:S(2)}) copy-start(bf16[1,2048,512]{2,1,0:T(8,128)(2,1)} %up_ref.1) | copy-start | bytes 6291460
  43.3 56.3 %copy-start.7 = (bf16[1,512,2048]{2,1,0:T(8,128)(2,1)S(1)}, bf16[1,512,2048]{2,1,0:T(8,128)(2,1)}, u32[]{:S(2)}) copy-start(bf16[1,512,2048]{2,1,0:T(8,128)(2,1)} %down_ref.1) | copy-start | bytes 6291460
  43.3 56.3 %copy-start.8 = (bf16[2048,512]{1,0:T(8,128)(2,1)S(1)}, bf16[2048,512]{1,0:T(8,128)(2,1)}, u32[]{:S(2)}) copy-start(bf16[2048,512]{1,0:T(8,128)(2,1)} %sgate_ref.1) | copy-start | bytes 6291460
  107.6 57.0 %copy-start.1 = (bf16[128,1024]{1,0:T(8,128)(2,1)S(1)}, bf16[128,1024]{1,0:T(8,128)(2,1)}, u32[]{:S(2)}) copy-start(bf16[128,1024]{1,0:T(8,128)(2,1)} %get-tuple-element.31.c_ref) | copy-start | bytes 786436
  107.6 57.0 %copy-start.3 = (f32[2048]{0:T(1024)S(1)}, f32[2048]{0:T(1024)}, u32[]{:S(2)}) copy-start(f32[2048]{0:T(1024)} %param.37) | copy-start | bytes 24580

commit v9 on v8

--- a/solution.py
+++ b/solution.py
@@ -127,7 +127,7 @@
         block = cv[:, cols].astype(BF16)
         rg[:, cols] = jnp.dot(block, rmap_ref[k], preferred_element_type=F32)
         ig[:, cols] = jnp.dot(block, imap_ref[k], preferred_element_type=F32)
-    lines = [small_ref[pl.ds(reach + 2, 1), k * tokens : (k + 1) * tokens] for k in range(heads)]
+    lines = [small_ref[pl.ds(reach + 2 + k, 1), :tokens] for k in range(heads)]
     full = jnp.concatenate(lines + [jnp.zeros((128 - heads, tokens), F32)], axis=0)
     full = jnp.transpose(full)
     for i in range(LANES):
@@ -263,10 +263,7 @@
     for j in range(4):
         rows = pl.ds(j * (tokens // 4), tokens // 4)
         pairs.append((mixed_hbm.at[pl.ds(0, 2), rows, :], mixed_ref.at[:, rows, :]))
-    for j in range(3):
-        at = (side if j < 2 else 1 - side) * channels + (j % 2) * strip
-        at = pl.multiple_of(at, strip)
-        pairs.append((w_hbm.at[pl.ds(at, strip), :], w_ref.at[pl.ds(j * strip, strip), :]))
+    pairs.append((w_hbm.at[pl.ds(pl.multiple_of(side * channels, strip), strip), :], w_ref))
     copies = fetch(pairs, sems)
     carried = jnp.zeros((LANES, 128), F32)
     for i in range(seen_ref.shape[0]):
@@ -326,24 +323,26 @@
         c_ref[:, cols] = jnp.transpose(jnp.where(chosen, to_slots(weight), 0.0)).astype(BF16)
 
 
-def project_kernel(mine_ref, res_ref, w_ref, w_hbm, out_ref, rest_ref, sems):
+def project_kernel(mine_ref, res_ref, w_ref, w_hbm, out_ref, rest_ref, own_ref, sems):
     depth = mine_ref.shape[1]
     half = depth // 2
-    at = pl.multiple_of((1 - lax.axis_index("tp")) * depth + half, half)
-    copies = fetch([(w_hbm.at[pl.ds(at, half), :], rest_ref)], sems)
+    side = lax.axis_index("tp")
+    pairs = [(w_hbm.at[pl.ds(pl.multiple_of(side * depth + half, half), half), :], own_ref)]
+    for j in range(2):
+        at = pl.multiple_of((1 - side) * depth + j * half, half)
+        pairs.append((w_hbm.at[pl.ds(at, half), :], rest_ref.at[pl.ds(j * half, half), :]))
+    copies = fetch(pairs, sems)
     out_ref[...] = ALPHA * res_ref[...].astype(F32) + jnp.dot(
-        mine_ref[...], w_ref[:depth], preferred_element_type=F32
+        mine_ref[:, :half], w_ref[...], preferred_element_type=F32
     )
     copies[0].wait()
-
-
-def dispatch_kernel(other_ref, w_ref, rest_ref, acc_ref, gain_ref, g_ref, normed_ref, out_ref):
-    depth = other_ref.shape[1]
-    values = (
-        acc_ref[...]
-        + jnp.dot(other_ref[:, : depth // 2], w_ref[depth:], preferred_element_type=F32)
-        + jnp.dot(other_ref[:, depth // 2 :], rest_ref[...], preferred_element_type=F32)
-    )
+    out_ref[...] += jnp.dot(mine_ref[:, half:], own_ref[...], preferred_element_type=F32)
+    for copy in copies[1:]:
+        copy.wait()
+
+
+def dispatch_kernel(other_ref, rest_ref, acc_ref, gain_ref, g_ref, normed_ref, out_ref):
+    values = acc_ref[...] + jnp.dot(other_ref[...], rest_ref[...], preferred_element_type=F32)
     normed = layer_norm(values, gain_ref[...]).astype(BF16)
     normed_ref[...] = normed
 
@@ -417,7 +416,12 @@
         )(*operands)
 
     small = jnp.concatenate(
-        [conv_taps.astype(F32), rate_logit[None], decay_shift.T.reshape(1, -1)], axis=0
+        [
+            conv_taps.astype(F32),
+            rate_logit[None],
+            jnp.pad(decay_shift.T, ((0, 0), (0, channels - tokens))),
+        ],
+        axis=0,
     )
     made = (
         shape((sp, 2 * LANES, 128), BF16),
@@ -447,32 +451,32 @@
     piece = shape((rows, channels), BF16)
     mine, theirs, most = call(
         mix_kernel,
-        (piece, piece, shape((3 * channels // 2, model), BF16)),
+        (piece, piece, shape((channels // 2, model), BF16)),
         [VMEM, HBM, HBM],
         10**8,
-        [pltpu.VMEM((2, tokens, channels), F32), sem((7,))],
+        [pltpu.VMEM((2, tokens, channels), F32), sem((5,))],
         name="mix",
-        limit=44,
+        limit=48,
     )(seen, parts, out_weight)
     other = lax.ppermute(theirs, "tp", [(0, 1), (1, 0)])
     wide = shape((rows, model), F32)
     acc, rest = call(
         project_kernel,
-        (wide, shape((channels // 2, model), BF16)),
+        (wide, shape((channels, model), BF16)),
         [VMEM, VMEM, VMEM, HBM],
         10**9,
-        [sem((1,))],
+        [pltpu.VMEM((channels // 2, model), BF16), sem((3,))],
         name="project",
-        limit=40,
+        limit=41,
     )(mine, residual, most, out_weight)
     normed, outgoing = call(
         dispatch_kernel,
         (shape((rows, model), BF16), shape((slots, model), BF16)),
-        [VMEM] * 6,
+        [VMEM] * 5,
         2 * 10**9,
         name="dispatch",
         limit=24,
-    )(other, most, rest, acc, gain_mix[None], g)
+    )(other, rest, acc, gain_mix[None], g)
 
     def exchanged(x):
         x = x.reshape(experts, CAP, model)

time: 167 us -> 166 us (level)
  transfers between devices with their start and end apart: 3 -> 3, of which waited for: 1 -> 1; matrix products, arithmetic and copies ran while one was open for 1% -> 1% of each run, Pallas kernels for 3% -> 4%
where the time goes in v9:
time: 166 us
  blocking collectives  113 us (68%)
  Pallas kernels  26.1 us (16%)
  starting transfers between devices  18.2 us (11%)
  waiting for transfers between devices  5.95 us (4%)
    all_to_all x2, blocking collectives, exchanged(): x = lax.all_to_all(x, ('sp', 'tp'), split_axis=0, concat_axis=0, tiled=True)  113 us
    all_to_all x1, starting transfers between devices, on_device(): seen = lax.all_to_all(totals, 'sp', 0, 0, tiled=True)  11 us
    pallas_call x1, Pallas kernels, on_device(): call(expert_kernel, (shape((slots, model), BF16), wide), [VMEM] * 8, 7 *...  7.93 us
    all_to_all x1, waiting for transfers between devices, on_device(): seen = lax.all_to_all(totals, 'sp', 0, 0, tiled=True)  5.94 us
    pallas_call x1, Pallas kernels, on_device(): call(scan_kernel, made, [VMEM] * 2 + [HBM] * 3, 10 ** 9, [pltpu.VMEM(x.sh...  5.3 us
    ppermute x1, starting transfers between devices, on_device(): lax.ppermute(conv_in[tokens - reach:], 'sp', [(i, i + 1) for i in range(s...  3.92 us
    pallas_call x1, Pallas kernels, staged(): call(kernel, made, [HBM] * len(operands), flops, held + scratch, name=nam...  3.52 us
    ppermute x1, starting transfers between devices, on_device(): other = lax.ppermute(theirs, 'tp', [(0, 1), (1, 0)])  3.32 us
  transfers between devices with their start and end apart: 3, of which 1 were waited for; matrix products, arithmetic and copies ran while one was open for 1% of the time, Pallas kernels for 4%

profile of v9, /device:TPU:1, one launch (start us, length us, event | category | flops | bytes accessed | tf_op | source)
XLA Modules:
  0.0 165.9 jit_solution(7646240045899008560)
XLA Ops:
  0.0 0.7 slice.3
  0.7 3.9 %collective-permute-start = (bf16[3,1024]{1,0:T(4,128)(2,1)S(1)}, bf16[3,1024]{1,0:T(4,128)(2,1)S(1)}, u32[]{:S(2)}, u32[]{:S(2)}) collective-permute-start(bf16[3,1024]{1,0:T(4,128)(2,1)S(1)} %slice.3), channel_id=1, source_target_pairs={{0,2},{2,4},{4,6},{6,8},{8,10},{10,12},{12,14},{14,16},{16,18},{18... | collective-permute-start | bytes 18440 | tf_op jit(solution)/shard_map/ppermute | solution.py:396
  4.7 0.7 convert_element_type.5
  5.4 0.7 select_maximum_fusion.small_ref
  6.1 0.0 collective-permute-done.halo_ref
  6.1 5.3 %scan.1 = (bf16[64,16,128]{2,1,0:T(8,128)(2,1)}, f32[2,8,264,128]{3,2,1,0:T(8,128)}) custom-call(bf16[3,1024]{1,0:T(4,128)(2,1)S(1)} %collective-permute-done.halo_ref, f32[9,1024]{1,0:T(8,128)S(1)} %select_maximum_fusion.small_ref, bf16[256,1024]{1,0:T(8,128)(2,1)} %x_hbm.1, bf16[4,256,256]{2,1,0:T(8,128)(2,1)} %rmap_hbm.1, bf16[4,256,256]{2,1,0:T(8,128)(2,1)} %imap_hbm.1), custom_call_target="tpu_custom_call" | custom-call | flops 1000000000 | bytes 1048576 | tf_op jit(solution)/shard_map/scan/pallas_call | solution.py:431
  11.4 11.0 %all-to-all-start = ((bf16[64,16,128]{2,1,0:T(8,128)(2,1)}), bf16[64,16,128]{2,1,0:T(8,128)(2,1)S(1)}, u32[]{:S(2)}, u32[]{:S(2)}) async-start(bf16[64,16,128]{2,1,0:T(8,128)(2,1)} %get-tuple-element.19), calls=%async_computation | async-start | bytes 524288 | tf_op jit(solution)/shard_map/all_to_all | solution.py:442
  22.4 3.5 %side.1 = (f32[8,256,1024]{2,1,0:T(8,128)}, bf16[1024,128]{1,0:T(8,128)(2,1)}, bf16[128,1024]{1,0:T(8,128)(2,1)}) custom-call(bf16[256,1024]{1,0:T(8,128)(2,1)} %gate_hbm.1, s32[4,128]{1,0:T(4,128)} %bitcast.18, f32[4,128]{1,0:T(4,128)} %bitcast.19, f32[2,8,264,128]{3,2,1,0:T(8,128)} %get-tuple-element.20.run_hbm), custom_call_target="tpu_custom_call" | custom-call | flops 10000000000 | bytes 1048576 | tf_op jit(solution)/shard_map/side/pallas_call | solution.py:407
  25.9 5.9 %all-to-all-done.seen_ref = bf16[64,16,128]{2,1,0:T(8,128)(2,1)S(1)} async-done(((bf16[64,16,128]{2,1,0:T(8,128)(2,1)}), bf16[64,16,128]{2,1,0:T(8,128)(2,1)S(1)}, u32[]{:S(2)}, u32[]{:S(2)}) %all-to-all-start) | async-done | bytes 262176 | tf_op jit(solution)/shard_map/all_to_all | solution.py:442
  31.9 0.0 copy-start
  31.9 2.3 %mix.1 = (bf16[128,1024]{1,0:T(8,128)(2,1)S(1)}, bf16[128,1024]{1,0:T(8,128)(2,1)S(1)}, bf16[512,2048]{1,0:T(8,128)(2,1)S(1)}) custom-call(bf16[64,16,128]{2,1,0:T(8,128)(2,1)S(1)} %all-to-all-done.seen_ref, f32[8,256,1024]{2,1,0:T(8,128)} %get-tuple-element.21.mixed_hbm, bf16[2048,2048]{1,0:T(8,128)(2,1)} %w_hbm.3), custom_call_target="tpu_custom_call" | custom-call | flops 100000000 | bytes 1048576 | tf_op jit(solution)/shard_map/mix/pallas_call | solution.py:452
  34.2 3.3 %collective-permute-start.1 = (bf16[128,1024]{1,0:T(8,128)(2,1)S(1)}, bf16[128,1024]{1,0:T(8,128)(2,1)S(1)}, u32[]{:S(2)}, u32[]{:S(2)}) collective-permute-start(bf16[128,1024]{1,0:T(8,128)(2,1)S(1)} %get-tuple-element.22), channel_id=1, source_target_pairs={{0,1},{1,0},{2,3},{3,2},{4,5},{5,4},{6,7},{7,6},{8,9},{9,8},{10,11... | collective-permute-start | bytes 786440 | tf_op jit(solution)/shard_map/ppermute | solution.py:461
  37.5 0.0 copy-done
  37.5 0.0 copy-start.9
  37.5 0.0 copy-start.10
  37.5 2.9 %project.1 = (f32[128,2048]{1,0:T(8,128)S(1)}, bf16[1024,2048]{1,0:T(8,128)(2,1)S(1)}) custom-call(bf16[128,1024]{1,0:T(8,128)(2,1)S(1)} %get-tuple-element.23.mine_ref, bf16[128,2048]{1,0:T(8,128)(2,1)S(1)} %copy-done, bf16[512,2048]{1,0:T(8,128)(2,1)S(1)} %get-tuple-element.24.w_ref, bf16[2048,2048]{1,0:T(8,128)(2,1)} %w_hbm.3), custom_call_target="tpu_custom_call" | custom-call | flops 1000000000 | bytes 1048576 | tf_op jit(solution)/shard_map/project/pallas_call | solution.py:463
  40.5 0.0 collective-permute-done.1.other_ref
  40.5 0.0 copy-done.9
  40.5 0.0 copy-done.10
  40.5 0.0 copy-start.7
  40.5 0.0 copy-start.8
  40.5 2.2 %dispatch.1 = (bf16[128,2048]{1,0:T(8,128)(2,1)S(1)}, bf16[1024,2048]{1,0:T(8,128)(2,1)S(1)}) custom-call(bf16[128,1024]{1,0:T(8,128)(2,1)S(1)} %collective-permute-done.1.other_ref, bf16[1024,2048]{1,0:T(8,128)(2,1)S(1)} %get-tuple-element.25.rest_ref, f32[128,2048]{1,0:T(8,128)S(1)} %get-tuple-element.26.acc_ref, f32[1,2048]{1,0:T(1,128)S(1)} %bitcast.15, ...), custom_call_target="tpu_custom_call" | custom-call | flops 2000000000 | bytes 1048576 | tf_op jit(solution)/shard_map/dispatch/pallas_call | solution.py:472
  42.8 0.0 copy-start.3
  42.8 0.0 copy-start.4
  42.8 0.0 copy-start.5
  42.8 0.0 copy-start.6
  42.8 56.3 %all_to_all.15 = bf16[128,8,2048]{2,1,0:T(8,128)(2,1)S(1)} all-to-all(bf16[128,8,2048]{2,1,0:T(8,128)(2,1)S(1)} %bitcast.11), channel_id=1, replica_groups=mesh['sp'=64,'tp'=2] {'sp','tp'}, dimensions={0} | all-to-all | bytes 8388608 | tf_op jit(solution)/shard_map/all_to_all | solution.py:483
  99.1 0.0 copy-done.7
  99.1 0.0 copy-done.8
  99.1 0.0 copy-done.3
  99.1 0.0 copy-done.4
  99.1 0.0 copy-done.5
  99.1 0.0 copy-done.6
  99.1 7.9 %expert.1 = (bf16[1024,2048]{1,0:T(8,128)(2,1)S(1)}, f32[128,2048]{1,0:T(8,128)S(1)}) custom-call(bf16[1024,2048]{1,0:T(8,128)(2,1)S(1)} %bitcast.12, bf16[1,2048,512]{2,1,0:T(8,128)(2,1)S(1)} %copy-done.3, bf16[1,2048,512]{2,1,0:T(8,128)(2,1)S(1)} %copy-done.4, bf16[1,512,2048]{2,1,0:T(8,128)(2,1)S(1)} %copy-done.5, ...), custom_call_target="tpu_custom_call" | custom-call | flops 7000000000 | bytes 1048576 | tf_op jit(solution)/shard_map/expert/pallas_call | solution.py:487
  107.1 0.0 copy-start.1
  107.1 0.0 copy-start.2
  107.1 57.0 %all_to_all.16 = bf16[128,8,2048]{2,1,0:T(8,128)(2,1)S(1)} all-to-all(bf16[128,8,2048]{2,1,0:T(8,128)(2,1)S(1)} %bitcast.13), channel_id=1, replica_groups=mesh['sp'=64,'tp'=2] {'sp','tp'}, dimensions={0} | all-to-all | bytes 8388608 | tf_op jit(solution)/shard_map/all_to_all | solution.py:483
  164.1 0.0 copy-done.1
  164.1 0.0 copy-done.2
  164.1 1.8 %finish.1 = bf16[128,2048]{1,0:T(8,128)(2,1)} custom-call(f32[128,2048]{1,0:T(8,128)S(1)} %get-tuple-element.30.base_ref, bf16[128,1024]{1,0:T(8,128)(2,1)S(1)} %copy-done.1, bf16[1024,2048]{1,0:T(8,128)(2,1)S(1)} %bitcast.10, f32[1,2048]{1,0:T(1,128)S(1)} %bitcast.14), custom_call_target="tpu_custom_call" | custom-call | flops 1000000000 | bytes 1048576 | tf_op jit(solution)/shard_map/finish/pallas_call | solution.py:498
Async XLA Ops:
  0.7 5.4 %collective-permute-start = (bf16[3,1024]{1,0:T(4,128)(2,1)S(1)}, bf16[3,1024]{1,0:T(4,128)(2,1)S(1)}, u32[]{:S(2)}, u32[]{:S(2)}) collective-permute-start(bf16[3,1024]{1,0:T(4,128)(2,1)S(1)} %slice.3), channel_id=1, source_target_pairs={{0,2},{2,4},{4,6},{6,8},{8,10},{10,12},{12,14},{14,16},{16,18},{18... | collective-permute-start | bytes 18440 | tf_op jit(solution)/shard_map/ppermute | solution.py:396
  11.4 20.5 %all-to-all-start = ((bf16[64,16,128]{2,1,0:T(8,128)(2,1)}), bf16[64,16,128]{2,1,0:T(8,128)(2,1)S(1)}, u32[]{:S(2)}, u32[]{:S(2)}) async-start(bf16[64,16,128]{2,1,0:T(8,128)(2,1)} %get-tuple-element.19), calls=%async_computation | async-start | bytes 524288 | tf_op jit(solution)/shard_map/all_to_all | solution.py:442
  31.9 5.7 %copy-start = (bf16[128,2048]{1,0:T(8,128)(2,1)S(1)}, bf16[128,2048]{1,0:T(8,128)(2,1)}, u32[]{:S(2)}) copy-start(bf16[128,2048]{1,0:T(8,128)(2,1)} %res_ref.1) | copy-start | bytes 1572868
  34.2 6.3 %collective-permute-start.1 = (bf16[128,1024]{1,0:T(8,128)(2,1)S(1)}, bf16[128,1024]{1,0:T(8,128)(2,1)S(1)}, u32[]{:S(2)}, u32[]{:S(2)}) collective-permute-start(bf16[128,1024]{1,0:T(8,128)(2,1)S(1)} %get-tuple-element.22), channel_id=1, source_target_pairs={{0,1},{1,0},{2,3},{3,2},{4,5},{5,4},{6,7},{7,6},{8,9},{9,8},{10,11... | collective-permute-start | bytes 786440 | tf_op jit(solution)/shard_map/ppermute | solution.py:461
  37.5 3.0 %copy-start.9 = (f32[2048]{0:T(1024)S(1)}, f32[2048]{0:T(1024)}, u32[]{:S(2)}) copy-start(f32[2048]{0:T(1024)} %param.28) | copy-start | bytes 24580
  37.5 3.0 %copy-start.10 = (bf16[1024,128]{1,0:T(8,128)(2,1)S(1)}, bf16[1024,128]{1,0:T(8,128)(2,1)}, u32[]{:S(2)}) copy-start(bf16[1024,128]{1,0:T(8,128)(2,1)} %get-tuple-element.27.g_ref) | copy-start | bytes 786436
  40.5 58.6 %copy-start.7 = (bf16[2048,512]{1,0:T(8,128)(2,1)S(1)}, bf16[2048,512]{1,0:T(8,128)(2,1)}, u32[]{:S(2)}) copy-start(bf16[2048,512]{1,0:T(8,128)(2,1)} %sup_ref.1) | copy-start | bytes 6291460
  40.5 58.6 %copy-start.8 = (bf16[512,2048]{1,0:T(8,128)(2,1)S(1)}, bf16[512,2048]{1,0:T(8,128)(2,1)}, u32[]{:S(2)}) copy-start(bf16[512,2048]{1,0:T(8,128)(2,1)} %sdown_ref.1) | copy-start | bytes 6291460
  42.8 56.4 %copy-start.3 = (bf16[1,2048,512]{2,1,0:T(8,128)(2,1)S(1)}, bf16[1,2048,512]{2,1,0:T(8,128)(2,1)}, u32[]{:S(2)}) copy-start(bf16[1,2048,512]{2,1,0:T(8,128)(2,1)} %gate_ref.1) | copy-start | bytes 6291460
  42.8 56.3 %copy-start.4 = (bf16[1,2048,512]{2,1,0:T(8,128)(2,1)S(1)}, bf16[1,2048,512]{2,1,0:T(8,128)(2,1)}, u32[]{:S(2)}) copy-start(bf16[1,2048,512]{2,1,0:T(8,128)(2,1)} %up_ref.1) | copy-start | bytes 6291460
  42.8 56.3 %copy-start.5 = (bf16[1,512,2048]{2,1,0:T(8,128)(2,1)S(1)}, bf16[1,512,2048]{2,1,0:T(8,128)(2,1)}, u32[]{:S(2)}) copy-start(bf16[1,512,2048]{2,1,0:T(8,128)(2,1)} %down_ref.1) | copy-start | bytes 6291460
  42.8 56.3 %copy-start.6 = (bf16[2048,512]{1,0:T(8,128)(2,1)S(1)}, bf16[2048,512]{1,0:T(8,128)(2,1)}, u32[]{:S(2)}) copy-start(bf16[2048,512]{1,0:T(8,128)(2,1)} %sgate_ref.1) | copy-start | bytes 6291460
  107.1 57.0 %copy-start.1 = (bf16[128,1024]{1,0:T(8,128)(2,1)S(1)}, bf16[128,1024]{1,0:T(8,128)(2,1)}, u32[]{:S(2)}) copy-start(bf16[128,1024]{1,0:T(8,128)(2,1)} %get-tuple-element.31.c_ref) | copy-start | bytes 786436
  107.1 57.0 %copy-start.2 = (f32[2048]{0:T(1024)S(1)}, f32[2048]{0:T(1024)}, u32[]{:S(2)}) copy-start(f32[2048]{0:T(1024)} %param.37) | copy-start | bytes 24580

commit v10 on v9

--- a/solution.py
+++ b/solution.py
@@ -260,9 +260,10 @@
     half = tokens // 2
     strip = channels // 2
     pairs = []
-    for j in range(4):
-        rows = pl.ds(j * (tokens // 4), tokens // 4)
-        pairs.append((mixed_hbm.at[pl.ds(0, 2), rows, :], mixed_ref.at[:, rows, :]))
+    for j in range(2):
+        at = pl.multiple_of((1 - side if j == 0 else side) * half, half)
+        for k in range(2):
+            pairs.append((mixed_hbm.at[k, pl.ds(at, half), :], mixed_ref.at[k, pl.ds(j * half, half), :]))
     pairs.append((w_hbm.at[pl.ds(pl.multiple_of(side * channels, strip), strip), :], w_ref))
     copies = fetch(pairs, sems)
     carried = jnp.zeros((LANES, 128), F32)
@@ -271,19 +272,18 @@
         carried = jnp.where(i < here, jnp.exp(pair[:LANES]) * carried + pair[LANES:], carried)
     carried = jnp.concatenate([carried[i : i + 1] for i in range(LANES)], axis=1)
     block = 16
-    for copy in copies[:4]:
-        copy.wait()
-
-    def put(i, _):
-        at = pl.multiple_of(i * block, block)
-        for ref, part in ((theirs_ref, 1 - side), (mine_ref, side)):
-            rows = pl.ds(pl.multiple_of(part * half + at, block), block)
-            ref[pl.ds(at, block), :] = (mixed_ref[0, rows, :] + mixed_ref[1, rows, :] * carried).astype(
-                BF16
-            )
-        return 0
-
-    lax.fori_loop(0, half // block, put, 0, unroll=2)
+    for j, ref in enumerate((theirs_ref, mine_ref)):
+        for copy in copies[2 * j : 2 * j + 2]:
+            copy.wait()
+
+        def put(i, _):
+            rows = pl.ds(pl.multiple_of(j * half + i * block, block), block)
+            ref[pl.ds(pl.multiple_of(i * block, block), block), :] = (
+                mixed_ref[0, rows, :] + mixed_ref[1, rows, :] * carried
+            ).astype(BF16)
+            return 0
+
+        lax.fori_loop(0, half // block, put, 0, unroll=2)
     for copy in copies[4:]:
         copy.wait()
 

time: 166 us -> 166 us (level)
  no operation moved by 1% of the time
where the time goes in v10:
time: 166 us
  blocking collectives  113 us (68%)
  Pallas kernels  26.1 us (16%)
  starting transfers between devices  18.2 us (11%)
  waiting for transfers between devices  5.95 us (4%)
    all_to_all x2, blocking collectives, exchanged(): x = lax.all_to_all(x, ('sp', 'tp'), split_axis=0, concat_axis=0, tiled=True)  113 us
    all_to_all x1, starting transfers between devices, on_device(): seen = lax.all_to_all(totals, 'sp', 0, 0, tiled=True)  11 us
    pallas_call x1, Pallas kernels, on_device(): call(expert_kernel, (shape((slots, model), BF16), wide), [VMEM] * 8, 7 *...  7.93 us
    all_to_all x1, waiting for transfers between devices, on_device(): seen = lax.all_to_all(totals, 'sp', 0, 0, tiled=True)  5.94 us
    pallas_call x1, Pallas kernels, on_device(): call(scan_kernel, made, [VMEM] * 2 + [HBM] * 3, 10 ** 9, [pltpu.VMEM(x.sh...  5.3 us
    ppermute x1, starting transfers between devices, on_device(): lax.ppermute(conv_in[tokens - reach:], 'sp', [(i, i + 1) for i in range(s...  3.92 us
    pallas_call x1, Pallas kernels, staged(): call(kernel, made, [HBM] * len(operands), flops, held + scratch, name=nam...  3.52 us
    ppermute x1, starting transfers between devices, on_device(): other = lax.ppermute(theirs, 'tp', [(0, 1), (1, 0)])  3.32 us
  transfers between devices with their start and end apart: 3, of which 1 were waited for; matrix products, arithmetic and copies ran while one was open for 1% of the time, Pallas kernels for 4%

profile of v10, /device:TPU:1, one launch (start us, length us, event | category | flops | bytes accessed | tf_op | source)
XLA Modules:
  0.0 165.9 jit_solution(4435515176375398873)
XLA Ops:
  0.0 0.7 slice.3
  0.7 3.9 %collective-permute-start = (bf16[3,1024]{1,0:T(4,128)(2,1)S(1)}, bf16[3,1024]{1,0:T(4,128)(2,1)S(1)}, u32[]{:S(2)}, u32[]{:S(2)}) collective-permute-start(bf16[3,1024]{1,0:T(4,128)(2,1)S(1)} %slice.3), channel_id=1, source_target_pairs={{0,2},{2,4},{4,6},{6,8},{8,10},{10,12},{12,14},{14,16},{16,18},{18... | collective-permute-start | bytes 18440 | tf_op jit(solution)/shard_map/ppermute | solution.py:396
  4.7 0.7 convert_element_type.5
  5.4 0.7 select_maximum_fusion.small_ref
  6.1 0.0 collective-permute-done.halo_ref
  6.1 5.3 %scan.1 = (bf16[64,16,128]{2,1,0:T(8,128)(2,1)}, f32[2,8,264,128]{3,2,1,0:T(8,128)}) custom-call(bf16[3,1024]{1,0:T(4,128)(2,1)S(1)} %collective-permute-done.halo_ref, f32[9,1024]{1,0:T(8,128)S(1)} %select_maximum_fusion.small_ref, bf16[256,1024]{1,0:T(8,128)(2,1)} %x_hbm.1, bf16[4,256,256]{2,1,0:T(8,128)(2,1)} %rmap_hbm.1, bf16[4,256,256]{2,1,0:T(8,128)(2,1)} %imap_hbm.1), custom_call_target="tpu_custom_call" | custom-call | flops 1000000000 | bytes 1048576 | tf_op jit(solution)/shard_map/scan/pallas_call | solution.py:431
  11.4 11.0 %all-to-all-start = ((bf16[64,16,128]{2,1,0:T(8,128)(2,1)}), bf16[64,16,128]{2,1,0:T(8,128)(2,1)S(1)}, u32[]{:S(2)}, u32[]{:S(2)}) async-start(bf16[64,16,128]{2,1,0:T(8,128)(2,1)} %get-tuple-element.19), calls=%async_computation | async-start | bytes 524288 | tf_op jit(solution)/shard_map/all_to_all | solution.py:442
  22.4 3.5 %side.1 = (f32[8,256,1024]{2,1,0:T(8,128)}, bf16[1024,128]{1,0:T(8,128)(2,1)}, bf16[128,1024]{1,0:T(8,128)(2,1)}) custom-call(bf16[256,1024]{1,0:T(8,128)(2,1)} %gate_hbm.1, s32[4,128]{1,0:T(4,128)} %bitcast.18, f32[4,128]{1,0:T(4,128)} %bitcast.19, f32[2,8,264,128]{3,2,1,0:T(8,128)} %get-tuple-element.20.run_hbm), custom_call_target="tpu_custom_call" | custom-call | flops 10000000000 | bytes 1048576 | tf_op jit(solution)/shard_map/side/pallas_call | solution.py:407
  25.9 5.9 %all-to-all-done.seen_ref = bf16[64,16,128]{2,1,0:T(8,128)(2,1)S(1)} async-done(((bf16[64,16,128]{2,1,0:T(8,128)(2,1)}), bf16[64,16,128]{2,1,0:T(8,128)(2,1)S(1)}, u32[]{:S(2)}, u32[]{:S(2)}) %all-to-all-start) | async-done | bytes 262176 | tf_op jit(solution)/shard_map/all_to_all | solution.py:442
  31.9 0.0 copy-start
  31.9 2.4 %mix.1 = (bf16[128,1024]{1,0:T(8,128)(2,1)S(1)}, bf16[128,1024]{1,0:T(8,128)(2,1)S(1)}, bf16[512,2048]{1,0:T(8,128)(2,1)S(1)}) custom-call(bf16[64,16,128]{2,1,0:T(8,128)(2,1)S(1)} %all-to-all-done.seen_ref, f32[8,256,1024]{2,1,0:T(8,128)} %get-tuple-element.21.mixed_hbm, bf16[2048,2048]{1,0:T(8,128)(2,1)} %w_hbm.3), custom_call_target="tpu_custom_call" | custom-call | flops 100000000 | bytes 1048576 | tf_op jit(solution)/shard_map/mix/pallas_call | solution.py:452
  34.2 3.3 %collective-permute-start.1 = (bf16[128,1024]{1,0:T(8,128)(2,1)S(1)}, bf16[128,1024]{1,0:T(8,128)(2,1)S(1)}, u32[]{:S(2)}, u32[]{:S(2)}) collective-permute-start(bf16[128,1024]{1,0:T(8,128)(2,1)S(1)} %get-tuple-element.22), channel_id=1, source_target_pairs={{0,1},{1,0},{2,3},{3,2},{4,5},{5,4},{6,7},{7,6},{8,9},{9,8},{10,11... | collective-permute-start | bytes 786440 | tf_op jit(solution)/shard_map/ppermute | solution.py:461
  37.5 0.0 copy-done
  37.5 0.0 copy-start.9
  37.5 0.0 copy-start.10
  37.6 2.9 %project.1 = (f32[128,2048]{1,0:T(8,128)S(1)}, bf16[1024,2048]{1,0:T(8,128)(2,1)S(1)}) custom-call(bf16[128,1024]{1,0:T(8,128)(2,1)S(1)} %get-tuple-element.23.mine_ref, bf16[128,2048]{1,0:T(8,128)(2,1)S(1)} %copy-done, bf16[512,2048]{1,0:T(8,128)(2,1)S(1)} %get-tuple-element.24.w_ref, bf16[2048,2048]{1,0:T(8,128)(2,1)} %w_hbm.3), custom_call_target="tpu_custom_call" | custom-call | flops 1000000000 | bytes 1048576 | tf_op jit(solution)/shard_map/project/pallas_call | solution.py:463
  40.5 0.0 collective-permute-done.1.other_ref
  40.5 0.0 copy-done.9
  40.5 0.0 copy-done.10
  40.5 0.0 copy-start.7
  40.5 0.0 copy-start.8
  40.5 2.2 %dispatch.1 = (bf16[128,2048]{1,0:T(8,128)(2,1)S(1)}, bf16[1024,2048]{1,0:T(8,128)(2,1)S(1)}) custom-call(bf16[128,1024]{1,0:T(8,128)(2,1)S(1)} %collective-permute-done.1.other_ref, bf16[1024,2048]{1,0:T(8,128)(2,1)S(1)} %get-tuple-element.25.rest_ref, f32[128,2048]{1,0:T(8,128)S(1)} %get-tuple-element.26.acc_ref, f32[1,2048]{1,0:T(1,128)S(1)} %bitcast.15, ...), custom_call_target="tpu_custom_call" | custom-call | flops 2000000000 | bytes 1048576 | tf_op jit(solution)/shard_map/dispatch/pallas_call | solution.py:472
  42.8 0.0 copy-start.3
  42.8 0.0 copy-start.4
  42.8 0.0 copy-start.5
  42.8 0.0 copy-start.6
  42.8 56.3 %all_to_all.15 = bf16[128,8,2048]{2,1,0:T(8,128)(2,1)S(1)} all-to-all(bf16[128,8,2048]{2,1,0:T(8,128)(2,1)S(1)} %bitcast.11), channel_id=1, replica_groups=mesh['sp'=64,'tp'=2] {'sp','tp'}, dimensions={0} | all-to-all | bytes 8388608 | tf_op jit(solution)/shard_map/all_to_all | solution.py:483
  99.1 0.0 copy-done.7
  99.1 0.0 copy-done.8
  99.1 0.0 copy-done.3
  99.1 0.0 copy-done.4
  99.1 0.0 copy-done.5
  99.2 0.0 copy-done.6
  99.2 7.9 %expert.1 = (bf16[1024,2048]{1,0:T(8,128)(2,1)S(1)}, f32[128,2048]{1,0:T(8,128)S(1)}) custom-call(bf16[1024,2048]{1,0:T(8,128)(2,1)S(1)} %bitcast.12, bf16[1,2048,512]{2,1,0:T(8,128)(2,1)S(1)} %copy-done.3, bf16[1,2048,512]{2,1,0:T(8,128)(2,1)S(1)} %copy-done.4, bf16[1,512,2048]{2,1,0:T(8,128)(2,1)S(1)} %copy-done.5, ...), custom_call_target="tpu_custom_call" | custom-call | flops 7000000000 | bytes 1048576 | tf_op jit(solution)/shard_map/expert/pallas_call | solution.py:487
  107.1 0.0 copy-start.1
  107.1 0.0 copy-start.2
  107.1 57.0 %all_to_all.16 = bf16[128,8,2048]{2,1,0:T(8,128)(2,1)S(1)} all-to-all(bf16[128,8,2048]{2,1,0:T(8,128)(2,1)S(1)} %bitcast.13), channel_id=1, replica_groups=mesh['sp'=64,'tp'=2] {'sp','tp'}, dimensions={0} | all-to-all | bytes 8388608 | tf_op jit(solution)/shard_map/all_to_all | solution.py:483
  164.1 0.0 copy-done.1
  164.1 0.0 copy-done.2
  164.1 1.8 %finish.1 = bf16[128,2048]{1,0:T(8,128)(2,1)} custom-call(f32[128,2048]{1,0:T(8,128)S(1)} %get-tuple-element.30.base_ref, bf16[128,1024]{1,0:T(8,128)(2,1)S(1)} %copy-done.1, bf16[1024,2048]{1,0:T(8,128)(2,1)S(1)} %bitcast.10, f32[1,2048]{1,0:T(1,128)S(1)} %bitcast.14), custom_call_target="tpu_custom_call" | custom-call | flops 1000000000 | bytes 1048576 | tf_op jit(solution)/shard_map/finish/pallas_call | solution.py:498
Async XLA Ops:
  0.7 5.4 %collective-permute-start = (bf16[3,1024]{1,0:T(4,128)(2,1)S(1)}, bf16[3,1024]{1,0:T(4,128)(2,1)S(1)}, u32[]{:S(2)}, u32[]{:S(2)}) collective-permute-start(bf16[3,1024]{1,0:T(4,128)(2,1)S(1)} %slice.3), channel_id=1, source_target_pairs={{0,2},{2,4},{4,6},{6,8},{8,10},{10,12},{12,14},{14,16},{16,18},{18... | collective-permute-start | bytes 18440 | tf_op jit(solution)/shard_map/ppermute | solution.py:396
  11.4 20.5 %all-to-all-start = ((bf16[64,16,128]{2,1,0:T(8,128)(2,1)}), bf16[64,16,128]{2,1,0:T(8,128)(2,1)S(1)}, u32[]{:S(2)}, u32[]{:S(2)}) async-start(bf16[64,16,128]{2,1,0:T(8,128)(2,1)} %get-tuple-element.19), calls=%async_computation | async-start | bytes 524288 | tf_op jit(solution)/shard_map/all_to_all | solution.py:442
  31.9 5.7 %copy-start = (bf16[128,2048]{1,0:T(8,128)(2,1)S(1)}, bf16[128,2048]{1,0:T(8,128)(2,1)}, u32[]{:S(2)}) copy-start(bf16[128,2048]{1,0:T(8,128)(2,1)} %res_ref.1) | copy-start | bytes 1572868
  34.2 6.3 %collective-permute-start.1 = (bf16[128,1024]{1,0:T(8,128)(2,1)S(1)}, bf16[128,1024]{1,0:T(8,128)(2,1)S(1)}, u32[]{:S(2)}, u32[]{:S(2)}) collective-permute-start(bf16[128,1024]{1,0:T(8,128)(2,1)S(1)} %get-tuple-element.22), channel_id=1, source_target_pairs={{0,1},{1,0},{2,3},{3,2},{4,5},{5,4},{6,7},{7,6},{8,9},{9,8},{10,11... | collective-permute-start | bytes 786440 | tf_op jit(solution)/shard_map/ppermute | solution.py:461
  37.5 3.0 %copy-start.9 = (f32[2048]{0:T(1024)S(1)}, f32[2048]{0:T(1024)}, u32[]{:S(2)}) copy-start(f32[2048]{0:T(1024)} %param.28) | copy-start | bytes 24580
  37.5 3.0 %copy-start.10 = (bf16[1024,128]{1,0:T(8,128)(2,1)S(1)}, bf16[1024,128]{1,0:T(8,128)(2,1)}, u32[]{:S(2)}) copy-start(bf16[1024,128]{1,0:T(8,128)(2,1)} %get-tuple-element.27.g_ref) | copy-start | bytes 786436
  40.5 58.6 %copy-start.7 = (bf16[2048,512]{1,0:T(8,128)(2,1)S(1)}, bf16[2048,512]{1,0:T(8,128)(2,1)}, u32[]{:S(2)}) copy-start(bf16[2048,512]{1,0:T(8,128)(2,1)} %sup_ref.1) | copy-start | bytes 6291460
  40.5 58.6 %copy-start.8 = (bf16[512,2048]{1,0:T(8,128)(2,1)S(1)}, bf16[512,2048]{1,0:T(8,128)(2,1)}, u32[]{:S(2)}) copy-start(bf16[512,2048]{1,0:T(8,128)(2,1)} %sdown_ref.1) | copy-start | bytes 6291460
  42.8 56.4 %copy-start.3 = (bf16[1,2048,512]{2,1,0:T(8,128)(2,1)S(1)}, bf16[1,2048,512]{2,1,0:T(8,128)(2,1)}, u32[]{:S(2)}) copy-start(bf16[1,2048,512]{2,1,0:T(8,128)(2,1)} %gate_ref.1) | copy-start | bytes 6291460
  42.8 56.3 %copy-start.4 = (bf16[1,2048,512]{2,1,0:T(8,128)(2,1)S(1)}, bf16[1,2048,512]{2,1,0:T(8,128)(2,1)}, u32[]{:S(2)}) copy-start(bf16[1,2048,512]{2,1,0:T(8,128)(2,1)} %up_ref.1) | copy-start | bytes 6291460
  42.8 56.3 %copy-start.5 = (bf16[1,512,2048]{2,1,0:T(8,128)(2,1)S(1)}, bf16[1,512,2048]{2,1,0:T(8,128)(2,1)}, u32[]{:S(2)}) copy-start(bf16[1,512,2048]{2,1,0:T(8,128)(2,1)} %down_ref.1) | copy-start | bytes 6291460
  42.8 56.3 %copy-start.6 = (bf16[2048,512]{1,0:T(8,128)(2,1)S(1)}, bf16[2048,512]{1,0:T(8,128)(2,1)}, u32[]{:S(2)}) copy-start(bf16[2048,512]{1,0:T(8,128)(2,1)} %sgate_ref.1) | copy-start | bytes 6291460
  107.1 57.0 %copy-start.1 = (bf16[128,1024]{1,0:T(8,128)(2,1)S(1)}, bf16[128,1024]{1,0:T(8,128)(2,1)}, u32[]{:S(2)}) copy-start(bf16[128,1024]{1,0:T(8,128)(2,1)} %get-tuple-element.31.c_ref) | copy-start | bytes 786436
  107.1 57.0 %copy-start.2 = (f32[2048]{0:T(1024)S(1)}, f32[2048]{0:T(1024)}, u32[]{:S(2)}) copy-start(f32[2048]{0:T(1024)} %param.37) | copy-start | bytes 24580
